TPU v7x, 512 devices: a whole 4x8x8 slice. The times are simulated.
512 devices in a mesh: rep: 2 (over z_hi), fs: 32 (over z_lo, y), tp: 8 (over x, core).
Axes of the slice: x: 4, y: 8, z: 8 (z_hi: 2, z_lo: 4; z = z_hi * 4 + z_lo), core: 2. Of those that a mesh axis runs over, the one named last changes fastest.
Arguments:
- later_input: bfloat16 [8192, 2048], P(('rep', 'fs')), may hold values from -6 to 6
- earlier_input: bfloat16 [8192, 2048], P(('rep', 'fs')), may hold values from -6 to 6
- cotangent: bfloat16 [8192, 2048], P(('rep', 'fs')), may hold values from -16 to 16
- gate_weight: bfloat16 [2048, 3072], P('fs', 'tp'), may hold values from -0.125 to 0.125
- up_weight: bfloat16 [2048, 3072], P('fs', 'tp'), may hold values from -0.125 to 0.125
- down_weight: bfloat16 [2048, 3072], P('fs', 'tp'), may hold values from -0.109375 to 0.109375
- gate_sum: float32 [2048, 3072], P('fs', 'tp'), may hold values from -192 to 192
- up_sum: float32 [2048, 3072], P('fs', 'tp'), may hold values from -192 to 192
- down_sum: float32 [2048, 3072], P('fs', 'tp'), may hold values from -192 to 192
Outputs:
- later_output: bfloat16 [8192, 2048], P(('rep', 'fs'))
- earlier_input_grad: bfloat16 [8192, 2048], P(('rep', 'fs'))
- gate_sum_new: float32 [2048, 3072], P('fs', 'tp')
- up_sum_new: float32 [2048, 3072], P('fs', 'tp')
- down_sum_new: float32 [2048, 3072], P('fs', 'tp')
All inputs are finite; a program needn't handle non-finite values.
Results may differ from a plain program's by a relative error of at most 0.02.
Values may be sent and summed in bfloat16 or wider, within the bound.
No kernel may reach another device: no remote copies, remote signals or barrier semaphores. Data moves between devices by JAX's collectives and lax.ppermute only.
A program may use at most 128 MiB of HBM per device.

v0:
```python
import jax
import jax.numpy as jnp
from jax import lax
from jax.sharding import Mesh, PartitionSpec as P


NZ = 8
NZL = 4
NY = 8
RING = ("zh", "zl")
TP = ("x", "c")
SHIFTS = (1, -1, -2)


def shift_z(array, by):
    return lax.ppermute(array, RING, [(i, (i + by) % NZ) for i in range(NZ)])


def contract_last(first, second):
    return lax.dot_general(
        first, second, (((1,), (1,)), ((), ())), preferred_element_type=jnp.float32
    )


def contract_first(first, second):
    return lax.dot_general(
        first, second, (((0,), (0,)), ((), ())), preferred_element_type=jnp.float32
    )


def dot(first, second):
    return jnp.dot(first, second, preferred_element_type=jnp.float32)


def shift(array, axis, count, by):
    return lax.ppermute(array, axis, [(i, (i + by) % count) for i in range(count)])


def put(buffer, block, at, dim=0):
    return lax.dynamic_update_slice_in_dim(buffer, jnp.expand_dims(block, dim), at, dim)


def swap_columns(array, outer, inner):
    rows, columns = array.shape
    parts = array.reshape(rows, outer, inner, columns // (outer * inner))
    return parts.transpose(0, 2, 1, 3).reshape(rows, columns)


def spread_y(block):
    copies = jnp.broadcast_to(block, (NY, *block.shape))
    return lax.all_to_all(copies, "y", split_axis=0, concat_axis=0, tiled=True)


def gather_z_then_y(shard, zl):
    near = jnp.zeros((NZL, *shard.shape), shard.dtype)
    near = put(near, shard, zl)
    for by in SHIFTS:
        block = shift_z(shard, by)
        near = put(near, block, jnp.mod(zl - by + NZL, NZL))
    return spread_y(near)


def gather_y_then_z(shard, zl):
    column = spread_y(shard)
    full = jnp.zeros((NY, NZL, *shard.shape), shard.dtype)
    full = put(full, column, zl, 1)
    for by in (1, -1):
        block = shift_z(column, by)
        full = put(full, block, jnp.mod(zl - by + NZL, NZL), 1)
    far_low = shift_z(column[: NY // 2], 2)
    far_high = shift_z(column[NY // 2 :], -2)
    far = jnp.concatenate((far_low, far_high), axis=0)
    return put(full, far, jnp.mod(zl + 2, NZL), 1)


def reduce_on_tp(late, early, x, c):
    n_x = lax.axis_size("x")
    tokens, width = late.shape
    cut = lambda a: a.reshape(n_x, 2, tokens // (2 * n_x), width)
    both = jnp.concatenate((cut(late), cut(early)), axis=2)
    pick = lambda at: lax.dynamic_index_in_dim(both, at, 1, keepdims=False)
    other = lax.ppermute(pick(1 - c), "c", [(0, 1), (1, 0)])
    pair = (pick(c).astype(jnp.float32) + other.astype(jnp.float32)).astype(late.dtype)
    part = lambda at: lax.dynamic_index_in_dim(pair, at, 0, keepdims=False)
    total = part(x).astype(jnp.float32)
    for by in (1, -1, 2):
        block = part(jnp.mod(x + by + n_x, n_x))
        sent = shift(block, "x", n_x, by)
        total = total + sent.astype(jnp.float32)
    return total.astype(late.dtype)


def everywhere_on_tp(own, x, c):
    n_x = lax.axis_size("x")
    line = jnp.zeros((n_x, *own.shape), own.dtype)
    line = put(line, own, x)
    for by in (1, -1, 2):
        line = put(line, shift(own, "x", n_x, by), jnp.mod(x - by + n_x, n_x))
    other = lax.ppermute(line, "c", [(0, 1), (1, 0)])
    both = jnp.zeros((n_x, 2, *own.shape), own.dtype)
    both = put(both, line, c, 1)
    both = put(both, other, 1 - c, 1)
    return both.reshape(2 * n_x, *own.shape)


def per_device(
    later_input,
    earlier_input,
    cotangent,
    gate_weight,
    up_weight,
    down_weight,
    gate_sum,
    up_sum,
    down_sum,
):
    bf = jnp.bfloat16
    zl = lax.axis_index("zl")
    rows, width = gate_weight.shape
    later_half = jnp.concatenate((up_weight, down_weight), axis=1)
    part_b = gather_y_then_z(later_half, zl).reshape(-1, 2 * width)
    gate_full = gather_z_then_y(gate_weight, zl).reshape(-1, width)
    up_full = part_b[:, :width]
    down_full = part_b[:, width:]

    block = rows * NY

    def features_for(where):
        cut = lambda a: lax.dynamic_slice_in_dim(a, where * block, block, 1)
        return jnp.concatenate((cut(earlier_input), cut(cotangent)), axis=1)

    features = [features_for(zl)]
    for by in SHIFTS:
        sent = features_for(jnp.mod(zl + by + NZL, NZL))
        features.append(shift_z(sent, by))

    early = swap_columns(earlier_input, NZL, NY)
    cot = swap_columns(cotangent, NZL, NY)
    late = swap_columns(later_input, NZL, NY)

    gate_early = dot(early, gate_full)
    up_early = dot(early, up_full)
    hidden_grad = dot(cot, down_full)
    sigmoid_gate = jax.nn.sigmoid(gate_early)
    silu_early = gate_early * sigmoid_gate
    gate_grad = (
        hidden_grad * up_early * sigmoid_gate * (1.0 + gate_early * (1.0 - sigmoid_gate))
    ).astype(bf)
    up_grad = (hidden_grad * silu_early).astype(bf)
    hidden_early = (silu_early * up_early).astype(bf)

    piece = jnp.concatenate((gate_grad, up_grad, hidden_early), axis=1)
    pieces = [piece] + [shift_z(piece, by) for by in SHIFTS]

    gate_late = dot(late, gate_full)
    up_late = dot(late, up_full)
    hidden_late = (jax.nn.silu(gate_late) * up_late).astype(bf)
    partial_late = contract_last(hidden_late, down_full).astype(bf)
    partial_early = (
        contract_last(gate_grad, gate_full) + contract_last(up_grad, up_full)
    ).astype(bf)
    tokens = partial_late.shape[0]
    n_tp = lax.axis_size(TP)
    x, c = lax.axis_index("x"), lax.axis_index("c")
    own = reduce_on_tp(partial_late, partial_early, x, c)
    own = swap_columns(own, NY, NZL)
    outs = everywhere_on_tp(own, x, c)
    later_output = outs[:, : tokens // n_tp].reshape(tokens, -1)
    earlier_input_grad = outs[:, tokens // n_tp :].reshape(tokens, -1)

    first = jnp.concatenate(features, axis=0)
    second = jnp.concatenate(pieces, axis=0)
    both_local = contract_first(first[:, :block], second[:, : 2 * width])
    down_local = contract_first(first[:, block:], second[:, 2 * width :])
    local = jnp.concatenate((both_local.astype(bf), down_local.astype(bf)), axis=1)
    local = local.reshape(NY, rows, 3 * width)
    local = lax.all_to_all(local, "y", split_axis=0, concat_axis=0, tiled=True)
    mine = jnp.sum(local.astype(jnp.float32), axis=0).astype(bf)
    other = lax.ppermute(mine, "zh", [(0, 1), (1, 0)])
    total = mine.astype(jnp.float32) + other.astype(jnp.float32)
    return (
        later_output,
        earlier_input_grad,
        gate_sum + total[:, :width],
        up_sum + total[:, width : 2 * width],
        down_sum + total[:, 2 * width :],
    )


def solution(mesh):
    fine = Mesh(mesh.devices.reshape(2, NZL, NY, -1, 2), ("zh", "zl", "y", "x", "c"))
    tokens = P(("zh", "zl", "y"), None)
    weights = P(("zl", "y"), ("x", "c"))
    return jax.shard_map(
        per_device,
        mesh=fine,
        in_specs=(tokens,) * 3 + (weights,) * 6,
        out_specs=(tokens,) * 2 + (weights,) * 3,
        check_vma=False,
    )
```

profile of v0, /device:TPU:2, one launch (start us, length us, event | category | flops | bytes accessed | tf_op | source)
XLA Modules:
  0.0 206.2 jit_solution(11631240819272314914)
XLA Ops:
  2.4 7.1 %all-to-all-start.1 = ((bf16[8,64,768]{2,1,0:T(8,128)(2,1)}), bf16[8,64,768]{2,1,0:T(8,128)(2,1)S(1)}, u32[]{:S(2)}, u32[]{:S(2)}) async-start(bf16[8,64,768]{2,1,0:T(8,128)(2,1)} %broadcast_in_dim.66), calls=%async_computation.1 | async-start | bytes 1572864 | tf_op jit(solution)/shard_map/all_to_all | solution.py:51
  9.6 4.3 %collective-permute-start = (bf16[64,384]{1,0:T(8,128)(2,1)S(1)}, bf16[64,384]{1,0:T(8,128)(2,1)S(1)}, u32[]{:S(2)}, u32[]{:S(2)}) collective-permute-start(bf16[64,384]{1,0:T(8,128)(2,1)S(1)} %copy-done.13), channel_id=1, source_target_pairs={{0,64},{64,128},{128,192},{192,256},{256,320},{320,384},{384,448},... | collective-permute-start | bytes 147464 | tf_op jit(solution)/shard_map/ppermute | solution.py:16
  13.8 8.6 %collective-permute-start.1 = (bf16[64,384]{1,0:T(8,128)(2,1)S(1)}, bf16[64,384]{1,0:T(8,128)(2,1)S(1)}, u32[]{:S(2)}, u32[]{:S(2)}) collective-permute-start(bf16[64,384]{1,0:T(8,128)(2,1)S(1)} %copy-done.13), channel_id=1, source_target_pairs={{0,448},{64,0},{128,64},{192,128},{256,192},{320,256},{384,320},{4... | collective-permute-start | bytes 147464 | tf_op jit(solution)/shard_map/ppermute | solution.py:16
  22.4 3.9 %collective-permute-start.2 = (bf16[64,384]{1,0:T(8,128)(2,1)S(1)}, bf16[64,384]{1,0:T(8,128)(2,1)S(1)}, u32[]{:S(2)}, u32[]{:S(2)}) collective-permute-start(bf16[64,384]{1,0:T(8,128)(2,1)S(1)} %copy-done.13), channel_id=1, source_target_pairs={{0,384},{64,448},{128,0},{192,64},{256,128},{320,192},{384,256},{4... | collective-permute-start | bytes 147464 | tf_op jit(solution)/shard_map/ppermute | solution.py:16
  34.0 3.9 %all-to-all-start = ((bf16[8,4,64,384]{3,2,1,0:T(8,128)(2,1)}), bf16[8,4,64,384]{3,2,1,0:T(8,128)(2,1)S(1)}, u32[]{:S(2)}, u32[]{:S(2)}) async-start(bf16[8,4,64,384]{3,2,1,0:T(8,128)(2,1)} %broadcast_in_dim.64), calls=%async_computation | async-start | bytes 3145728 | tf_op jit(solution)/shard_map/all_to_all | solution.py:51
  39.5 4.0 %collective-permute-start.15 = (bf16[128,1024]{1,0:T(8,128)(2,1)}, bf16[128,1024]{1,0:T(8,128)(2,1)}, u32[]{:S(2)}, u32[]{:S(2)}) collective-permute-start(bf16[128,1024]{1,0:T(8,128)(2,1)} %pad_maximum_fusion.4), channel_id=1, source_target_pairs={{0,64},{64,128},{128,192},{192,256},{256,320},{320,384},{384,448},... | collective-permute-start | bytes 786440 | tf_op jit(solution)/shard_map/ppermute | solution.py:16
  44.2 8.6 %collective-permute-start.16 = (bf16[128,1024]{1,0:T(8,128)(2,1)}, bf16[128,1024]{1,0:T(8,128)(2,1)}, u32[]{:S(2)}, u32[]{:S(2)}) collective-permute-start(bf16[128,1024]{1,0:T(8,128)(2,1)} %pad_maximum_fusion.5), channel_id=1, source_target_pairs={{0,448},{64,0},{128,64},{192,128},{256,192},{320,256},{384,320},{4... | collective-permute-start | bytes 786440 | tf_op jit(solution)/shard_map/ppermute | solution.py:16
  53.5 3.9 %collective-permute-start.17 = (bf16[128,1024]{1,0:T(8,128)(2,1)}, bf16[128,1024]{1,0:T(8,128)(2,1)}, u32[]{:S(2)}, u32[]{:S(2)}) collective-permute-start(bf16[128,1024]{1,0:T(8,128)(2,1)} %pad_maximum_fusion.6), channel_id=1, source_target_pairs={{0,384},{64,448},{128,0},{192,64},{256,128},{320,192},{384,256},{4... | collective-permute-start | bytes 786440 | tf_op jit(solution)/shard_map/ppermute | solution.py:16
  67.1 3.7 %collective-permute-start.4 = (bf16[8,64,768]{2,1,0:T(8,128)(2,1)S(1)}, bf16[8,64,768]{2,1,0:T(8,128)(2,1)S(1)}, u32[]{:S(2)}, u32[]{:S(2)}) collective-permute-start(bf16[8,64,768]{2,1,0:T(8,128)(2,1)S(1)} %all-to-all-done.1), channel_id=1, source_target_pairs={{0,448},{64,0},{128,64},{192,128},{256,192},{320,256},{384,320},{4... | collective-permute-start | bytes 2359304 | tf_op jit(solution)/shard_map/ppermute | solution.py:16
  73.1 6.3 %collective-permute-start.5 = (bf16[4,64,768]{2,1,0:T(8,128)(2,1)S(1)}, bf16[4,64,768]{2,1,0:T(8,128)(2,1)S(1)}, u32[]{:S(2)}, u32[]{:S(2)}) collective-permute-start(bf16[4,64,768]{2,1,0:T(8,128)(2,1)S(1)} %get-tuple-element.7), channel_id=1, source_target_pairs={{0,128},{64,192},{128,256},{192,320},{256,384},{320,448},{384,0},{... | collective-permute-start | bytes 1179656 | tf_op jit(solution)/shard_map/ppermute | solution.py:16
  84.3 13.5 %collective-permute-done.4 = bf16[8,64,768]{2,1,0:T(8,128)(2,1)S(1)} collective-permute-done((bf16[8,64,768]{2,1,0:T(8,128)(2,1)S(1)}, bf16[8,64,768]{2,1,0:T(8,128)(2,1)S(1)}, u32[]{:S(2)}, u32[]{:S(2)}) %collective-permute-start.4) | collective-permute-done | bytes 786464 | tf_op jit(solution)/shard_map/ppermute | solution.py:16
  97.9 5.8 %collective-permute-done.6 = bf16[4,64,768]{2,1,0:T(8,128)(2,1)S(1)} collective-permute-done((bf16[4,64,768]{2,1,0:T(8,128)(2,1)S(1)}, bf16[4,64,768]{2,1,0:T(8,128)(2,1)S(1)}, u32[]{:S(2)}, u32[]{:S(2)}) %collective-permute-start.6) | collective-permute-done | bytes 393248 | tf_op jit(solution)/shard_map/ppermute | solution.py:16
  109.9 5.8 %collective-permute-start.18 = (bf16[128,1152]{0,1:T(8,128)(2,1)}, bf16[128,1152]{0,1:T(8,128)(2,1)}, u32[]{:S(2)}, u32[]{:S(2)}) collective-permute-start(bf16[128,1152]{0,1:T(8,128)(2,1)} %pad_maximum_fusion.3), channel_id=1, source_target_pairs={{0,64},{64,128},{128,192},{192,256},{256,320},{320,384},{384,448},... | collective-permute-start | bytes 884744 | tf_op jit(solution)/shard_map/ppermute | solution.py:16
  117.6 4.6 %collective-permute-start.20 = (bf16[128,1152]{0,1:T(8,128)(2,1)}, bf16[128,1152]{0,1:T(8,128)(2,1)}, u32[]{:S(2)}, u32[]{:S(2)}) collective-permute-start(bf16[128,1152]{0,1:T(8,128)(2,1)} %pad_maximum_fusion.3), channel_id=1, source_target_pairs={{0,384},{64,448},{128,0},{192,64},{256,128},{320,192},{384,256},{4... | collective-permute-start | bytes 884744 | tf_op jit(solution)/shard_map/ppermute | solution.py:16
  124.2 4.0 %convolution_convert_fusion = bf16[128,2048]{1,0:T(8,128)(2,1)S(1)} fusion(bf16[2048,768]{1,0:T(8,128)(2,1)} %bitcast.113, bf16[128,2048]{0,1:T(8,128)(2,1)} %bitcast.127, f32[128,384]{0,1:T(8,128)} %convolution_bitcast_fusion.1), kind=kOutput, calls=%fused_computation.2 | convolution fusion | flops 403210240 | bytes 4390912 | tf_op jit(solution)/shard_map/dot_general | solution.py:20
  132.4 6.6 %collective-permute-done.20 = bf16[128,1152]{0,1:T(8,128)(2,1)} collective-permute-done((bf16[128,1152]{0,1:T(8,128)(2,1)}, bf16[128,1152]{0,1:T(8,128)(2,1)}, u32[]{:S(2)}, u32[]{:S(2)}) %collective-permute-start.20) | collective-permute-done | bytes 294944 | tf_op jit(solution)/shard_map/ppermute | solution.py:16
  142.6 4.0 %collective-permute-start.10 = (bf16[32,2048]{1,0:T(8,128)(2,1)S(1)}, bf16[32,2048]{1,0:T(8,128)(2,1)S(1)}, u32[]{:S(2)}, u32[]{:S(2)}) collective-permute-start(bf16[32,2048]{1,0:T(8,128)(2,1)S(1)} %get-tuple-element.18), channel_id=1, source_target_pairs={{0,4},{2,6},{4,0},{6,2},{1,5},{3,7},{5,1},{7,3},{8,12},{10,14},{12... | collective-permute-start | bytes 393224 | tf_op jit(solution)/shard_map/ppermute | solution.py:36
  148.6 3.9 %collective-permute-start.9 = (bf16[32,2048]{1,0:T(8,128)(2,1)S(1)}, bf16[32,2048]{1,0:T(8,128)(2,1)S(1)}, u32[]{:S(2)}, u32[]{:S(2)}) collective-permute-start(bf16[32,2048]{1,0:T(8,128)(2,1)S(1)} %get-tuple-element.19), channel_id=1, source_target_pairs={{0,6},{2,0},{4,2},{6,4},{1,7},{3,1},{5,3},{7,5},{8,14},{10,8},{12,... | collective-permute-start | bytes 393224 | tf_op jit(solution)/shard_map/ppermute | solution.py:36
  153.7 6.8 %all-to-all-start.2 = ((bf16[8,64,1152]{2,1,0:T(8,128)(2,1)}), bf16[8,64,1152]{2,1,0:T(8,128)(2,1)S(1)}, u32[]{:S(2)}, u32[]{:S(2)}) async-start(bf16[8,64,1152]{2,1,0:T(8,128)(2,1)} %bitcast.54), calls=%async_computation.2 | async-start | bytes 2359296 | tf_op jit(solution)/shard_map/all_to_all | solution.py:177
  163.3 4.6 %collective-permute-start.12 = (bf16[32,2048]{1,0:T(8,128)(2,1)S(1)}, bf16[32,2048]{1,0:T(8,128)(2,1)S(1)}, u32[]{:S(2)}, u32[]{:S(2)}) collective-permute-start(bf16[32,2048]{1,0:T(8,128)(2,1)S(1)} %reshape.73), channel_id=1, source_target_pairs={{0,6},{2,0},{4,2},{6,4},{1,7},{3,1},{5,3},{7,5},{8,14},{10,8},{12,... | collective-permute-start | bytes 393224 | tf_op jit(solution)/shard_map/ppermute | solution.py:36
  167.9 4.0 %collective-permute-start.13 = (bf16[32,2048]{1,0:T(8,128)(2,1)S(1)}, bf16[32,2048]{1,0:T(8,128)(2,1)S(1)}, u32[]{:S(2)}, u32[]{:S(2)}) collective-permute-start(bf16[32,2048]{1,0:T(8,128)(2,1)S(1)} %reshape.73), channel_id=1, source_target_pairs={{0,4},{2,6},{4,0},{6,2},{1,5},{3,7},{5,1},{7,3},{8,12},{10,14},{12... | collective-permute-start | bytes 393224 | tf_op jit(solution)/shard_map/ppermute | solution.py:36
  172.0 4.2 %collective-permute-done.13 = bf16[32,2048]{1,0:T(8,128)(2,1)S(1)} collective-permute-done((bf16[32,2048]{1,0:T(8,128)(2,1)S(1)}, bf16[32,2048]{1,0:T(8,128)(2,1)S(1)}, u32[]{:S(2)}, u32[]{:S(2)}) %collective-permute-start.13) | collective-permute-done | bytes 131104 | tf_op jit(solution)/shard_map/ppermute | solution.py:36
  180.2 10.3 %all-to-all-done.2 = bf16[8,64,1152]{2,1,0:T(8,128)(2,1)S(1)} async-done(((bf16[8,64,1152]{2,1,0:T(8,128)(2,1)}), bf16[8,64,1152]{2,1,0:T(8,128)(2,1)S(1)}, u32[]{:S(2)}, u32[]{:S(2)}) %all-to-all-start.2) | async-done | bytes 1179680 | tf_op jit(solution)/shard_map/all_to_all | solution.py:177
  194.6 10.8 %collective-permute-done.21 = bf16[64,1152]{1,0:T(8,128)(2,1)S(1)} collective-permute-done((bf16[64,1152]{1,0:T(8,128)(2,1)S(1)}, bf16[64,1152]{1,0:T(8,128)(2,1)S(1)}, u32[]{:S(2)}, u32[]{:S(2)}) %collective-permute-start.21) | collective-permute-done | bytes 147488 | tf_op jit(solution)/shard_map/ppermute | solution.py:179
  (112 shorter events, 61.6 us)
Async XLA Ops:
  2.4 30.2 %all-to-all-start.1 = ((bf16[8,64,768]{2,1,0:T(8,128)(2,1)}), bf16[8,64,768]{2,1,0:T(8,128)(2,1)S(1)}, u32[]{:S(2)}, u32[]{:S(2)}) async-start(bf16[8,64,768]{2,1,0:T(8,128)(2,1)} %broadcast_in_dim.66), calls=%async_computation.1 | async-start | bytes 1572864 | tf_op jit(solution)/shard_map/all_to_all | solution.py:51
  9.6 16.9 %collective-permute-start = (bf16[64,384]{1,0:T(8,128)(2,1)S(1)}, bf16[64,384]{1,0:T(8,128)(2,1)S(1)}, u32[]{:S(2)}, u32[]{:S(2)}) collective-permute-start(bf16[64,384]{1,0:T(8,128)(2,1)S(1)} %copy-done.13), channel_id=1, source_target_pairs={{0,64},{64,128},{128,192},{192,256},{256,320},{320,384},{384,448},... | collective-permute-start | bytes 147464 | tf_op jit(solution)/shard_map/ppermute | solution.py:16
  13.8 12.7 %collective-permute-start.1 = (bf16[64,384]{1,0:T(8,128)(2,1)S(1)}, bf16[64,384]{1,0:T(8,128)(2,1)S(1)}, u32[]{:S(2)}, u32[]{:S(2)}) collective-permute-start(bf16[64,384]{1,0:T(8,128)(2,1)S(1)} %copy-done.13), channel_id=1, source_target_pairs={{0,448},{64,0},{128,64},{192,128},{256,192},{320,256},{384,320},{4... | collective-permute-start | bytes 147464 | tf_op jit(solution)/shard_map/ppermute | solution.py:16
  22.4 6.9 %collective-permute-start.2 = (bf16[64,384]{1,0:T(8,128)(2,1)S(1)}, bf16[64,384]{1,0:T(8,128)(2,1)S(1)}, u32[]{:S(2)}, u32[]{:S(2)}) collective-permute-start(bf16[64,384]{1,0:T(8,128)(2,1)S(1)} %copy-done.13), channel_id=1, source_target_pairs={{0,384},{64,448},{128,0},{192,64},{256,128},{320,192},{384,256},{4... | collective-permute-start | bytes 147464 | tf_op jit(solution)/shard_map/ppermute | solution.py:16
  34.0 72.0 %all-to-all-start = ((bf16[8,4,64,384]{3,2,1,0:T(8,128)(2,1)}), bf16[8,4,64,384]{3,2,1,0:T(8,128)(2,1)S(1)}, u32[]{:S(2)}, u32[]{:S(2)}) async-start(bf16[8,4,64,384]{3,2,1,0:T(8,128)(2,1)} %broadcast_in_dim.64), calls=%async_computation | async-start | bytes 3145728 | tf_op jit(solution)/shard_map/all_to_all | solution.py:51
  39.5 31.3 %collective-permute-start.15 = (bf16[128,1024]{1,0:T(8,128)(2,1)}, bf16[128,1024]{1,0:T(8,128)(2,1)}, u32[]{:S(2)}, u32[]{:S(2)}) collective-permute-start(bf16[128,1024]{1,0:T(8,128)(2,1)} %pad_maximum_fusion.4), channel_id=1, source_target_pairs={{0,64},{64,128},{128,192},{192,256},{256,320},{320,384},{384,448},... | collective-permute-start | bytes 786440 | tf_op jit(solution)/shard_map/ppermute | solution.py:16
  44.2 26.6 %collective-permute-start.16 = (bf16[128,1024]{1,0:T(8,128)(2,1)}, bf16[128,1024]{1,0:T(8,128)(2,1)}, u32[]{:S(2)}, u32[]{:S(2)}) collective-permute-start(bf16[128,1024]{1,0:T(8,128)(2,1)} %pad_maximum_fusion.5), channel_id=1, source_target_pairs={{0,448},{64,0},{128,64},{192,128},{256,192},{320,256},{384,320},{4... | collective-permute-start | bytes 786440 | tf_op jit(solution)/shard_map/ppermute | solution.py:16
  53.5 17.3 %collective-permute-start.17 = (bf16[128,1024]{1,0:T(8,128)(2,1)}, bf16[128,1024]{1,0:T(8,128)(2,1)}, u32[]{:S(2)}, u32[]{:S(2)}) collective-permute-start(bf16[128,1024]{1,0:T(8,128)(2,1)} %pad_maximum_fusion.6), channel_id=1, source_target_pairs={{0,384},{64,448},{128,0},{192,64},{256,128},{320,192},{384,256},{4... | collective-permute-start | bytes 786440 | tf_op jit(solution)/shard_map/ppermute | solution.py:16
  57.4 25.7 %collective-permute-start.3 = (bf16[8,64,768]{2,1,0:T(8,128)(2,1)S(1)}, bf16[8,64,768]{2,1,0:T(8,128)(2,1)}, u32[]{:S(2)}, u32[]{:S(2)}) collective-permute-start(bf16[8,64,768]{2,1,0:T(8,128)(2,1)S(1)} %all-to-all-done.1), channel_id=1, source_target_pairs={{0,64},{64,128},{128,192},{192,256},{256,320},{320,384},{384,448},... | collective-permute-start | bytes 2359304 | tf_op jit(solution)/shard_map/ppermute | solution.py:16
  67.1 30.7 %collective-permute-start.4 = (bf16[8,64,768]{2,1,0:T(8,128)(2,1)S(1)}, bf16[8,64,768]{2,1,0:T(8,128)(2,1)S(1)}, u32[]{:S(2)}, u32[]{:S(2)}) collective-permute-start(bf16[8,64,768]{2,1,0:T(8,128)(2,1)S(1)} %all-to-all-done.1), channel_id=1, source_target_pairs={{0,448},{64,0},{128,64},{192,128},{256,192},{320,256},{384,320},{4... | collective-permute-start | bytes 2359304 | tf_op jit(solution)/shard_map/ppermute | solution.py:16
  73.1 24.8 %collective-permute-start.5 = (bf16[4,64,768]{2,1,0:T(8,128)(2,1)S(1)}, bf16[4,64,768]{2,1,0:T(8,128)(2,1)S(1)}, u32[]{:S(2)}, u32[]{:S(2)}) collective-permute-start(bf16[4,64,768]{2,1,0:T(8,128)(2,1)S(1)} %get-tuple-element.7), channel_id=1, source_target_pairs={{0,128},{64,192},{128,256},{192,320},{256,384},{320,448},{384,0},{... | collective-permute-start | bytes 1179656 | tf_op jit(solution)/shard_map/ppermute | solution.py:16
  79.4 24.3 %collective-permute-start.6 = (bf16[4,64,768]{2,1,0:T(8,128)(2,1)S(1)}, bf16[4,64,768]{2,1,0:T(8,128)(2,1)S(1)}, u32[]{:S(2)}, u32[]{:S(2)}) collective-permute-start(bf16[4,64,768]{2,1,0:T(8,128)(2,1)S(1)} %get-tuple-element.8), channel_id=1, source_target_pairs={{0,384},{64,448},{128,0},{192,64},{256,128},{320,192},{384,256},{4... | collective-permute-start | bytes 1179656 | tf_op jit(solution)/shard_map/ppermute | solution.py:16
  109.9 22.5 %collective-permute-start.18 = (bf16[128,1152]{0,1:T(8,128)(2,1)}, bf16[128,1152]{0,1:T(8,128)(2,1)}, u32[]{:S(2)}, u32[]{:S(2)}) collective-permute-start(bf16[128,1152]{0,1:T(8,128)(2,1)} %pad_maximum_fusion.3), channel_id=1, source_target_pairs={{0,64},{64,128},{128,192},{192,256},{256,320},{320,384},{384,448},... | collective-permute-start | bytes 884744 | tf_op jit(solution)/shard_map/ppermute | solution.py:16
  115.7 16.7 %collective-permute-start.19 = (bf16[128,1152]{0,1:T(8,128)(2,1)}, bf16[128,1152]{0,1:T(8,128)(2,1)}, u32[]{:S(2)}, u32[]{:S(2)}) collective-permute-start(bf16[128,1152]{0,1:T(8,128)(2,1)} %pad_maximum_fusion.3), channel_id=1, source_target_pairs={{0,448},{64,0},{128,64},{192,128},{256,192},{320,256},{384,320},{4... | collective-permute-start | bytes 884744 | tf_op jit(solution)/shard_map/ppermute | solution.py:16
  117.6 21.4 %collective-permute-start.20 = (bf16[128,1152]{0,1:T(8,128)(2,1)}, bf16[128,1152]{0,1:T(8,128)(2,1)}, u32[]{:S(2)}, u32[]{:S(2)}) collective-permute-start(bf16[128,1152]{0,1:T(8,128)(2,1)} %pad_maximum_fusion.3), channel_id=1, source_target_pairs={{0,384},{64,448},{128,0},{192,64},{256,128},{320,192},{384,256},{4... | collective-permute-start | bytes 884744 | tf_op jit(solution)/shard_map/ppermute | solution.py:16
  130.3 12.1 %collective-permute-start.7 = (bf16[4,32,2048]{2,1,0:T(8,128)(2,1)S(1)}, bf16[4,32,2048]{2,1,0:T(8,128)(2,1)S(1)}, u32[]{:S(2)}, u32[]{:S(2)}) collective-permute-start(bf16[4,32,2048]{2,1,0:T(8,128)(2,1)S(1)} %fusion.30), channel_id=1, source_target_pairs={{0,1},{1,0},{2,3},{3,2},{4,5},{5,4},{6,7},{7,6},{8,9},{9,8},{10,11... | collective-permute-start | bytes 1572872 | tf_op jit(solution)/shard_map/ppermute | solution.py:82
  142.6 17.8 %collective-permute-start.10 = (bf16[32,2048]{1,0:T(8,128)(2,1)S(1)}, bf16[32,2048]{1,0:T(8,128)(2,1)S(1)}, u32[]{:S(2)}, u32[]{:S(2)}) collective-permute-start(bf16[32,2048]{1,0:T(8,128)(2,1)S(1)} %get-tuple-element.18), channel_id=1, source_target_pairs={{0,4},{2,6},{4,0},{6,2},{1,5},{3,7},{5,1},{7,3},{8,12},{10,14},{12... | collective-permute-start | bytes 393224 | tf_op jit(solution)/shard_map/ppermute | solution.py:36
  146.7 13.8 %collective-permute-start.8 = (bf16[32,2048]{1,0:T(8,128)(2,1)S(1)}, bf16[32,2048]{1,0:T(8,128)(2,1)S(1)}, u32[]{:S(2)}, u32[]{:S(2)}) collective-permute-start(bf16[32,2048]{1,0:T(8,128)(2,1)S(1)} %get-tuple-element.17), channel_id=1, source_target_pairs={{0,2},{2,4},{4,6},{6,0},{1,3},{3,5},{5,7},{7,1},{8,10},{10,12},{12... | collective-permute-start | bytes 393224 | tf_op jit(solution)/shard_map/ppermute | solution.py:36
  148.6 11.9 %collective-permute-start.9 = (bf16[32,2048]{1,0:T(8,128)(2,1)S(1)}, bf16[32,2048]{1,0:T(8,128)(2,1)S(1)}, u32[]{:S(2)}, u32[]{:S(2)}) collective-permute-start(bf16[32,2048]{1,0:T(8,128)(2,1)S(1)} %get-tuple-element.19), channel_id=1, source_target_pairs={{0,6},{2,0},{4,2},{6,4},{1,7},{3,1},{5,3},{7,5},{8,14},{10,8},{12,... | collective-permute-start | bytes 393224 | tf_op jit(solution)/shard_map/ppermute | solution.py:36
  153.7 36.8 %all-to-all-start.2 = ((bf16[8,64,1152]{2,1,0:T(8,128)(2,1)}), bf16[8,64,1152]{2,1,0:T(8,128)(2,1)S(1)}, u32[]{:S(2)}, u32[]{:S(2)}) async-start(bf16[8,64,1152]{2,1,0:T(8,128)(2,1)} %bitcast.54), calls=%async_computation.2 | async-start | bytes 2359296 | tf_op jit(solution)/shard_map/all_to_all | solution.py:177
  161.4 10.5 %collective-permute-start.11 = (bf16[32,2048]{1,0:T(8,128)(2,1)S(1)}, bf16[32,2048]{1,0:T(8,128)(2,1)S(1)}, u32[]{:S(2)}, u32[]{:S(2)}) collective-permute-start(bf16[32,2048]{1,0:T(8,128)(2,1)S(1)} %reshape.73), channel_id=1, source_target_pairs={{0,2},{2,4},{4,6},{6,0},{1,3},{3,5},{5,7},{7,1},{8,10},{10,12},{12... | collective-permute-start | bytes 393224 | tf_op jit(solution)/shard_map/ppermute | solution.py:36
  163.3 8.7 %collective-permute-start.12 = (bf16[32,2048]{1,0:T(8,128)(2,1)S(1)}, bf16[32,2048]{1,0:T(8,128)(2,1)S(1)}, u32[]{:S(2)}, u32[]{:S(2)}) collective-permute-start(bf16[32,2048]{1,0:T(8,128)(2,1)S(1)} %reshape.73), channel_id=1, source_target_pairs={{0,6},{2,0},{4,2},{6,4},{1,7},{3,1},{5,3},{7,5},{8,14},{10,8},{12,... | collective-permute-start | bytes 393224 | tf_op jit(solution)/shard_map/ppermute | solution.py:36
  167.9 8.4 %collective-permute-start.13 = (bf16[32,2048]{1,0:T(8,128)(2,1)S(1)}, bf16[32,2048]{1,0:T(8,128)(2,1)S(1)}, u32[]{:S(2)}, u32[]{:S(2)}) collective-permute-start(bf16[32,2048]{1,0:T(8,128)(2,1)S(1)} %reshape.73), channel_id=1, source_target_pairs={{0,4},{2,6},{4,0},{6,2},{1,5},{3,7},{5,1},{7,3},{8,12},{10,14},{12... | collective-permute-start | bytes 393224 | tf_op jit(solution)/shard_map/ppermute | solution.py:36
  190.6 14.8 %collective-permute-start.21 = (bf16[64,1152]{1,0:T(8,128)(2,1)S(1)}, bf16[64,1152]{1,0:T(8,128)(2,1)S(1)}, u32[]{:S(2)}, u32[]{:S(2)}) collective-permute-start(bf16[64,1152]{1,0:T(8,128)(2,1)S(1)} %reduce_sum.12), channel_id=1, source_target_pairs={{0,256},{256,0},{1,257},{257,1},{2,258},{258,2},{3,259},{259,3},{4... | collective-permute-start | bytes 442376 | tf_op jit(solution)/shard_map/ppermute | solution.py:179
  (15 other events, 188.7 us)
where the time goes:
time: 207 us; the launch traced here: 206 us
  starting transfers between devices  106 us (51%)
  waiting for transfers between devices  60.3 us (29%)
  local copies, waits for them, and re-layouts  15.5 us (7%)
  matrix products  13.4 us (6%)
  other arithmetic  9.68 us (5%)
    ppermute x13, starting transfers between devices, shift_z(): return lax.ppermute(array, RING, [(i, (i + by) % NZ) for i in range(NZ)])  60.8 us
    ppermute x13, waiting for transfers between devices, shift_z(): return lax.ppermute(array, RING, [(i, (i + by) % NZ) for i in range(NZ)])  30.1 us
    ppermute x6, starting transfers between devices, shift(): lax.ppermute(array, axis, [(i, (i + by) % count) for i in range(count)])  20.3 us
    all_to_all x2, starting transfers between devices, spread_y(): return lax.all_to_all(copies, 'y', split_axis=0, concat_axis=0, tiled=True)  11 us
    ppermute x1, waiting for transfers between devices, per_device(): other = lax.ppermute(mine, 'zh', [(0, 1), (1, 0)])  10.8 us
    all_to_all x1, waiting for transfers between devices, per_device(): local = lax.all_to_all(local, 'y', split_axis=0, concat_axis=0, tiled=True)  10.3 us
    all_to_all x1, starting transfers between devices, per_device(): local = lax.all_to_all(local, 'y', split_axis=0, concat_axis=0, tiled=True)  6.8 us
    dot_general x3, matrix products, contract_last(): lax.dot_general(first, second, (((1,), (1,)), ((), ())), preferred_elemen...  6.72 us
  transfers between devices with their start and end apart: 25, of which 10 were waited for; matrix products, arithmetic and copies ran while one was open for 14% of the time, Pallas kernels for 0%

commit v1 on v0

--- a/solution.py
+++ b/solution.py
@@ -40,15 +40,8 @@
     return lax.dynamic_update_slice_in_dim(buffer, jnp.expand_dims(block, dim), at, dim)
 
 
-def swap_columns(array, outer, inner):
-    rows, columns = array.shape
-    parts = array.reshape(rows, outer, inner, columns // (outer * inner))
-    return parts.transpose(0, 2, 1, 3).reshape(rows, columns)
-
-
 def spread_y(block):
-    copies = jnp.broadcast_to(block, (NY, *block.shape))
-    return lax.all_to_all(copies, "y", split_axis=0, concat_axis=0, tiled=True)
+    return lax.all_to_all(block, "y", split_axis=0, concat_axis=0, tiled=True)
 
 
 def gather_z_then_y(shard, zl):
@@ -57,20 +50,22 @@
     for by in SHIFTS:
         block = shift_z(shard, by)
         near = put(near, block, jnp.mod(zl - by + NZL, NZL))
-    return spread_y(near)
+    full = spread_y(jnp.broadcast_to(near, (NY, *near.shape)))
+    return full.transpose(1, 0, 2, 3)
 
 
-def gather_y_then_z(shard, zl):
-    column = spread_y(shard)
-    full = jnp.zeros((NY, NZL, *shard.shape), shard.dtype)
-    full = put(full, column, zl, 1)
+def gather_y_then_z(shards, zl):
+    shard = jnp.concatenate(shards, axis=1)
+    column = spread_y(jnp.broadcast_to(shard, (NY, *shard.shape)))
+    full = jnp.zeros((NZL, *column.shape), column.dtype)
+    full = put(full, column, zl)
     for by in (1, -1):
         block = shift_z(column, by)
-        full = put(full, block, jnp.mod(zl - by + NZL, NZL), 1)
+        full = put(full, block, jnp.mod(zl - by + NZL, NZL))
     far_low = shift_z(column[: NY // 2], 2)
     far_high = shift_z(column[NY // 2 :], -2)
     far = jnp.concatenate((far_low, far_high), axis=0)
-    return put(full, far, jnp.mod(zl + 2, NZL), 1)
+    return put(full, far, jnp.mod(zl + 2, NZL))
 
 
 def reduce_on_tp(late, early, x, c):
@@ -117,8 +112,7 @@
     bf = jnp.bfloat16
     zl = lax.axis_index("zl")
     rows, width = gate_weight.shape
-    later_half = jnp.concatenate((up_weight, down_weight), axis=1)
-    part_b = gather_y_then_z(later_half, zl).reshape(-1, 2 * width)
+    part_b = gather_y_then_z((up_weight, down_weight), zl).reshape(-1, 2 * width)
     gate_full = gather_z_then_y(gate_weight, zl).reshape(-1, width)
     up_full = part_b[:, :width]
     down_full = part_b[:, width:]
@@ -134,13 +128,9 @@
         sent = features_for(jnp.mod(zl + by + NZL, NZL))
         features.append(shift_z(sent, by))
 
-    early = swap_columns(earlier_input, NZL, NY)
-    cot = swap_columns(cotangent, NZL, NY)
-    late = swap_columns(later_input, NZL, NY)
-
-    gate_early = dot(early, gate_full)
-    up_early = dot(early, up_full)
-    hidden_grad = dot(cot, down_full)
+    gate_early = dot(earlier_input, gate_full)
+    up_early = dot(earlier_input, up_full)
+    hidden_grad = dot(cotangent, down_full)
     sigmoid_gate = jax.nn.sigmoid(gate_early)
     silu_early = gate_early * sigmoid_gate
     gate_grad = (
@@ -150,10 +140,12 @@
     hidden_early = (silu_early * up_early).astype(bf)
 
     piece = jnp.concatenate((gate_grad, up_grad, hidden_early), axis=1)
-    pieces = [piece] + [shift_z(piece, by) for by in SHIFTS]
+    pieces = [piece]
+    for by in SHIFTS:
+        pieces.append(shift_z(piece, by))
 
-    gate_late = dot(late, gate_full)
-    up_late = dot(late, up_full)
+    gate_late = dot(later_input, gate_full)
+    up_late = dot(later_input, up_full)
     hidden_late = (jax.nn.silu(gate_late) * up_late).astype(bf)
     partial_late = contract_last(hidden_late, down_full).astype(bf)
     partial_early = (
@@ -163,7 +155,6 @@
     n_tp = lax.axis_size(TP)
     x, c = lax.axis_index("x"), lax.axis_index("c")
     own = reduce_on_tp(partial_late, partial_early, x, c)
-    own = swap_columns(own, NY, NZL)
     outs = everywhere_on_tp(own, x, c)
     later_output = outs[:, : tokens // n_tp].reshape(tokens, -1)
     earlier_input_grad = outs[:, tokens // n_tp :].reshape(tokens, -1)

time: 207 us -> 209 us (level)
  local copies, waits for them, and re-layouts: 15.5 us -> 10.3 us
  waiting for transfers between devices: 60.3 us -> 64.9 us
  starting transfers between devices: 106 us -> 110 us
  matrix products: 13.4 us -> 11 us
    ppermute x13, waiting for transfers between devices: 30.1 us -> 36.1 us  [shift_z(): return lax.ppermute(array, RING, [(i, (i + by) % NZ) for i in range(NZ)])]
    ppermute x1, waiting for transfers between devices: 10.8 us -> 6.97 us  [per_device(): other = lax.ppermute(mine, 'zh', [(0, 1), (1, 0)])]
    transpose x4 -> x0, local copies, waits for them, and re-layouts: 3.66 us -> none  [swap_columns(): return parts.transpose(0, 2, 1, 3).reshape(rows, columns)]
    all_to_all x1, waiting for transfers between devices: 10.3 us -> 12.5 us  [per_device(): local = lax.all_to_all(local, 'y', split_axis=0, concat_axis=0, tiled=True)]
    ppermute x1, starting transfers between devices: 2.93 us -> 5.06 us  [per_device(): other = lax.ppermute(mine, 'zh', [(0, 1), (1, 0)])]
    unnamed x31 -> x18, local copies, waits for them, and re-layouts: 4.71 us -> 2.76 us
  transfers between devices with their start and end apart: 25 -> 25, of which waited for: 10 -> 13; matrix products, arithmetic and copies ran while one was open for 14% -> 10% of each run, Pallas kernels for 0% -> 0%
where the time goes in v1:
time: 209 us; the launch traced here: 208 us
  starting transfers between devices  110 us (53%)
  waiting for transfers between devices  64.9 us (31%)
  matrix products  11 us (5%)
  other arithmetic  10.5 us (5%)
  local copies, waits for them, and re-layouts  10.3 us (5%)
    ppermute x13, starting transfers between devices, shift_z(): return lax.ppermute(array, RING, [(i, (i + by) % NZ) for i in range(NZ)])  61 us
    ppermute x13, waiting for transfers between devices, shift_z(): return lax.ppermute(array, RING, [(i, (i + by) % NZ) for i in range(NZ)])  36.1 us
    ppermute x6, starting transfers between devices, shift(): lax.ppermute(array, axis, [(i, (i + by) % count) for i in range(count)])  22.3 us
    all_to_all x1, waiting for transfers between devices, per_device(): local = lax.all_to_all(local, 'y', split_axis=0, concat_axis=0, tiled=True)  12.5 us
    all_to_all x2, starting transfers between devices, spread_y(): return lax.all_to_all(block, 'y', split_axis=0, concat_axis=0, tiled=True)  11 us
    ppermute x1, waiting for transfers between devices, per_device(): other = lax.ppermute(mine, 'zh', [(0, 1), (1, 0)])  6.97 us
    all_to_all x1, starting transfers between devices, per_device(): local = lax.all_to_all(local, 'y', split_axis=0, concat_axis=0, tiled=True)  6.52 us
    dot_general x3, matrix products, contract_last(): lax.dot_general(first, second, (((1,), (1,)), ((), ())), preferred_elemen...  6.45 us
  transfers between devices with their start and end apart: 25, of which 13 were waited for; matrix products, arithmetic and copies ran while one was open for 10% of the time, Pallas kernels for 0%

profile of v1, /device:TPU:2, one launch (start us, length us, event | category | flops | bytes accessed | tf_op | source)
XLA Modules:
  0.0 207.9 jit_solution(5651165862432226661)
XLA Ops:
  2.5 7.1 %all-to-all-start.1 = ((bf16[8,64,768]{2,1,0:T(8,128)(2,1)}), bf16[8,64,768]{2,1,0:T(8,128)(2,1)S(1)}, u32[]{:S(2)}, u32[]{:S(2)}) async-start(bf16[8,64,768]{2,1,0:T(8,128)(2,1)} %broadcast_in_dim.69), calls=%async_computation.1 | async-start | bytes 1572864 | tf_op jit(solution)/shard_map/all_to_all | solution.py:44
  9.6 4.3 %collective-permute-start = (bf16[64,384]{1,0:T(8,128)(2,1)S(1)}, bf16[64,384]{1,0:T(8,128)(2,1)S(1)}, u32[]{:S(2)}, u32[]{:S(2)}) collective-permute-start(bf16[64,384]{1,0:T(8,128)(2,1)S(1)} %copy-done.8), channel_id=1, source_target_pairs={{0,64},{64,128},{128,192},{192,256},{256,320},{320,384},{384,448},... | collective-permute-start | bytes 147464 | tf_op jit(solution)/shard_map/ppermute | solution.py:16
  13.9 8.6 %collective-permute-start.1 = (bf16[64,384]{1,0:T(8,128)(2,1)S(1)}, bf16[64,384]{1,0:T(8,128)(2,1)S(1)}, u32[]{:S(2)}, u32[]{:S(2)}) collective-permute-start(bf16[64,384]{1,0:T(8,128)(2,1)S(1)} %copy-done.8), channel_id=1, source_target_pairs={{0,448},{64,0},{128,64},{192,128},{256,192},{320,256},{384,320},{4... | collective-permute-start | bytes 147464 | tf_op jit(solution)/shard_map/ppermute | solution.py:16
  22.5 3.9 %collective-permute-start.2 = (bf16[64,384]{1,0:T(8,128)(2,1)S(1)}, bf16[64,384]{1,0:T(8,128)(2,1)S(1)}, u32[]{:S(2)}, u32[]{:S(2)}) collective-permute-start(bf16[64,384]{1,0:T(8,128)(2,1)S(1)} %copy-done.8), channel_id=1, source_target_pairs={{0,384},{64,448},{128,0},{192,64},{256,128},{320,192},{384,256},{4... | collective-permute-start | bytes 147464 | tf_op jit(solution)/shard_map/ppermute | solution.py:16
  34.1 3.9 %all-to-all-start = ((bf16[8,4,64,384]{3,2,1,0:T(8,128)(2,1)}), bf16[8,4,64,384]{3,2,1,0:T(8,128)(2,1)S(1)}, u32[]{:S(2)}, u32[]{:S(2)}) async-start(bf16[8,4,64,384]{3,2,1,0:T(8,128)(2,1)} %broadcast_in_dim.67), calls=%async_computation | async-start | bytes 3145728 | tf_op jit(solution)/shard_map/all_to_all | solution.py:44
  40.6 4.0 %collective-permute-start.15 = (bf16[128,1024]{1,0:T(8,128)(2,1)}, bf16[128,1024]{1,0:T(8,128)(2,1)}, u32[]{:S(2)}, u32[]{:S(2)}) collective-permute-start(bf16[128,1024]{1,0:T(8,128)(2,1)} %pad_maximum_fusion.4), channel_id=1, source_target_pairs={{0,64},{64,128},{128,192},{192,256},{256,320},{320,384},{384,448},... | collective-permute-start | bytes 786440 | tf_op jit(solution)/shard_map/ppermute | solution.py:16
  45.3 8.6 %collective-permute-start.16 = (bf16[128,1024]{1,0:T(8,128)(2,1)}, bf16[128,1024]{1,0:T(8,128)(2,1)}, u32[]{:S(2)}, u32[]{:S(2)}) collective-permute-start(bf16[128,1024]{1,0:T(8,128)(2,1)} %pad_maximum_fusion.5), channel_id=1, source_target_pairs={{0,448},{64,0},{128,64},{192,128},{256,192},{320,256},{384,320},{4... | collective-permute-start | bytes 786440 | tf_op jit(solution)/shard_map/ppermute | solution.py:16
  54.6 3.9 %collective-permute-start.17 = (bf16[128,1024]{1,0:T(8,128)(2,1)}, bf16[128,1024]{1,0:T(8,128)(2,1)}, u32[]{:S(2)}, u32[]{:S(2)}) collective-permute-start(bf16[128,1024]{1,0:T(8,128)(2,1)} %pad_maximum_fusion.6), channel_id=1, source_target_pairs={{0,384},{64,448},{128,0},{192,64},{256,128},{320,192},{384,256},{4... | collective-permute-start | bytes 786440 | tf_op jit(solution)/shard_map/ppermute | solution.py:16
  65.7 6.3 %collective-permute-done.17 = bf16[128,1024]{1,0:T(8,128)(2,1)} collective-permute-done((bf16[128,1024]{1,0:T(8,128)(2,1)}, bf16[128,1024]{1,0:T(8,128)(2,1)}, u32[]{:S(2)}, u32[]{:S(2)}) %collective-permute-start.17) | collective-permute-done | bytes 262176 | tf_op jit(solution)/shard_map/ppermute | solution.py:16
  74.3 6.3 %collective-permute-start.5 = (bf16[4,64,768]{2,1,0:T(8,128)(2,1)S(1)}, bf16[4,64,768]{2,1,0:T(8,128)(2,1)S(1)}, u32[]{:S(2)}, u32[]{:S(2)}) collective-permute-start(bf16[4,64,768]{2,1,0:T(8,128)(2,1)S(1)} %get-tuple-element.9), channel_id=1, source_target_pairs={{0,128},{64,192},{128,256},{192,320},{256,384},{320,448},{384,0},{... | collective-permute-start | bytes 1179656 | tf_op jit(solution)/shard_map/ppermute | solution.py:16
  86.3 4.5 %collective-permute-done.4 = bf16[8,64,768]{2,1,0:T(8,128)(2,1)S(1)} collective-permute-done((bf16[8,64,768]{2,1,0:T(8,128)(2,1)S(1)}, bf16[8,64,768]{2,1,0:T(8,128)(2,1)S(1)}, u32[]{:S(2)}, u32[]{:S(2)}) %collective-permute-start.4) | collective-permute-done | bytes 786464 | tf_op jit(solution)/shard_map/ppermute | solution.py:16
  92.0 13.0 %collective-permute-done.6 = bf16[4,64,768]{2,1,0:T(8,128)(2,1)S(1)} collective-permute-done((bf16[4,64,768]{2,1,0:T(8,128)(2,1)S(1)}, bf16[4,64,768]{2,1,0:T(8,128)(2,1)S(1)}, u32[]{:S(2)}, u32[]{:S(2)}) %collective-permute-start.6) | collective-permute-done | bytes 393248 | tf_op jit(solution)/shard_map/ppermute | solution.py:16
  112.5 5.1 %collective-permute-start.19 = (bf16[128,1152]{0,1:T(8,128)(2,1)}, bf16[128,1152]{0,1:T(8,128)(2,1)}, u32[]{:S(2)}, u32[]{:S(2)}) collective-permute-start(bf16[128,1152]{0,1:T(8,128)(2,1)} %pad_maximum_fusion.3), channel_id=1, source_target_pairs={{0,448},{64,0},{128,64},{192,128},{256,192},{320,256},{384,320},{4... | collective-permute-start | bytes 884744 | tf_op jit(solution)/shard_map/ppermute | solution.py:16
  117.6 5.1 %collective-permute-start.20 = (bf16[128,1152]{0,1:T(8,128)(2,1)}, bf16[128,1152]{0,1:T(8,128)(2,1)}, u32[]{:S(2)}, u32[]{:S(2)}) collective-permute-start(bf16[128,1152]{0,1:T(8,128)(2,1)} %pad_maximum_fusion.3), channel_id=1, source_target_pairs={{0,384},{64,448},{128,0},{192,64},{256,128},{320,192},{384,256},{4... | collective-permute-start | bytes 884744 | tf_op jit(solution)/shard_map/ppermute | solution.py:16
  124.0 3.8 %convolution_convert_fusion = bf16[128,2048]{1,0:T(8,128)(2,1)S(1)} fusion(bf16[2048,768]{1,0:T(8,128)(2,1)} %bitcast.87, bf16[128,2048]{1,0:T(8,128)(2,1)S(1)} %copy-done, f32[128,384]{0,1:T(8,128)S(1)} %convolution_bitcast_fusion.1), kind=kOutput, calls=%fused_computation.2 | convolution fusion | flops 403210240 | bytes 4390912 | tf_op jit(solution)/shard_map/dot_general | solution.py:20
  132.0 6.6 %collective-permute-done.20 = bf16[128,1152]{0,1:T(8,128)(2,1)} collective-permute-done((bf16[128,1152]{0,1:T(8,128)(2,1)}, bf16[128,1152]{0,1:T(8,128)(2,1)}, u32[]{:S(2)}, u32[]{:S(2)}) %collective-permute-start.20) | collective-permute-done | bytes 294944 | tf_op jit(solution)/shard_map/ppermute | solution.py:16
  140.6 4.0 %collective-permute-start.10 = (bf16[32,2048]{1,0:T(8,128)(2,1)S(1)}, bf16[32,2048]{1,0:T(8,128)(2,1)S(1)}, u32[]{:S(2)}, u32[]{:S(2)}) collective-permute-start(bf16[32,2048]{1,0:T(8,128)(2,1)S(1)} %get-tuple-element.20), channel_id=1, source_target_pairs={{0,4},{2,6},{4,0},{6,2},{1,5},{3,7},{5,1},{7,3},{8,12},{10,14},{12... | collective-permute-start | bytes 393224 | tf_op jit(solution)/shard_map/ppermute | solution.py:36
  146.6 3.9 %collective-permute-start.9 = (bf16[32,2048]{1,0:T(8,128)(2,1)S(1)}, bf16[32,2048]{1,0:T(8,128)(2,1)S(1)}, u32[]{:S(2)}, u32[]{:S(2)}) collective-permute-start(bf16[32,2048]{1,0:T(8,128)(2,1)S(1)} %get-tuple-element.21), channel_id=1, source_target_pairs={{0,6},{2,0},{4,2},{6,4},{1,7},{3,1},{5,3},{7,5},{8,14},{10,8},{12,... | collective-permute-start | bytes 393224 | tf_op jit(solution)/shard_map/ppermute | solution.py:36
  153.6 3.9 %collective-permute-start.11 = (bf16[32,2048]{1,0:T(8,128)(2,1)S(1)}, bf16[32,2048]{1,0:T(8,128)(2,1)S(1)}, u32[]{:S(2)}, u32[]{:S(2)}) collective-permute-start(bf16[32,2048]{1,0:T(8,128)(2,1)S(1)} %get-tuple-element.6), channel_id=1, source_target_pairs={{0,2},{2,4},{4,6},{6,0},{1,3},{3,5},{5,7},{7,1},{8,10},{10,12},{12... | collective-permute-start | bytes 393224 | tf_op jit(solution)/shard_map/ppermute | solution.py:36
  158.7 6.5 %all-to-all-start.2 = ((bf16[8,64,1152]{2,1,0:T(8,128)(2,1)}), bf16[8,64,1152]{2,1,0:T(8,128)(2,1)S(1)}, u32[]{:S(2)}, u32[]{:S(2)}) async-start(bf16[8,64,1152]{2,1,0:T(8,128)(2,1)} %bitcast.92), calls=%async_computation.2 | async-start | bytes 2359296 | tf_op jit(solution)/shard_map/all_to_all | solution.py:168
  167.3 6.4 %collective-permute-start.13 = (bf16[32,2048]{1,0:T(8,128)(2,1)S(1)}, bf16[32,2048]{1,0:T(8,128)(2,1)S(1)}, u32[]{:S(2)}, u32[]{:S(2)}) collective-permute-start(bf16[32,2048]{1,0:T(8,128)(2,1)S(1)} %get-tuple-element.6), channel_id=1, source_target_pairs={{0,4},{2,6},{4,0},{6,2},{1,5},{3,7},{5,1},{7,3},{8,12},{10,14},{12... | collective-permute-start | bytes 393224 | tf_op jit(solution)/shard_map/ppermute | solution.py:36
  180.5 12.5 %all-to-all-done.2 = bf16[8,64,1152]{2,1,0:T(8,128)(2,1)S(1)} async-done(((bf16[8,64,1152]{2,1,0:T(8,128)(2,1)}), bf16[8,64,1152]{2,1,0:T(8,128)(2,1)S(1)}, u32[]{:S(2)}, u32[]{:S(2)}) %all-to-all-start.2) | async-done | bytes 1179680 | tf_op jit(solution)/shard_map/all_to_all | solution.py:168
  193.2 5.1 %collective-permute-start.21 = (bf16[64,1152]{1,0:T(8,128)(2,1)S(1)}, bf16[64,1152]{1,0:T(8,128)(2,1)S(1)}, u32[]{:S(2)}, u32[]{:S(2)}) collective-permute-start(bf16[64,1152]{1,0:T(8,128)(2,1)S(1)} %reduce_sum.12), channel_id=1, source_target_pairs={{0,256},{256,0},{1,257},{257,1},{2,258},{258,2},{3,259},{259,3},{4... | collective-permute-start | bytes 442376 | tf_op jit(solution)/shard_map/ppermute | solution.py:170
  199.3 7.0 %collective-permute-done.21 = bf16[64,1152]{1,0:T(8,128)(2,1)S(1)} collective-permute-done((bf16[64,1152]{1,0:T(8,128)(2,1)S(1)}, bf16[64,1152]{1,0:T(8,128)(2,1)S(1)}, u32[]{:S(2)}, u32[]{:S(2)}) %collective-permute-start.21) | collective-permute-done | bytes 147488 | tf_op jit(solution)/shard_map/ppermute | solution.py:170
  (92 shorter events, 62.3 us)
Async XLA Ops:
  2.5 30.2 %all-to-all-start.1 = ((bf16[8,64,768]{2,1,0:T(8,128)(2,1)}), bf16[8,64,768]{2,1,0:T(8,128)(2,1)S(1)}, u32[]{:S(2)}, u32[]{:S(2)}) async-start(bf16[8,64,768]{2,1,0:T(8,128)(2,1)} %broadcast_in_dim.69), calls=%async_computation.1 | async-start | bytes 1572864 | tf_op jit(solution)/shard_map/all_to_all | solution.py:44
  9.6 16.9 %collective-permute-start = (bf16[64,384]{1,0:T(8,128)(2,1)S(1)}, bf16[64,384]{1,0:T(8,128)(2,1)S(1)}, u32[]{:S(2)}, u32[]{:S(2)}) collective-permute-start(bf16[64,384]{1,0:T(8,128)(2,1)S(1)} %copy-done.8), channel_id=1, source_target_pairs={{0,64},{64,128},{128,192},{192,256},{256,320},{320,384},{384,448},... | collective-permute-start | bytes 147464 | tf_op jit(solution)/shard_map/ppermute | solution.py:16
  13.9 12.7 %collective-permute-start.1 = (bf16[64,384]{1,0:T(8,128)(2,1)S(1)}, bf16[64,384]{1,0:T(8,128)(2,1)S(1)}, u32[]{:S(2)}, u32[]{:S(2)}) collective-permute-start(bf16[64,384]{1,0:T(8,128)(2,1)S(1)} %copy-done.8), channel_id=1, source_target_pairs={{0,448},{64,0},{128,64},{192,128},{256,192},{320,256},{384,320},{4... | collective-permute-start | bytes 147464 | tf_op jit(solution)/shard_map/ppermute | solution.py:16
  22.5 6.9 %collective-permute-start.2 = (bf16[64,384]{1,0:T(8,128)(2,1)S(1)}, bf16[64,384]{1,0:T(8,128)(2,1)S(1)}, u32[]{:S(2)}, u32[]{:S(2)}) collective-permute-start(bf16[64,384]{1,0:T(8,128)(2,1)S(1)} %copy-done.8), channel_id=1, source_target_pairs={{0,384},{64,448},{128,0},{192,64},{256,128},{320,192},{384,256},{4... | collective-permute-start | bytes 147464 | tf_op jit(solution)/shard_map/ppermute | solution.py:16
  34.1 73.2 %all-to-all-start = ((bf16[8,4,64,384]{3,2,1,0:T(8,128)(2,1)}), bf16[8,4,64,384]{3,2,1,0:T(8,128)(2,1)S(1)}, u32[]{:S(2)}, u32[]{:S(2)}) async-start(bf16[8,4,64,384]{3,2,1,0:T(8,128)(2,1)} %broadcast_in_dim.67), calls=%async_computation | async-start | bytes 3145728 | tf_op jit(solution)/shard_map/all_to_all | solution.py:44
  40.6 25.1 %collective-permute-start.15 = (bf16[128,1024]{1,0:T(8,128)(2,1)}, bf16[128,1024]{1,0:T(8,128)(2,1)}, u32[]{:S(2)}, u32[]{:S(2)}) collective-permute-start(bf16[128,1024]{1,0:T(8,128)(2,1)} %pad_maximum_fusion.4), channel_id=1, source_target_pairs={{0,64},{64,128},{128,192},{192,256},{256,320},{320,384},{384,448},... | collective-permute-start | bytes 786440 | tf_op jit(solution)/shard_map/ppermute | solution.py:16
  45.3 20.4 %collective-permute-start.16 = (bf16[128,1024]{1,0:T(8,128)(2,1)}, bf16[128,1024]{1,0:T(8,128)(2,1)}, u32[]{:S(2)}, u32[]{:S(2)}) collective-permute-start(bf16[128,1024]{1,0:T(8,128)(2,1)} %pad_maximum_fusion.5), channel_id=1, source_target_pairs={{0,448},{64,0},{128,64},{192,128},{256,192},{320,256},{384,320},{4... | collective-permute-start | bytes 786440 | tf_op jit(solution)/shard_map/ppermute | solution.py:16
  54.6 17.4 %collective-permute-start.17 = (bf16[128,1024]{1,0:T(8,128)(2,1)}, bf16[128,1024]{1,0:T(8,128)(2,1)}, u32[]{:S(2)}, u32[]{:S(2)}) collective-permute-start(bf16[128,1024]{1,0:T(8,128)(2,1)} %pad_maximum_fusion.6), channel_id=1, source_target_pairs={{0,384},{64,448},{128,0},{192,64},{256,128},{320,192},{384,256},{4... | collective-permute-start | bytes 786440 | tf_op jit(solution)/shard_map/ppermute | solution.py:16
  58.6 26.6 %collective-permute-start.3 = (bf16[8,64,768]{2,1,0:T(8,128)(2,1)S(1)}, bf16[8,64,768]{2,1,0:T(8,128)(2,1)}, u32[]{:S(2)}, u32[]{:S(2)}) collective-permute-start(bf16[8,64,768]{2,1,0:T(8,128)(2,1)S(1)} %all-to-all-done.1), channel_id=1, source_target_pairs={{0,64},{64,128},{128,192},{192,256},{256,320},{320,384},{384,448},... | collective-permute-start | bytes 2359304 | tf_op jit(solution)/shard_map/ppermute | solution.py:16
  62.0 28.9 %collective-permute-start.4 = (bf16[8,64,768]{2,1,0:T(8,128)(2,1)S(1)}, bf16[8,64,768]{2,1,0:T(8,128)(2,1)S(1)}, u32[]{:S(2)}, u32[]{:S(2)}) collective-permute-start(bf16[8,64,768]{2,1,0:T(8,128)(2,1)S(1)} %all-to-all-done.1), channel_id=1, source_target_pairs={{0,448},{64,0},{128,64},{192,128},{256,192},{320,256},{384,320},{4... | collective-permute-start | bytes 2359304 | tf_op jit(solution)/shard_map/ppermute | solution.py:16
  74.3 17.7 %collective-permute-start.5 = (bf16[4,64,768]{2,1,0:T(8,128)(2,1)S(1)}, bf16[4,64,768]{2,1,0:T(8,128)(2,1)S(1)}, u32[]{:S(2)}, u32[]{:S(2)}) collective-permute-start(bf16[4,64,768]{2,1,0:T(8,128)(2,1)S(1)} %get-tuple-element.9), channel_id=1, source_target_pairs={{0,128},{64,192},{128,256},{192,320},{256,384},{320,448},{384,0},{... | collective-permute-start | bytes 1179656 | tf_op jit(solution)/shard_map/ppermute | solution.py:16
  80.5 24.4 %collective-permute-start.6 = (bf16[4,64,768]{2,1,0:T(8,128)(2,1)S(1)}, bf16[4,64,768]{2,1,0:T(8,128)(2,1)S(1)}, u32[]{:S(2)}, u32[]{:S(2)}) collective-permute-start(bf16[4,64,768]{2,1,0:T(8,128)(2,1)S(1)} %get-tuple-element.10), channel_id=1, source_target_pairs={{0,384},{64,448},{128,0},{192,64},{256,128},{320,192},{384,256},{4... | collective-permute-start | bytes 1179656 | tf_op jit(solution)/shard_map/ppermute | solution.py:16
  110.6 21.4 %collective-permute-start.18 = (bf16[128,1152]{0,1:T(8,128)(2,1)}, bf16[128,1152]{0,1:T(8,128)(2,1)S(1)}, u32[]{:S(2)}, u32[]{:S(2)}) collective-permute-start(bf16[128,1152]{0,1:T(8,128)(2,1)} %pad_maximum_fusion.3), channel_id=1, source_target_pairs={{0,64},{64,128},{128,192},{192,256},{256,320},{320,384},{384,448},... | collective-permute-start | bytes 884744 | tf_op jit(solution)/shard_map/ppermute | solution.py:16
  112.5 19.5 %collective-permute-start.19 = (bf16[128,1152]{0,1:T(8,128)(2,1)}, bf16[128,1152]{0,1:T(8,128)(2,1)}, u32[]{:S(2)}, u32[]{:S(2)}) collective-permute-start(bf16[128,1152]{0,1:T(8,128)(2,1)} %pad_maximum_fusion.3), channel_id=1, source_target_pairs={{0,448},{64,0},{128,64},{192,128},{256,192},{320,256},{384,320},{4... | collective-permute-start | bytes 884744 | tf_op jit(solution)/shard_map/ppermute | solution.py:16
  117.6 21.0 %collective-permute-start.20 = (bf16[128,1152]{0,1:T(8,128)(2,1)}, bf16[128,1152]{0,1:T(8,128)(2,1)}, u32[]{:S(2)}, u32[]{:S(2)}) collective-permute-start(bf16[128,1152]{0,1:T(8,128)(2,1)} %pad_maximum_fusion.3), channel_id=1, source_target_pairs={{0,384},{64,448},{128,0},{192,64},{256,128},{320,192},{384,256},{4... | collective-permute-start | bytes 884744 | tf_op jit(solution)/shard_map/ppermute | solution.py:16
  129.9 10.5 %collective-permute-start.7 = (bf16[4,32,2048]{2,1,0:T(8,128)(2,1)S(1)}, bf16[4,32,2048]{2,1,0:T(8,128)(2,1)S(1)}, u32[]{:S(2)}, u32[]{:S(2)}) collective-permute-start(bf16[4,32,2048]{2,1,0:T(8,128)(2,1)S(1)} %fusion.30), channel_id=1, source_target_pairs={{0,1},{1,0},{2,3},{3,2},{4,5},{5,4},{6,7},{7,6},{8,9},{9,8},{10,11... | collective-permute-start | bytes 1572872 | tf_op jit(solution)/shard_map/ppermute | solution.py:77
  140.6 11.3 %collective-permute-start.10 = (bf16[32,2048]{1,0:T(8,128)(2,1)S(1)}, bf16[32,2048]{1,0:T(8,128)(2,1)S(1)}, u32[]{:S(2)}, u32[]{:S(2)}) collective-permute-start(bf16[32,2048]{1,0:T(8,128)(2,1)S(1)} %get-tuple-element.20), channel_id=1, source_target_pairs={{0,4},{2,6},{4,0},{6,2},{1,5},{3,7},{5,1},{7,3},{8,12},{10,14},{12... | collective-permute-start | bytes 393224 | tf_op jit(solution)/shard_map/ppermute | solution.py:36
  144.7 7.3 %collective-permute-start.8 = (bf16[32,2048]{1,0:T(8,128)(2,1)S(1)}, bf16[32,2048]{1,0:T(8,128)(2,1)S(1)}, u32[]{:S(2)}, u32[]{:S(2)}) collective-permute-start(bf16[32,2048]{1,0:T(8,128)(2,1)S(1)} %get-tuple-element.19), channel_id=1, source_target_pairs={{0,2},{2,4},{4,6},{6,0},{1,3},{3,5},{5,7},{7,1},{8,10},{10,12},{12... | collective-permute-start | bytes 393224 | tf_op jit(solution)/shard_map/ppermute | solution.py:36
  146.6 6.9 %collective-permute-start.9 = (bf16[32,2048]{1,0:T(8,128)(2,1)S(1)}, bf16[32,2048]{1,0:T(8,128)(2,1)S(1)}, u32[]{:S(2)}, u32[]{:S(2)}) collective-permute-start(bf16[32,2048]{1,0:T(8,128)(2,1)S(1)} %get-tuple-element.21), channel_id=1, source_target_pairs={{0,6},{2,0},{4,2},{6,4},{1,7},{3,1},{5,3},{7,5},{8,14},{10,8},{12,... | collective-permute-start | bytes 393224 | tf_op jit(solution)/shard_map/ppermute | solution.py:36
  153.6 20.1 %collective-permute-start.11 = (bf16[32,2048]{1,0:T(8,128)(2,1)S(1)}, bf16[32,2048]{1,0:T(8,128)(2,1)S(1)}, u32[]{:S(2)}, u32[]{:S(2)}) collective-permute-start(bf16[32,2048]{1,0:T(8,128)(2,1)S(1)} %get-tuple-element.6), channel_id=1, source_target_pairs={{0,2},{2,4},{4,6},{6,0},{1,3},{3,5},{5,7},{7,1},{8,10},{10,12},{12... | collective-permute-start | bytes 393224 | tf_op jit(solution)/shard_map/ppermute | solution.py:36
  158.7 34.3 %all-to-all-start.2 = ((bf16[8,64,1152]{2,1,0:T(8,128)(2,1)}), bf16[8,64,1152]{2,1,0:T(8,128)(2,1)S(1)}, u32[]{:S(2)}, u32[]{:S(2)}) async-start(bf16[8,64,1152]{2,1,0:T(8,128)(2,1)} %bitcast.92), calls=%async_computation.2 | async-start | bytes 2359296 | tf_op jit(solution)/shard_map/all_to_all | solution.py:168
  165.2 8.5 %collective-permute-start.12 = (bf16[32,2048]{1,0:T(8,128)(2,1)S(1)}, bf16[32,2048]{1,0:T(8,128)(2,1)S(1)}, u32[]{:S(2)}, u32[]{:S(2)}) collective-permute-start(bf16[32,2048]{1,0:T(8,128)(2,1)S(1)} %get-tuple-element.6), channel_id=1, source_target_pairs={{0,6},{2,0},{4,2},{6,4},{1,7},{3,1},{5,3},{7,5},{8,14},{10,8},{12,... | collective-permute-start | bytes 393224 | tf_op jit(solution)/shard_map/ppermute | solution.py:36
  167.3 9.3 %collective-permute-start.13 = (bf16[32,2048]{1,0:T(8,128)(2,1)S(1)}, bf16[32,2048]{1,0:T(8,128)(2,1)S(1)}, u32[]{:S(2)}, u32[]{:S(2)}) collective-permute-start(bf16[32,2048]{1,0:T(8,128)(2,1)S(1)} %get-tuple-element.6), channel_id=1, source_target_pairs={{0,4},{2,6},{4,0},{6,2},{1,5},{3,7},{5,1},{7,3},{8,12},{10,14},{12... | collective-permute-start | bytes 393224 | tf_op jit(solution)/shard_map/ppermute | solution.py:36
  193.2 13.1 %collective-permute-start.21 = (bf16[64,1152]{1,0:T(8,128)(2,1)S(1)}, bf16[64,1152]{1,0:T(8,128)(2,1)S(1)}, u32[]{:S(2)}, u32[]{:S(2)}) collective-permute-start(bf16[64,1152]{1,0:T(8,128)(2,1)S(1)} %reduce_sum.12), channel_id=1, source_target_pairs={{0,256},{256,0},{1,257},{257,1},{2,258},{258,2},{3,259},{259,3},{4... | collective-permute-start | bytes 442376 | tf_op jit(solution)/shard_map/ppermute | solution.py:170
  (10 other events, 232.6 us)

commit v2 on v1

--- a/solution.py
+++ b/solution.py
@@ -90,7 +90,8 @@
     line = jnp.zeros((n_x, *own.shape), own.dtype)
     line = put(line, own, x)
     for by in (1, -1, 2):
-        line = put(line, shift(own, "x", n_x, by), jnp.mod(x - by + n_x, n_x))
+        block = shift(own, "x", n_x, by)
+        line = put(line, block, jnp.mod(x - by + n_x, n_x))
     other = lax.ppermute(line, "c", [(0, 1), (1, 0)])
     both = jnp.zeros((n_x, 2, *own.shape), own.dtype)
     both = put(both, line, c, 1)
@@ -124,9 +125,20 @@
         return jnp.concatenate((cut(earlier_input), cut(cotangent)), axis=1)
 
     features = [features_for(zl)]
-    for by in SHIFTS:
+    c = lax.axis_index("c")
+    halves = []
+    for k, by in enumerate(SHIFTS):
         sent = features_for(jnp.mod(zl + by + NZL, NZL))
-        features.append(shift_z(sent, by))
+        if k:
+            tokens_half = sent.shape[0] // 2
+            sent = lax.dynamic_slice_in_dim(sent, c * tokens_half, tokens_half, 0)
+        arrived = shift_z(sent, by)
+        (halves if k else features).append(arrived)
+    halves = jnp.stack(halves)
+    others = lax.ppermute(halves, "c", [(0, 1), (1, 0)])
+    far = jnp.zeros((halves.shape[0], 2, *halves.shape[1:]), halves.dtype)
+    far = put(put(far, halves, c, 1), others, 1 - c, 1)
+    features += [f.reshape(-1, f.shape[-1]) for f in far]
 
     gate_early = dot(earlier_input, gate_full)
     up_early = dot(earlier_input, up_full)
@@ -153,7 +165,7 @@
     ).astype(bf)
     tokens = partial_late.shape[0]
     n_tp = lax.axis_size(TP)
-    x, c = lax.axis_index("x"), lax.axis_index("c")
+    x = lax.axis_index("x")
     own = reduce_on_tp(partial_late, partial_early, x, c)
     outs = everywhere_on_tp(own, x, c)
     later_output = outs[:, : tokens // n_tp].reshape(tokens, -1)

time: 209 us -> 217 us (1.038)
  the two profiles are of different devices: /device:TPU:2 before, /device:TPU:4 now
where the time goes in v2:
time: 217 us; the launch traced here: 215 us
  starting transfers between devices  108 us (50%)
  waiting for transfers between devices  71.1 us (33%)
  other arithmetic  14.2 us (7%)
  matrix products  11 us (5%)
  local copies, waits for them, and re-layouts  9.97 us (5%)
    ppermute x13, starting transfers between devices, shift_z(): return lax.ppermute(array, RING, [(i, (i + by) % NZ) for i in range(NZ)])  58.6 us
    ppermute x13, waiting for transfers between devices, shift_z(): return lax.ppermute(array, RING, [(i, (i + by) % NZ) for i in range(NZ)])  38.3 us
    ppermute x6, starting transfers between devices, shift(): lax.ppermute(array, axis, [(i, (i + by) % count) for i in range(count)])  19.4 us
    all_to_all x1, waiting for transfers between devices, per_device(): local = lax.all_to_all(local, 'y', split_axis=0, concat_axis=0, tiled=True)  14.4 us
    all_to_all x2, starting transfers between devices, spread_y(): return lax.all_to_all(block, 'y', split_axis=0, concat_axis=0, tiled=True)  11 us
    ppermute x6, waiting for transfers between devices, shift(): lax.ppermute(array, axis, [(i, (i + by) % count) for i in range(count)])  7.86 us
    all_to_all x1, starting transfers between devices, per_device(): local = lax.all_to_all(local, 'y', split_axis=0, concat_axis=0, tiled=True)  6.83 us
    dot_general x3, matrix products, contract_last(): lax.dot_general(first, second, (((1,), (1,)), ((), ())), preferred_elemen...  6.45 us
  transfers between devices with their start and end apart: 26, of which 15 were waited for; matrix products, arithmetic and copies ran while one was open for 12% of the time, Pallas kernels for 0%

profile of v2, /device:TPU:4, one launch (start us, length us, event | category | flops | bytes accessed | tf_op | source)
XLA Modules:
  0.0 215.4 jit_solution(14099992828716963049)
XLA Ops:
  2.6 7.1 %all-to-all-start.1 = ((bf16[8,64,768]{2,1,0:T(8,128)(2,1)}), bf16[8,64,768]{2,1,0:T(8,128)(2,1)S(1)}, u32[]{:S(2)}, u32[]{:S(2)}) async-start(bf16[8,64,768]{2,1,0:T(8,128)(2,1)} %broadcast_in_dim.78), calls=%async_computation.1 | async-start | bytes 1572864 | tf_op jit(solution)/shard_map/all_to_all | solution.py:44
  9.7 4.3 %collective-permute-start = (bf16[64,384]{1,0:T(8,128)(2,1)S(1)}, bf16[64,384]{1,0:T(8,128)(2,1)S(1)}, u32[]{:S(2)}, u32[]{:S(2)}) collective-permute-start(bf16[64,384]{1,0:T(8,128)(2,1)S(1)} %copy-done.11), channel_id=1, source_target_pairs={{0,64},{64,128},{128,192},{192,256},{256,320},{320,384},{384,448},... | collective-permute-start | bytes 147464 | tf_op jit(solution)/shard_map/ppermute | solution.py:16
  14.0 8.6 %collective-permute-start.1 = (bf16[64,384]{1,0:T(8,128)(2,1)S(1)}, bf16[64,384]{1,0:T(8,128)(2,1)S(1)}, u32[]{:S(2)}, u32[]{:S(2)}) collective-permute-start(bf16[64,384]{1,0:T(8,128)(2,1)S(1)} %copy-done.11), channel_id=1, source_target_pairs={{0,448},{64,0},{128,64},{192,128},{256,192},{320,256},{384,320},{4... | collective-permute-start | bytes 147464 | tf_op jit(solution)/shard_map/ppermute | solution.py:16
  22.6 3.9 %collective-permute-start.2 = (bf16[64,384]{1,0:T(8,128)(2,1)S(1)}, bf16[64,384]{1,0:T(8,128)(2,1)S(1)}, u32[]{:S(2)}, u32[]{:S(2)}) collective-permute-start(bf16[64,384]{1,0:T(8,128)(2,1)S(1)} %copy-done.11), channel_id=1, source_target_pairs={{0,384},{64,448},{128,0},{192,64},{256,128},{320,192},{384,256},{4... | collective-permute-start | bytes 147464 | tf_op jit(solution)/shard_map/ppermute | solution.py:16
  29.5 3.3 %all-to-all-done.1 = bf16[8,64,768]{2,1,0:T(8,128)(2,1)S(1)} async-done(((bf16[8,64,768]{2,1,0:T(8,128)(2,1)}), bf16[8,64,768]{2,1,0:T(8,128)(2,1)S(1)}, u32[]{:S(2)}, u32[]{:S(2)}) %all-to-all-start.1) | async-done | bytes 786464 | tf_op jit(solution)/shard_map/all_to_all | solution.py:44
  34.2 3.9 %all-to-all-start = ((bf16[8,4,64,384]{3,2,1,0:T(8,128)(2,1)}), bf16[8,4,64,384]{3,2,1,0:T(8,128)(2,1)S(1)}, u32[]{:S(2)}, u32[]{:S(2)}) async-start(bf16[8,4,64,384]{3,2,1,0:T(8,128)(2,1)} %broadcast_in_dim.76), calls=%async_computation | async-start | bytes 3145728 | tf_op jit(solution)/shard_map/all_to_all | solution.py:44
  38.9 10.7 %collective-permute-start.16 = (bf16[64,1024]{1,0:T(8,128)(2,1)S(1)}, bf16[64,1024]{1,0:T(8,128)(2,1)S(1)}, u32[]{:S(2)}, u32[]{:S(2)}) collective-permute-start(bf16[64,1024]{1,0:T(8,128)(2,1)S(1)} %fusion.56), channel_id=1, source_target_pairs={{0,448},{64,0},{128,64},{192,128},{256,192},{320,256},{384,320},{4... | collective-permute-start | bytes 393224 | tf_op jit(solution)/shard_map/ppermute | solution.py:16
  53.0 5.7 %collective-permute-done.17 = bf16[64,1024]{1,0:T(8,128)(2,1)} collective-permute-done((bf16[64,1024]{1,0:T(8,128)(2,1)S(1)}, bf16[64,1024]{1,0:T(8,128)(2,1)}, u32[]{:S(2)}, u32[]{:S(2)}) %collective-permute-start.17) | collective-permute-done | bytes 131104 | tf_op jit(solution)/shard_map/ppermute | solution.py:16
  71.3 4.9 %collective-permute-start.4 = (bf16[8,64,768]{2,1,0:T(8,128)(2,1)S(1)}, bf16[8,64,768]{2,1,0:T(8,128)(2,1)S(1)}, u32[]{:S(2)}, u32[]{:S(2)}) collective-permute-start(bf16[8,64,768]{2,1,0:T(8,128)(2,1)S(1)} %all-to-all-done.1), channel_id=1, source_target_pairs={{0,448},{64,0},{128,64},{192,128},{256,192},{320,256},{384,320},{4... | collective-permute-start | bytes 2359304 | tf_op jit(solution)/shard_map/ppermute | solution.py:16
  81.7 6.0 %collective-permute-start.6 = (bf16[4,64,768]{2,1,0:T(8,128)(2,1)S(1)}, bf16[4,64,768]{2,1,0:T(8,128)(2,1)S(1)}, u32[]{:S(2)}, u32[]{:S(2)}) collective-permute-start(bf16[4,64,768]{2,1,0:T(8,128)(2,1)S(1)} %get-tuple-element.10), channel_id=1, source_target_pairs={{0,384},{64,448},{128,0},{192,64},{256,128},{320,192},{384,256},{4... | collective-permute-start | bytes 1179656 | tf_op jit(solution)/shard_map/ppermute | solution.py:16
  88.2 6.2 %collective-permute-done.3 = bf16[8,64,768]{2,1,0:T(8,128)(2,1)S(1)} collective-permute-done((bf16[8,64,768]{2,1,0:T(8,128)(2,1)S(1)}, bf16[8,64,768]{2,1,0:T(8,128)(2,1)S(1)}, u32[]{:S(2)}, u32[]{:S(2)}) %collective-permute-start.3) | collective-permute-done | bytes 786464 | tf_op jit(solution)/shard_map/ppermute | solution.py:16
  96.0 16.3 %collective-permute-done.5 = bf16[4,64,768]{2,1,0:T(8,128)(2,1)S(1)} collective-permute-done((bf16[4,64,768]{2,1,0:T(8,128)(2,1)S(1)}, bf16[4,64,768]{2,1,0:T(8,128)(2,1)S(1)}, u32[]{:S(2)}, u32[]{:S(2)}) %collective-permute-start.5) | collective-permute-done | bytes 393248 | tf_op jit(solution)/shard_map/ppermute | solution.py:16
  119.9 5.1 %collective-permute-start.20 = (bf16[128,1152]{0,1:T(8,128)(2,1)}, bf16[128,1152]{0,1:T(8,128)(2,1)}, u32[]{:S(2)}, u32[]{:S(2)}) collective-permute-start(bf16[128,1152]{0,1:T(8,128)(2,1)} %pad_maximum_fusion.3), channel_id=1, source_target_pairs={{0,448},{64,0},{128,64},{192,128},{256,192},{320,256},{384,320},{4... | collective-permute-start | bytes 884744 | tf_op jit(solution)/shard_map/ppermute | solution.py:16
  125.0 3.5 %collective-permute-start.21 = (bf16[128,1152]{0,1:T(8,128)(2,1)}, bf16[128,1152]{0,1:T(8,128)(2,1)}, u32[]{:S(2)}, u32[]{:S(2)}) collective-permute-start(bf16[128,1152]{0,1:T(8,128)(2,1)} %pad_maximum_fusion.3), channel_id=1, source_target_pairs={{0,384},{64,448},{128,0},{192,64},{256,128},{320,192},{384,256},{4... | collective-permute-start | bytes 884744 | tf_op jit(solution)/shard_map/ppermute | solution.py:16
  129.8 3.8 %convolution_convert_fusion = bf16[128,2048]{1,0:T(8,128)(2,1)S(1)} fusion(bf16[2048,768]{1,0:T(8,128)(2,1)} %bitcast.99, bf16[128,2048]{1,0:T(8,128)(2,1)S(1)} %copy-done, f32[128,384]{0,1:T(8,128)S(1)} %convolution_bitcast_fusion.1), kind=kOutput, calls=%fused_computation.2 | convolution fusion | flops 403210240 | bytes 4390912 | tf_op jit(solution)/shard_map/dot_general | solution.py:20
  137.8 6.0 %collective-permute-done.21 = bf16[128,1152]{0,1:T(8,128)(2,1)} collective-permute-done((bf16[128,1152]{0,1:T(8,128)(2,1)}, bf16[128,1152]{0,1:T(8,128)(2,1)}, u32[]{:S(2)}, u32[]{:S(2)}) %collective-permute-start.21) | collective-permute-done | bytes 294944 | tf_op jit(solution)/shard_map/ppermute | solution.py:16
  148.2 4.0 %collective-permute-start.8 = (bf16[32,2048]{1,0:T(8,128)(2,1)S(1)}, bf16[32,2048]{1,0:T(8,128)(2,1)S(1)}, u32[]{:S(2)}, u32[]{:S(2)}) collective-permute-start(bf16[32,2048]{1,0:T(8,128)(2,1)S(1)} %get-tuple-element.21), channel_id=1, source_target_pairs={{0,2},{2,4},{4,6},{6,0},{1,3},{3,5},{5,7},{7,1},{8,10},{10,12},{12... | collective-permute-start | bytes 393224 | tf_op jit(solution)/shard_map/ppermute | solution.py:36
  159.3 5.1 %collective-permute-start.11 = (bf16[32,2048]{1,0:T(8,128)(2,1)S(1)}, bf16[32,2048]{1,0:T(8,128)(2,1)S(1)}, u32[]{:S(2)}, u32[]{:S(2)}) collective-permute-start(bf16[32,2048]{1,0:T(8,128)(2,1)S(1)} %get-tuple-element.6), channel_id=1, source_target_pairs={{0,2},{2,4},{4,6},{6,0},{1,3},{3,5},{5,7},{7,1},{8,10},{10,12},{12... | collective-permute-start | bytes 393224 | tf_op jit(solution)/shard_map/ppermute | solution.py:36
  165.6 6.8 %all-to-all-start.2 = ((bf16[8,64,1152]{2,1,0:T(8,128)(2,1)}), bf16[8,64,1152]{2,1,0:T(8,128)(2,1)S(1)}, u32[]{:S(2)}, u32[]{:S(2)}) async-start(bf16[8,64,1152]{2,1,0:T(8,128)(2,1)} %bitcast.104), calls=%async_computation.2 | async-start | bytes 2359296 | tf_op jit(solution)/shard_map/all_to_all | solution.py:180
  174.3 4.0 %collective-permute-start.13 = (bf16[32,2048]{1,0:T(8,128)(2,1)S(1)}, bf16[32,2048]{1,0:T(8,128)(2,1)S(1)}, u32[]{:S(2)}, u32[]{:S(2)}) collective-permute-start(bf16[32,2048]{1,0:T(8,128)(2,1)S(1)} %get-tuple-element.6), channel_id=1, source_target_pairs={{0,4},{2,6},{4,0},{6,2},{1,5},{3,7},{5,1},{7,3},{8,12},{10,14},{12... | collective-permute-start | bytes 393224 | tf_op jit(solution)/shard_map/ppermute | solution.py:36
  179.3 3.4 %collective-permute-done.13 = bf16[32,2048]{1,0:T(8,128)(2,1)S(1)} collective-permute-done((bf16[32,2048]{1,0:T(8,128)(2,1)S(1)}, bf16[32,2048]{1,0:T(8,128)(2,1)S(1)}, u32[]{:S(2)}, u32[]{:S(2)}) %collective-permute-start.13) | collective-permute-done | bytes 131104 | tf_op jit(solution)/shard_map/ppermute | solution.py:36
  186.6 14.4 %all-to-all-done.2 = bf16[8,64,1152]{2,1,0:T(8,128)(2,1)S(1)} async-done(((bf16[8,64,1152]{2,1,0:T(8,128)(2,1)}), bf16[8,64,1152]{2,1,0:T(8,128)(2,1)S(1)}, u32[]{:S(2)}, u32[]{:S(2)}) %all-to-all-start.2) | async-done | bytes 1179680 | tf_op jit(solution)/shard_map/all_to_all | solution.py:180
  201.1 6.0 %collective-permute-start.22 = (bf16[64,1152]{1,0:T(8,128)(2,1)S(1)}, bf16[64,1152]{1,0:T(8,128)(2,1)S(1)}, u32[]{:S(2)}, u32[]{:S(2)}) collective-permute-start(bf16[64,1152]{1,0:T(8,128)(2,1)S(1)} %reduce_sum.12), channel_id=1, source_target_pairs={{0,256},{256,0},{1,257},{257,1},{2,258},{258,2},{3,259},{259,3},{4... | collective-permute-start | bytes 442376 | tf_op jit(solution)/shard_map/ppermute | solution.py:182
  208.2 5.5 %collective-permute-done.22 = bf16[64,1152]{1,0:T(8,128)(2,1)S(1)} collective-permute-done((bf16[64,1152]{1,0:T(8,128)(2,1)S(1)}, bf16[64,1152]{1,0:T(8,128)(2,1)S(1)}, u32[]{:S(2)}, u32[]{:S(2)}) %collective-permute-start.22) | collective-permute-done | bytes 147488 | tf_op jit(solution)/shard_map/ppermute | solution.py:182
  (105 shorter events, 65.4 us)
Async XLA Ops:
  2.6 30.2 %all-to-all-start.1 = ((bf16[8,64,768]{2,1,0:T(8,128)(2,1)}), bf16[8,64,768]{2,1,0:T(8,128)(2,1)S(1)}, u32[]{:S(2)}, u32[]{:S(2)}) async-start(bf16[8,64,768]{2,1,0:T(8,128)(2,1)} %broadcast_in_dim.78), calls=%async_computation.1 | async-start | bytes 1572864 | tf_op jit(solution)/shard_map/all_to_all | solution.py:44
  9.7 18.5 %collective-permute-start = (bf16[64,384]{1,0:T(8,128)(2,1)S(1)}, bf16[64,384]{1,0:T(8,128)(2,1)S(1)}, u32[]{:S(2)}, u32[]{:S(2)}) collective-permute-start(bf16[64,384]{1,0:T(8,128)(2,1)S(1)} %copy-done.11), channel_id=1, source_target_pairs={{0,64},{64,128},{128,192},{192,256},{256,320},{320,384},{384,448},... | collective-permute-start | bytes 147464 | tf_op jit(solution)/shard_map/ppermute | solution.py:16
  14.0 14.2 %collective-permute-start.1 = (bf16[64,384]{1,0:T(8,128)(2,1)S(1)}, bf16[64,384]{1,0:T(8,128)(2,1)S(1)}, u32[]{:S(2)}, u32[]{:S(2)}) collective-permute-start(bf16[64,384]{1,0:T(8,128)(2,1)S(1)} %copy-done.11), channel_id=1, source_target_pairs={{0,448},{64,0},{128,64},{192,128},{256,192},{320,256},{384,320},{4... | collective-permute-start | bytes 147464 | tf_op jit(solution)/shard_map/ppermute | solution.py:16
  22.6 6.9 %collective-permute-start.2 = (bf16[64,384]{1,0:T(8,128)(2,1)S(1)}, bf16[64,384]{1,0:T(8,128)(2,1)S(1)}, u32[]{:S(2)}, u32[]{:S(2)}) collective-permute-start(bf16[64,384]{1,0:T(8,128)(2,1)S(1)} %copy-done.11), channel_id=1, source_target_pairs={{0,384},{64,448},{128,0},{192,64},{256,128},{320,192},{384,256},{4... | collective-permute-start | bytes 147464 | tf_op jit(solution)/shard_map/ppermute | solution.py:16
  34.2 80.5 %all-to-all-start = ((bf16[8,4,64,384]{3,2,1,0:T(8,128)(2,1)}), bf16[8,4,64,384]{3,2,1,0:T(8,128)(2,1)S(1)}, u32[]{:S(2)}, u32[]{:S(2)}) async-start(bf16[8,4,64,384]{3,2,1,0:T(8,128)(2,1)} %broadcast_in_dim.76), calls=%async_computation | async-start | bytes 3145728 | tf_op jit(solution)/shard_map/all_to_all | solution.py:44
  38.9 14.0 %collective-permute-start.16 = (bf16[64,1024]{1,0:T(8,128)(2,1)S(1)}, bf16[64,1024]{1,0:T(8,128)(2,1)S(1)}, u32[]{:S(2)}, u32[]{:S(2)}) collective-permute-start(bf16[64,1024]{1,0:T(8,128)(2,1)S(1)} %fusion.56), channel_id=1, source_target_pairs={{0,448},{64,0},{128,64},{192,128},{256,192},{320,256},{384,320},{4... | collective-permute-start | bytes 393224 | tf_op jit(solution)/shard_map/ppermute | solution.py:16
  50.5 8.1 %collective-permute-start.17 = (bf16[64,1024]{1,0:T(8,128)(2,1)S(1)}, bf16[64,1024]{1,0:T(8,128)(2,1)}, u32[]{:S(2)}, u32[]{:S(2)}) collective-permute-start(bf16[64,1024]{1,0:T(8,128)(2,1)S(1)} %fusion.55), channel_id=1, source_target_pairs={{0,384},{64,448},{128,0},{192,64},{256,128},{320,192},{384,256},{4... | collective-permute-start | bytes 393224 | tf_op jit(solution)/shard_map/ppermute | solution.py:16
  60.3 7.9 %collective-permute-start.18 = (bf16[2,64,1024]{2,1,0:T(8,128)(2,1)}, bf16[2,64,1024]{2,1,0:T(8,128)(2,1)}, u32[]{:S(2)}, u32[]{:S(2)}) collective-permute-start(bf16[2,64,1024]{2,1,0:T(8,128)(2,1)} %pad_maximum_fusion.5), channel_id=1, source_target_pairs={{0,1},{1,0},{2,3},{3,2},{4,5},{5,4},{6,7},{7,6},{8,9},{9,8},{10,11... | collective-permute-start | bytes 786440 | tf_op jit(solution)/shard_map/ppermute | solution.py:138
  63.9 13.8 %collective-permute-start.15 = (bf16[128,1024]{1,0:T(8,128)(2,1)}, bf16[128,1024]{1,0:T(8,128)(2,1)}, u32[]{:S(2)}, u32[]{:S(2)}) collective-permute-start(bf16[128,1024]{1,0:T(8,128)(2,1)} %pad_maximum_fusion.4), channel_id=1, source_target_pairs={{0,64},{64,128},{128,192},{192,256},{256,320},{320,384},{384,448},... | collective-permute-start | bytes 786440 | tf_op jit(solution)/shard_map/ppermute | solution.py:16
  69.1 25.3 %collective-permute-start.3 = (bf16[8,64,768]{2,1,0:T(8,128)(2,1)S(1)}, bf16[8,64,768]{2,1,0:T(8,128)(2,1)S(1)}, u32[]{:S(2)}, u32[]{:S(2)}) collective-permute-start(bf16[8,64,768]{2,1,0:T(8,128)(2,1)S(1)} %all-to-all-done.1), channel_id=1, source_target_pairs={{0,64},{64,128},{128,192},{192,256},{256,320},{320,384},{384,448},... | collective-permute-start | bytes 2359304 | tf_op jit(solution)/shard_map/ppermute | solution.py:16
  71.3 24.6 %collective-permute-start.4 = (bf16[8,64,768]{2,1,0:T(8,128)(2,1)S(1)}, bf16[8,64,768]{2,1,0:T(8,128)(2,1)S(1)}, u32[]{:S(2)}, u32[]{:S(2)}) collective-permute-start(bf16[8,64,768]{2,1,0:T(8,128)(2,1)S(1)} %all-to-all-done.1), channel_id=1, source_target_pairs={{0,448},{64,0},{128,64},{192,128},{256,192},{320,256},{384,320},{4... | collective-permute-start | bytes 2359304 | tf_op jit(solution)/shard_map/ppermute | solution.py:16
  79.8 32.5 %collective-permute-start.5 = (bf16[4,64,768]{2,1,0:T(8,128)(2,1)S(1)}, bf16[4,64,768]{2,1,0:T(8,128)(2,1)S(1)}, u32[]{:S(2)}, u32[]{:S(2)}) collective-permute-start(bf16[4,64,768]{2,1,0:T(8,128)(2,1)S(1)} %get-tuple-element.9), channel_id=1, source_target_pairs={{0,128},{64,192},{128,256},{192,320},{256,384},{320,448},{384,0},{... | collective-permute-start | bytes 1179656 | tf_op jit(solution)/shard_map/ppermute | solution.py:16
  81.7 30.6 %collective-permute-start.6 = (bf16[4,64,768]{2,1,0:T(8,128)(2,1)S(1)}, bf16[4,64,768]{2,1,0:T(8,128)(2,1)S(1)}, u32[]{:S(2)}, u32[]{:S(2)}) collective-permute-start(bf16[4,64,768]{2,1,0:T(8,128)(2,1)S(1)} %get-tuple-element.10), channel_id=1, source_target_pairs={{0,384},{64,448},{128,0},{192,64},{256,128},{320,192},{384,256},{4... | collective-permute-start | bytes 1179656 | tf_op jit(solution)/shard_map/ppermute | solution.py:16
  118.0 19.8 %collective-permute-start.19 = (bf16[128,1152]{0,1:T(8,128)(2,1)}, bf16[128,1152]{0,1:T(8,128)(2,1)S(1)}, u32[]{:S(2)}, u32[]{:S(2)}) collective-permute-start(bf16[128,1152]{0,1:T(8,128)(2,1)} %pad_maximum_fusion.3), channel_id=1, source_target_pairs={{0,64},{64,128},{128,192},{192,256},{256,320},{320,384},{384,448},... | collective-permute-start | bytes 884744 | tf_op jit(solution)/shard_map/ppermute | solution.py:16
  119.9 17.9 %collective-permute-start.20 = (bf16[128,1152]{0,1:T(8,128)(2,1)}, bf16[128,1152]{0,1:T(8,128)(2,1)}, u32[]{:S(2)}, u32[]{:S(2)}) collective-permute-start(bf16[128,1152]{0,1:T(8,128)(2,1)} %pad_maximum_fusion.3), channel_id=1, source_target_pairs={{0,448},{64,0},{128,64},{192,128},{256,192},{320,256},{384,320},{4... | collective-permute-start | bytes 884744 | tf_op jit(solution)/shard_map/ppermute | solution.py:16
  125.0 18.7 %collective-permute-start.21 = (bf16[128,1152]{0,1:T(8,128)(2,1)}, bf16[128,1152]{0,1:T(8,128)(2,1)}, u32[]{:S(2)}, u32[]{:S(2)}) collective-permute-start(bf16[128,1152]{0,1:T(8,128)(2,1)} %pad_maximum_fusion.3), channel_id=1, source_target_pairs={{0,384},{64,448},{128,0},{192,64},{256,128},{320,192},{384,256},{4... | collective-permute-start | bytes 884744 | tf_op jit(solution)/shard_map/ppermute | solution.py:16
  135.7 9.9 %collective-permute-start.7 = (bf16[4,32,2048]{2,1,0:T(8,128)(2,1)S(1)}, bf16[4,32,2048]{2,1,0:T(8,128)(2,1)S(1)}, u32[]{:S(2)}, u32[]{:S(2)}) collective-permute-start(bf16[4,32,2048]{2,1,0:T(8,128)(2,1)S(1)} %fusion.30), channel_id=1, source_target_pairs={{0,1},{1,0},{2,3},{3,2},{4,5},{5,4},{6,7},{7,6},{8,9},{9,8},{10,11... | collective-permute-start | bytes 1572872 | tf_op jit(solution)/shard_map/ppermute | solution.py:77
  145.8 9.9 %collective-permute-start.10 = (bf16[32,2048]{1,0:T(8,128)(2,1)S(1)}, bf16[32,2048]{1,0:T(8,128)(2,1)S(1)}, u32[]{:S(2)}, u32[]{:S(2)}) collective-permute-start(bf16[32,2048]{1,0:T(8,128)(2,1)S(1)} %get-tuple-element.22), channel_id=1, source_target_pairs={{0,4},{2,6},{4,0},{6,2},{1,5},{3,7},{5,1},{7,3},{8,12},{10,14},{12... | collective-permute-start | bytes 393224 | tf_op jit(solution)/shard_map/ppermute | solution.py:36
  148.2 8.0 %collective-permute-start.8 = (bf16[32,2048]{1,0:T(8,128)(2,1)S(1)}, bf16[32,2048]{1,0:T(8,128)(2,1)S(1)}, u32[]{:S(2)}, u32[]{:S(2)}) collective-permute-start(bf16[32,2048]{1,0:T(8,128)(2,1)S(1)} %get-tuple-element.21), channel_id=1, source_target_pairs={{0,2},{2,4},{4,6},{6,0},{1,3},{3,5},{5,7},{7,1},{8,10},{10,12},{12... | collective-permute-start | bytes 393224 | tf_op jit(solution)/shard_map/ppermute | solution.py:36
  152.2 6.9 %collective-permute-start.9 = (bf16[32,2048]{1,0:T(8,128)(2,1)S(1)}, bf16[32,2048]{1,0:T(8,128)(2,1)S(1)}, u32[]{:S(2)}, u32[]{:S(2)}) collective-permute-start(bf16[32,2048]{1,0:T(8,128)(2,1)S(1)} %get-tuple-element.23), channel_id=1, source_target_pairs={{0,6},{2,0},{4,2},{6,4},{1,7},{3,1},{5,3},{7,5},{8,14},{10,8},{12,... | collective-permute-start | bytes 393224 | tf_op jit(solution)/shard_map/ppermute | solution.py:36
  159.3 19.0 %collective-permute-start.11 = (bf16[32,2048]{1,0:T(8,128)(2,1)S(1)}, bf16[32,2048]{1,0:T(8,128)(2,1)S(1)}, u32[]{:S(2)}, u32[]{:S(2)}) collective-permute-start(bf16[32,2048]{1,0:T(8,128)(2,1)S(1)} %get-tuple-element.6), channel_id=1, source_target_pairs={{0,2},{2,4},{4,6},{6,0},{1,3},{3,5},{5,7},{7,1},{8,10},{10,12},{12... | collective-permute-start | bytes 393224 | tf_op jit(solution)/shard_map/ppermute | solution.py:36
  165.6 35.4 %all-to-all-start.2 = ((bf16[8,64,1152]{2,1,0:T(8,128)(2,1)}), bf16[8,64,1152]{2,1,0:T(8,128)(2,1)S(1)}, u32[]{:S(2)}, u32[]{:S(2)}) async-start(bf16[8,64,1152]{2,1,0:T(8,128)(2,1)} %bitcast.104), calls=%async_computation.2 | async-start | bytes 2359296 | tf_op jit(solution)/shard_map/all_to_all | solution.py:180
  174.3 8.4 %collective-permute-start.13 = (bf16[32,2048]{1,0:T(8,128)(2,1)S(1)}, bf16[32,2048]{1,0:T(8,128)(2,1)S(1)}, u32[]{:S(2)}, u32[]{:S(2)}) collective-permute-start(bf16[32,2048]{1,0:T(8,128)(2,1)S(1)} %get-tuple-element.6), channel_id=1, source_target_pairs={{0,4},{2,6},{4,0},{6,2},{1,5},{3,7},{5,1},{7,3},{8,12},{10,14},{12... | collective-permute-start | bytes 393224 | tf_op jit(solution)/shard_map/ppermute | solution.py:36
  201.1 12.6 %collective-permute-start.22 = (bf16[64,1152]{1,0:T(8,128)(2,1)S(1)}, bf16[64,1152]{1,0:T(8,128)(2,1)S(1)}, u32[]{:S(2)}, u32[]{:S(2)}) collective-permute-start(bf16[64,1152]{1,0:T(8,128)(2,1)S(1)} %reduce_sum.12), channel_id=1, source_target_pairs={{0,256},{256,0},{1,257},{257,1},{2,258},{258,2},{3,259},{259,3},{4... | collective-permute-start | bytes 442376 | tf_op jit(solution)/shard_map/ppermute | solution.py:182
  (14 other events, 315.2 us)

commit v3 on v2

--- a/solution.py
+++ b/solution.py
@@ -64,8 +64,7 @@
         full = put(full, block, jnp.mod(zl - by + NZL, NZL))
     far_low = shift_z(column[: NY // 2], 2)
     far_high = shift_z(column[NY // 2 :], -2)
-    far = jnp.concatenate((far_low, far_high), axis=0)
-    return put(full, far, jnp.mod(zl + 2, NZL))
+    return full, far_low, far_high
 
 
 def reduce_on_tp(late, early, x, c):
@@ -113,7 +112,10 @@
     bf = jnp.bfloat16
     zl = lax.axis_index("zl")
     rows, width = gate_weight.shape
-    part_b = gather_y_then_z((up_weight, down_weight), zl).reshape(-1, 2 * width)
+    near, far_low, far_high = gather_y_then_z((up_weight, down_weight), zl)
+    far = jnp.concatenate((far_low, far_high), axis=0)
+    far_at = jnp.mod(zl + 2, NZL)
+    part_b = put(near, far, far_at).reshape(-1, 2 * width)
     gate_full = gather_z_then_y(gate_weight, zl).reshape(-1, width)
     up_full = part_b[:, :width]
     down_full = part_b[:, width:]
@@ -140,9 +142,22 @@
     far = put(put(far, halves, c, 1), others, 1 - c, 1)
     features += [f.reshape(-1, f.shape[-1]) for f in far]
 
+    near_rows = near.reshape(-1, 2 * width)
+    near_up = dot(earlier_input, near_rows[:, :width])
+    near_grad = dot(cotangent, near_rows[:, width:])
     gate_early = dot(earlier_input, gate_full)
-    up_early = dot(earlier_input, up_full)
-    hidden_grad = dot(cotangent, down_full)
+    near_up, near_grad = lax.optimization_barrier((near_up, near_grad))
+    low = far_low.reshape(-1, 2 * width)
+    high = far_high.reshape(-1, 2 * width)
+    far_x, far_cot = jnp.split(features_for(far_at), 2, axis=1)
+
+    def with_far(total, array, at):
+        n = low.shape[0]
+        total = total + dot(array[:, :n], low[:, at : at + width])
+        return total + dot(array[:, n:], high[:, at : at + width])
+
+    up_early = with_far(near_up, far_x, 0)
+    hidden_grad = with_far(near_grad, far_cot, width)
     sigmoid_gate = jax.nn.sigmoid(gate_early)
     silu_early = gate_early * sigmoid_gate
     gate_grad = (

time: 217 us -> 202 us (0.931)
  waiting for transfers between devices: 71.1 us -> 56.1 us
  starting transfers between devices: 108 us -> 99.8 us
  local copies, waits for them, and re-layouts: 9.97 us -> 16.1 us
  matrix products: 11 us -> 16.9 us
  other arithmetic: 14.2 us -> 10.5 us
    ppermute x13, waiting for transfers between devices: 38.3 us -> 25.2 us  [shift_z(): return lax.ppermute(array, RING, [(i, (i + by) % NZ) for i in range(NZ)])]
    ppermute x13, starting transfers between devices: 58.6 us -> 49.1 us  [shift_z(): return lax.ppermute(array, RING, [(i, (i + by) % NZ) for i in range(NZ)])]
    dot_general x4 -> x8, matrix products: 2.48 us -> 8.37 us  [dot(): return jnp.dot(first, second, preferred_element_type=jnp.float32)]
    dynamic_update_slice x13, local copies, waits for them, and re-layouts: 1.36 us -> 6.96 us  [put(): lax.dynamic_update_slice_in_dim(buffer, jnp.expand_dims(block, dim), at,...]
    concatenate x3, other arithmetic: 3.43 us -> 0.76 us  [features_for(): return jnp.concatenate((cut(earlier_input), cut(cotangent)), axis=1)]
    unnamed x24 -> x26, local copies, waits for them, and re-layouts: 2.77 us -> 0.6 us
  transfers between devices with their start and end apart: 26 -> 26, of which waited for: 15 -> 12; matrix products, arithmetic and copies ran while one was open for 12% -> 19% of each run, Pallas kernels for 0% -> 0%
where the time goes in v3:
time: 202 us; the launch traced here: 201 us
  starting transfers between devices  99.8 us (49%)
  waiting for transfers between devices  56.1 us (28%)
  matrix products  16.9 us (8%)
  local copies, waits for them, and re-layouts  16.1 us (8%)
  other arithmetic  10.5 us (5%)
    ppermute x13, starting transfers between devices, shift_z(): return lax.ppermute(array, RING, [(i, (i + by) % NZ) for i in range(NZ)])  49.1 us
    ppermute x13, waiting for transfers between devices, shift_z(): return lax.ppermute(array, RING, [(i, (i + by) % NZ) for i in range(NZ)])  25.2 us
    ppermute x6, starting transfers between devices, shift(): lax.ppermute(array, axis, [(i, (i + by) % count) for i in range(count)])  20.6 us
    all_to_all x1, waiting for transfers between devices, per_device(): local = lax.all_to_all(local, 'y', split_axis=0, concat_axis=0, tiled=True)  13.2 us
    all_to_all x2, starting transfers between devices, spread_y(): return lax.all_to_all(block, 'y', split_axis=0, concat_axis=0, tiled=True)  10.7 us
    dot_general x8, matrix products, dot(): return jnp.dot(first, second, preferred_element_type=jnp.float32)  8.37 us
    dynamic_update_slice x13, local copies, waits for them, and re-layouts, put(): lax.dynamic_update_slice_in_dim(buffer, jnp.expand_dims(block, dim), at,...  6.96 us
    ppermute x1, starting transfers between devices, per_device(): other = lax.ppermute(mine, 'zh', [(0, 1), (1, 0)])  6.83 us
  transfers between devices with their start and end apart: 26, of which 12 were waited for; matrix products, arithmetic and copies ran while one was open for 19% of the time, Pallas kernels for 0%

profile of v3, /device:TPU:4, one launch (start us, length us, event | category | flops | bytes accessed | tf_op | source)
XLA Modules:
  0.0 200.7 jit_solution(2953498330748738190)
XLA Ops:
  0.7 4.4 %collective-permute-start = (bf16[64,384]{1,0:T(8,128)(2,1)}, bf16[64,384]{1,0:T(8,128)(2,1)}, u32[]{:S(2)}, u32[]{:S(2)}) collective-permute-start(bf16[64,384]{1,0:T(8,128)(2,1)} %param.12), channel_id=1, source_target_pairs={{0,64},{64,128},{128,192},{192,256},{256,320},{320,384},{384,448},... | collective-permute-start | bytes 147464 | tf_op jit(solution)/shard_map/ppermute | solution.py:16
  5.1 8.6 %collective-permute-start.1 = (bf16[64,384]{1,0:T(8,128)(2,1)}, bf16[64,384]{1,0:T(8,128)(2,1)}, u32[]{:S(2)}, u32[]{:S(2)}) collective-permute-start(bf16[64,384]{1,0:T(8,128)(2,1)} %param.12), channel_id=1, source_target_pairs={{0,448},{64,0},{128,64},{192,128},{256,192},{320,256},{384,320},{4... | collective-permute-start | bytes 147464 | tf_op jit(solution)/shard_map/ppermute | solution.py:16
  13.7 3.9 %collective-permute-start.2 = (bf16[64,384]{1,0:T(8,128)(2,1)}, bf16[64,384]{1,0:T(8,128)(2,1)}, u32[]{:S(2)}, u32[]{:S(2)}) collective-permute-start(bf16[64,384]{1,0:T(8,128)(2,1)} %param.12), channel_id=1, source_target_pairs={{0,384},{64,448},{128,0},{192,64},{256,128},{320,192},{384,256},{4... | collective-permute-start | bytes 147464 | tf_op jit(solution)/shard_map/ppermute | solution.py:16
  19.4 7.1 %all-to-all-start.1 = ((bf16[8,64,768]{2,1,0:T(8,128)(2,1)}), bf16[8,64,768]{2,1,0:T(8,128)(2,1)S(1)}, u32[]{:S(2)}, u32[]{:S(2)}) async-start(bf16[8,64,768]{2,1,0:T(8,128)(2,1)} %broadcast_in_dim.78), calls=%async_computation.1 | async-start | bytes 1572864 | tf_op jit(solution)/shard_map/all_to_all | solution.py:44
  27.3 3.7 %collective-permute-start.17 = (bf16[64,1024]{1,0:T(8,128)(2,1)S(1)}, bf16[64,1024]{1,0:T(8,128)(2,1)S(1)}, u32[]{:S(2)}, u32[]{:S(2)}) collective-permute-start(bf16[64,1024]{1,0:T(8,128)(2,1)S(1)} %fusion.63), channel_id=1, source_target_pairs={{0,384},{64,448},{128,0},{192,64},{256,128},{320,192},{384,256},{4... | collective-permute-start | bytes 393224 | tf_op jit(solution)/shard_map/ppermute | solution.py:16
  34.5 3.9 %collective-permute-start.15 = (bf16[128,1024]{1,0:T(8,128)(2,1)}, bf16[128,1024]{1,0:T(8,128)(2,1)}, u32[]{:S(2)}, u32[]{:S(2)}) collective-permute-start(bf16[128,1024]{1,0:T(8,128)(2,1)} %pad_maximum_fusion.4), channel_id=1, source_target_pairs={{0,64},{64,128},{128,192},{192,256},{256,320},{320,384},{384,448},... | collective-permute-start | bytes 786440 | tf_op jit(solution)/shard_map/ppermute | solution.py:16
  45.2 3.6 %all-to-all-done.1 = bf16[8,64,768]{2,1,0:T(8,128)(2,1)S(1)} async-done(((bf16[8,64,768]{2,1,0:T(8,128)(2,1)}), bf16[8,64,768]{2,1,0:T(8,128)(2,1)S(1)}, u32[]{:S(2)}, u32[]{:S(2)}) %all-to-all-start.1) | async-done | bytes 786464 | tf_op jit(solution)/shard_map/all_to_all | solution.py:44
  50.2 3.6 %all-to-all-start = ((bf16[8,4,64,384]{3,2,1,0:T(8,128)(2,1)}), bf16[8,4,64,384]{3,2,1,0:T(8,128)(2,1)S(1)}, u32[]{:S(2)}, u32[]{:S(2)}) async-start(bf16[8,4,64,384]{3,2,1,0:T(8,128)(2,1)} %broadcast_in_dim.76), calls=%async_computation | async-start | bytes 3145728 | tf_op jit(solution)/shard_map/all_to_all | solution.py:44
  54.9 3.7 %collective-permute-start.6 = (bf16[4,64,768]{2,1,0:T(8,128)(2,1)S(1)}, bf16[4,64,768]{2,1,0:T(8,128)(2,1)S(1)}, u32[]{:S(2)}, u32[]{:S(2)}) collective-permute-start(bf16[4,64,768]{2,1,0:T(8,128)(2,1)S(1)} %get-tuple-element.14), channel_id=1, source_target_pairs={{0,384},{64,448},{128,0},{192,64},{256,128},{320,192},{384,256},{4... | collective-permute-start | bytes 1179656 | tf_op jit(solution)/shard_map/ppermute | solution.py:16
  63.5 3.8 %collective-permute-start.5 = (bf16[4,64,768]{2,1,0:T(8,128)(2,1)S(1)}, bf16[4,64,768]{2,1,0:T(8,128)(2,1)S(1)}, u32[]{:S(2)}, u32[]{:S(2)}) collective-permute-start(bf16[4,64,768]{2,1,0:T(8,128)(2,1)S(1)} %get-tuple-element.13), channel_id=1, source_target_pairs={{0,128},{64,192},{128,256},{192,320},{256,384},{320,448},{384,0},{... | collective-permute-start | bytes 1179656 | tf_op jit(solution)/shard_map/ppermute | solution.py:16
  67.3 3.7 %collective-permute-start.4 = (bf16[8,64,768]{2,1,0:T(8,128)(2,1)S(1)}, bf16[8,64,768]{2,1,0:T(8,128)(2,1)S(1)}, u32[]{:S(2)}, u32[]{:S(2)}) collective-permute-start(bf16[8,64,768]{2,1,0:T(8,128)(2,1)S(1)} %all-to-all-done.1), channel_id=1, source_target_pairs={{0,448},{64,0},{128,64},{192,128},{256,192},{320,256},{384,320},{4... | collective-permute-start | bytes 2359304 | tf_op jit(solution)/shard_map/ppermute | solution.py:16
  75.8 12.6 %collective-permute-done.3 = bf16[8,64,768]{2,1,0:T(8,128)(2,1)S(1)} collective-permute-done((bf16[8,64,768]{2,1,0:T(8,128)(2,1)S(1)}, bf16[8,64,768]{2,1,0:T(8,128)(2,1)S(1)}, u32[]{:S(2)}, u32[]{:S(2)}) %collective-permute-start.3) | collective-permute-done | bytes 786464 | tf_op jit(solution)/shard_map/ppermute | solution.py:16
  89.3 4.7 %collective-permute-done.4 = bf16[8,64,768]{2,1,0:T(8,128)(2,1)S(1)} collective-permute-done((bf16[8,64,768]{2,1,0:T(8,128)(2,1)S(1)}, bf16[8,64,768]{2,1,0:T(8,128)(2,1)S(1)}, u32[]{:S(2)}, u32[]{:S(2)}) %collective-permute-start.4) | collective-permute-done | bytes 786464 | tf_op jit(solution)/shard_map/ppermute | solution.py:16
  107.3 4.1 %collective-permute-start.20 = (bf16[128,1152]{0,1:T(8,128)(2,1)}, bf16[128,1152]{0,1:T(8,128)(2,1)}, u32[]{:S(2)}, u32[]{:S(2)}) collective-permute-start(bf16[128,1152]{0,1:T(8,128)(2,1)} %pad_maximum_fusion.3), channel_id=1, source_target_pairs={{0,448},{64,0},{128,64},{192,128},{256,192},{320,256},{384,320},{4... | collective-permute-start | bytes 884744 | tf_op jit(solution)/shard_map/ppermute | solution.py:16
  114.1 3.8 %convolution_convert_fusion = bf16[128,2048]{1,0:T(8,128)(2,1)S(1)} fusion(bf16[2048,768]{1,0:T(8,128)(2,1)} %bitcast.11, bf16[128,2048]{1,0:T(8,128)(2,1)S(1)} %copy-done, f32[128,384]{0,1:T(8,128)S(1)} %convolution_bitcast_fusion.1), kind=kOutput, calls=%fused_computation.2 | convolution fusion | flops 403210240 | bytes 4390912 | tf_op jit(solution)/shard_map/dot_general | solution.py:20
  122.8 6.4 %collective-permute-done.20 = bf16[128,1152]{0,1:T(8,128)(2,1)} collective-permute-done((bf16[128,1152]{0,1:T(8,128)(2,1)}, bf16[128,1152]{0,1:T(8,128)(2,1)}, u32[]{:S(2)}, u32[]{:S(2)}) %collective-permute-start.20) | collective-permute-done | bytes 294944 | tf_op jit(solution)/shard_map/ppermute | solution.py:16
  133.7 4.1 %collective-permute-start.9 = (bf16[32,2048]{1,0:T(8,128)(2,1)S(1)}, bf16[32,2048]{1,0:T(8,128)(2,1)S(1)}, u32[]{:S(2)}, u32[]{:S(2)}) collective-permute-start(bf16[32,2048]{1,0:T(8,128)(2,1)S(1)} %get-tuple-element.27), channel_id=1, source_target_pairs={{0,6},{2,0},{4,2},{6,4},{1,7},{3,1},{5,3},{7,5},{8,14},{10,8},{12,... | collective-permute-start | bytes 393224 | tf_op jit(solution)/shard_map/ppermute | solution.py:36
  141.5 3.1 %collective-permute-done.8 = bf16[32,2048]{1,0:T(8,128)(2,1)S(1)} collective-permute-done((bf16[32,2048]{1,0:T(8,128)(2,1)S(1)}, bf16[32,2048]{1,0:T(8,128)(2,1)S(1)}, u32[]{:S(2)}, u32[]{:S(2)}) %collective-permute-start.8) | collective-permute-done | bytes 131104 | tf_op jit(solution)/shard_map/ppermute | solution.py:36
  148.5 6.8 %all-to-all-start.2 = ((bf16[8,64,1152]{2,1,0:T(8,128)(2,1)}), bf16[8,64,1152]{2,1,0:T(8,128)(2,1)S(1)}, u32[]{:S(2)}, u32[]{:S(2)}) async-start(bf16[8,64,1152]{2,1,0:T(8,128)(2,1)} %bitcast.103), calls=%async_computation.2 | async-start | bytes 2359296 | tf_op jit(solution)/shard_map/all_to_all | solution.py:195
  155.3 3.2 %collective-permute-start.12 = (bf16[32,2048]{1,0:T(8,128)(2,1)S(1)}, bf16[32,2048]{1,0:T(8,128)(2,1)S(1)}, u32[]{:S(2)}, u32[]{:S(2)}) collective-permute-start(bf16[32,2048]{1,0:T(8,128)(2,1)S(1)} %get-tuple-element.10), channel_id=1, source_target_pairs={{0,6},{2,0},{4,2},{6,4},{1,7},{3,1},{5,3},{7,5},{8,14},{10,8},{12,... | collective-permute-start | bytes 393224 | tf_op jit(solution)/shard_map/ppermute | solution.py:36
  158.5 6.3 %collective-permute-start.13 = (bf16[32,2048]{1,0:T(8,128)(2,1)S(1)}, bf16[32,2048]{1,0:T(8,128)(2,1)S(1)}, u32[]{:S(2)}, u32[]{:S(2)}) collective-permute-start(bf16[32,2048]{1,0:T(8,128)(2,1)S(1)} %get-tuple-element.10), channel_id=1, source_target_pairs={{0,4},{2,6},{4,0},{6,2},{1,5},{3,7},{5,1},{7,3},{8,12},{10,14},{12... | collective-permute-start | bytes 393224 | tf_op jit(solution)/shard_map/ppermute | solution.py:36
  171.7 13.2 %all-to-all-done.2 = bf16[8,64,1152]{2,1,0:T(8,128)(2,1)S(1)} async-done(((bf16[8,64,1152]{2,1,0:T(8,128)(2,1)}), bf16[8,64,1152]{2,1,0:T(8,128)(2,1)S(1)}, u32[]{:S(2)}, u32[]{:S(2)}) %all-to-all-start.2) | async-done | bytes 1179680 | tf_op jit(solution)/shard_map/all_to_all | solution.py:195
  185.1 6.8 %collective-permute-start.22 = (bf16[64,1152]{1,0:T(8,128)(2,1)S(1)}, bf16[64,1152]{1,0:T(8,128)(2,1)S(1)}, u32[]{:S(2)}, u32[]{:S(2)}) collective-permute-start(bf16[64,1152]{1,0:T(8,128)(2,1)S(1)} %reduce_sum.12), channel_id=1, source_target_pairs={{0,256},{256,0},{1,257},{257,1},{2,258},{258,2},{3,259},{259,3},{4... | collective-permute-start | bytes 442376 | tf_op jit(solution)/shard_map/ppermute | solution.py:197
  192.9 6.1 %collective-permute-done.22 = bf16[64,1152]{1,0:T(8,128)(2,1)S(1)} collective-permute-done((bf16[64,1152]{1,0:T(8,128)(2,1)S(1)}, bf16[64,1152]{1,0:T(8,128)(2,1)S(1)}, u32[]{:S(2)}, u32[]{:S(2)}) %collective-permute-start.22) | collective-permute-done | bytes 147488 | tf_op jit(solution)/shard_map/ppermute | solution.py:197
  (111 shorter events, 68.4 us)
Async XLA Ops:
  0.7 33.8 %collective-permute-start = (bf16[64,384]{1,0:T(8,128)(2,1)}, bf16[64,384]{1,0:T(8,128)(2,1)}, u32[]{:S(2)}, u32[]{:S(2)}) collective-permute-start(bf16[64,384]{1,0:T(8,128)(2,1)} %param.12), channel_id=1, source_target_pairs={{0,64},{64,128},{128,192},{192,256},{256,320},{320,384},{384,448},... | collective-permute-start | bytes 147464 | tf_op jit(solution)/shard_map/ppermute | solution.py:16
  5.1 34.1 %collective-permute-start.1 = (bf16[64,384]{1,0:T(8,128)(2,1)}, bf16[64,384]{1,0:T(8,128)(2,1)}, u32[]{:S(2)}, u32[]{:S(2)}) collective-permute-start(bf16[64,384]{1,0:T(8,128)(2,1)} %param.12), channel_id=1, source_target_pairs={{0,448},{64,0},{128,64},{192,128},{256,192},{320,256},{384,320},{4... | collective-permute-start | bytes 147464 | tf_op jit(solution)/shard_map/ppermute | solution.py:16
  13.7 28.4 %collective-permute-start.2 = (bf16[64,384]{1,0:T(8,128)(2,1)}, bf16[64,384]{1,0:T(8,128)(2,1)}, u32[]{:S(2)}, u32[]{:S(2)}) collective-permute-start(bf16[64,384]{1,0:T(8,128)(2,1)} %param.12), channel_id=1, source_target_pairs={{0,384},{64,448},{128,0},{192,64},{256,128},{320,192},{384,256},{4... | collective-permute-start | bytes 147464 | tf_op jit(solution)/shard_map/ppermute | solution.py:16
  19.4 29.4 %all-to-all-start.1 = ((bf16[8,64,768]{2,1,0:T(8,128)(2,1)}), bf16[8,64,768]{2,1,0:T(8,128)(2,1)S(1)}, u32[]{:S(2)}, u32[]{:S(2)}) async-start(bf16[8,64,768]{2,1,0:T(8,128)(2,1)} %broadcast_in_dim.78), calls=%async_computation.1 | async-start | bytes 1572864 | tf_op jit(solution)/shard_map/all_to_all | solution.py:44
  27.3 12.8 %collective-permute-start.17 = (bf16[64,1024]{1,0:T(8,128)(2,1)S(1)}, bf16[64,1024]{1,0:T(8,128)(2,1)S(1)}, u32[]{:S(2)}, u32[]{:S(2)}) collective-permute-start(bf16[64,1024]{1,0:T(8,128)(2,1)S(1)} %fusion.63), channel_id=1, source_target_pairs={{0,384},{64,448},{128,0},{192,64},{256,128},{320,192},{384,256},{4... | collective-permute-start | bytes 393224 | tf_op jit(solution)/shard_map/ppermute | solution.py:16
  31.0 9.1 %collective-permute-start.16 = (bf16[64,1024]{1,0:T(8,128)(2,1)S(1)}, bf16[64,1024]{1,0:T(8,128)(2,1)S(1)}, u32[]{:S(2)}, u32[]{:S(2)}) collective-permute-start(bf16[64,1024]{1,0:T(8,128)(2,1)S(1)} %fusion.64), channel_id=1, source_target_pairs={{0,448},{64,0},{128,64},{192,128},{256,192},{320,256},{384,320},{4... | collective-permute-start | bytes 393224 | tf_op jit(solution)/shard_map/ppermute | solution.py:16
  34.5 27.0 %collective-permute-start.15 = (bf16[128,1024]{1,0:T(8,128)(2,1)}, bf16[128,1024]{1,0:T(8,128)(2,1)}, u32[]{:S(2)}, u32[]{:S(2)}) collective-permute-start(bf16[128,1024]{1,0:T(8,128)(2,1)} %pad_maximum_fusion.4), channel_id=1, source_target_pairs={{0,64},{64,128},{128,192},{192,256},{256,320},{320,384},{384,448},... | collective-permute-start | bytes 786440 | tf_op jit(solution)/shard_map/ppermute | solution.py:16
  50.2 51.5 %all-to-all-start = ((bf16[8,4,64,384]{3,2,1,0:T(8,128)(2,1)}), bf16[8,4,64,384]{3,2,1,0:T(8,128)(2,1)S(1)}, u32[]{:S(2)}, u32[]{:S(2)}) async-start(bf16[8,4,64,384]{3,2,1,0:T(8,128)(2,1)} %broadcast_in_dim.76), calls=%async_computation | async-start | bytes 3145728 | tf_op jit(solution)/shard_map/all_to_all | solution.py:44
  54.9 19.6 %collective-permute-start.6 = (bf16[4,64,768]{2,1,0:T(8,128)(2,1)S(1)}, bf16[4,64,768]{2,1,0:T(8,128)(2,1)S(1)}, u32[]{:S(2)}, u32[]{:S(2)}) collective-permute-start(bf16[4,64,768]{2,1,0:T(8,128)(2,1)S(1)} %get-tuple-element.14), channel_id=1, source_target_pairs={{0,384},{64,448},{128,0},{192,64},{256,128},{320,192},{384,256},{4... | collective-permute-start | bytes 1179656 | tf_op jit(solution)/shard_map/ppermute | solution.py:16
  58.6 29.8 %collective-permute-start.3 = (bf16[8,64,768]{2,1,0:T(8,128)(2,1)S(1)}, bf16[8,64,768]{2,1,0:T(8,128)(2,1)S(1)}, u32[]{:S(2)}, u32[]{:S(2)}) collective-permute-start(bf16[8,64,768]{2,1,0:T(8,128)(2,1)S(1)} %all-to-all-done.1), channel_id=1, source_target_pairs={{0,64},{64,128},{128,192},{192,256},{256,320},{320,384},{384,448},... | collective-permute-start | bytes 2359304 | tf_op jit(solution)/shard_map/ppermute | solution.py:16
  63.5 36.2 %collective-permute-start.5 = (bf16[4,64,768]{2,1,0:T(8,128)(2,1)S(1)}, bf16[4,64,768]{2,1,0:T(8,128)(2,1)S(1)}, u32[]{:S(2)}, u32[]{:S(2)}) collective-permute-start(bf16[4,64,768]{2,1,0:T(8,128)(2,1)S(1)} %get-tuple-element.13), channel_id=1, source_target_pairs={{0,128},{64,192},{128,256},{192,320},{256,384},{320,448},{384,0},{... | collective-permute-start | bytes 1179656 | tf_op jit(solution)/shard_map/ppermute | solution.py:16
  67.3 26.7 %collective-permute-start.4 = (bf16[8,64,768]{2,1,0:T(8,128)(2,1)S(1)}, bf16[8,64,768]{2,1,0:T(8,128)(2,1)S(1)}, u32[]{:S(2)}, u32[]{:S(2)}) collective-permute-start(bf16[8,64,768]{2,1,0:T(8,128)(2,1)S(1)} %all-to-all-done.1), channel_id=1, source_target_pairs={{0,448},{64,0},{128,64},{192,128},{256,192},{320,256},{384,320},{4... | collective-permute-start | bytes 2359304 | tf_op jit(solution)/shard_map/ppermute | solution.py:16
  104.7 18.1 %collective-permute-start.21 = (bf16[128,1152]{0,1:T(8,128)(2,1)}, bf16[128,1152]{0,1:T(8,128)(2,1)S(1)}, u32[]{:S(2)}, u32[]{:S(2)}) collective-permute-start(bf16[128,1152]{0,1:T(8,128)(2,1)} %pad_maximum_fusion.3), channel_id=1, source_target_pairs={{0,384},{64,448},{128,0},{192,64},{256,128},{320,192},{384,256},{4... | collective-permute-start | bytes 884744 | tf_op jit(solution)/shard_map/ppermute | solution.py:16
  107.3 22.0 %collective-permute-start.20 = (bf16[128,1152]{0,1:T(8,128)(2,1)}, bf16[128,1152]{0,1:T(8,128)(2,1)}, u32[]{:S(2)}, u32[]{:S(2)}) collective-permute-start(bf16[128,1152]{0,1:T(8,128)(2,1)} %pad_maximum_fusion.3), channel_id=1, source_target_pairs={{0,448},{64,0},{128,64},{192,128},{256,192},{320,256},{384,320},{4... | collective-permute-start | bytes 884744 | tf_op jit(solution)/shard_map/ppermute | solution.py:16
  111.4 17.9 %collective-permute-start.19 = (bf16[128,1152]{0,1:T(8,128)(2,1)}, bf16[128,1152]{0,1:T(8,128)(2,1)}, u32[]{:S(2)}, u32[]{:S(2)}) collective-permute-start(bf16[128,1152]{0,1:T(8,128)(2,1)} %pad_maximum_fusion.3), channel_id=1, source_target_pairs={{0,64},{64,128},{128,192},{192,256},{256,320},{320,384},{384,448},... | collective-permute-start | bytes 884744 | tf_op jit(solution)/shard_map/ppermute | solution.py:16
  120.0 11.1 %collective-permute-start.7 = (bf16[4,32,2048]{2,1,0:T(8,128)(2,1)S(1)}, bf16[4,32,2048]{2,1,0:T(8,128)(2,1)S(1)}, u32[]{:S(2)}, u32[]{:S(2)}) collective-permute-start(bf16[4,32,2048]{2,1,0:T(8,128)(2,1)S(1)} %fusion.32), channel_id=1, source_target_pairs={{0,1},{1,0},{2,3},{3,2},{4,5},{5,4},{6,7},{7,6},{8,9},{9,8},{10,11... | collective-permute-start | bytes 1572872 | tf_op jit(solution)/shard_map/ppermute | solution.py:76
  131.3 9.9 %collective-permute-start.10 = (bf16[32,2048]{1,0:T(8,128)(2,1)S(1)}, bf16[32,2048]{1,0:T(8,128)(2,1)S(1)}, u32[]{:S(2)}, u32[]{:S(2)}) collective-permute-start(bf16[32,2048]{1,0:T(8,128)(2,1)S(1)} %get-tuple-element.26), channel_id=1, source_target_pairs={{0,4},{2,6},{4,0},{6,2},{1,5},{3,7},{5,1},{7,3},{8,12},{10,14},{12... | collective-permute-start | bytes 393224 | tf_op jit(solution)/shard_map/ppermute | solution.py:36
  133.7 7.8 %collective-permute-start.9 = (bf16[32,2048]{1,0:T(8,128)(2,1)S(1)}, bf16[32,2048]{1,0:T(8,128)(2,1)S(1)}, u32[]{:S(2)}, u32[]{:S(2)}) collective-permute-start(bf16[32,2048]{1,0:T(8,128)(2,1)S(1)} %get-tuple-element.27), channel_id=1, source_target_pairs={{0,6},{2,0},{4,2},{6,4},{1,7},{3,1},{5,3},{7,5},{8,14},{10,8},{12,... | collective-permute-start | bytes 393224 | tf_op jit(solution)/shard_map/ppermute | solution.py:36
  137.7 6.9 %collective-permute-start.8 = (bf16[32,2048]{1,0:T(8,128)(2,1)S(1)}, bf16[32,2048]{1,0:T(8,128)(2,1)S(1)}, u32[]{:S(2)}, u32[]{:S(2)}) collective-permute-start(bf16[32,2048]{1,0:T(8,128)(2,1)S(1)} %get-tuple-element.25), channel_id=1, source_target_pairs={{0,2},{2,4},{4,6},{6,0},{1,3},{3,5},{5,7},{7,1},{8,10},{10,12},{12... | collective-permute-start | bytes 393224 | tf_op jit(solution)/shard_map/ppermute | solution.py:36
  144.7 20.1 %collective-permute-start.11 = (bf16[32,2048]{1,0:T(8,128)(2,1)S(1)}, bf16[32,2048]{1,0:T(8,128)(2,1)S(1)}, u32[]{:S(2)}, u32[]{:S(2)}) collective-permute-start(bf16[32,2048]{1,0:T(8,128)(2,1)S(1)} %get-tuple-element.10), channel_id=1, source_target_pairs={{0,2},{2,4},{4,6},{6,0},{1,3},{3,5},{5,7},{7,1},{8,10},{10,12},{12... | collective-permute-start | bytes 393224 | tf_op jit(solution)/shard_map/ppermute | solution.py:36
  148.5 36.4 %all-to-all-start.2 = ((bf16[8,64,1152]{2,1,0:T(8,128)(2,1)}), bf16[8,64,1152]{2,1,0:T(8,128)(2,1)S(1)}, u32[]{:S(2)}, u32[]{:S(2)}) async-start(bf16[8,64,1152]{2,1,0:T(8,128)(2,1)} %bitcast.103), calls=%async_computation.2 | async-start | bytes 2359296 | tf_op jit(solution)/shard_map/all_to_all | solution.py:195
  155.3 9.6 %collective-permute-start.12 = (bf16[32,2048]{1,0:T(8,128)(2,1)S(1)}, bf16[32,2048]{1,0:T(8,128)(2,1)S(1)}, u32[]{:S(2)}, u32[]{:S(2)}) collective-permute-start(bf16[32,2048]{1,0:T(8,128)(2,1)S(1)} %get-tuple-element.10), channel_id=1, source_target_pairs={{0,6},{2,0},{4,2},{6,4},{1,7},{3,1},{5,3},{7,5},{8,14},{10,8},{12,... | collective-permute-start | bytes 393224 | tf_op jit(solution)/shard_map/ppermute | solution.py:36
  158.5 9.3 %collective-permute-start.13 = (bf16[32,2048]{1,0:T(8,128)(2,1)S(1)}, bf16[32,2048]{1,0:T(8,128)(2,1)S(1)}, u32[]{:S(2)}, u32[]{:S(2)}) collective-permute-start(bf16[32,2048]{1,0:T(8,128)(2,1)S(1)} %get-tuple-element.10), channel_id=1, source_target_pairs={{0,4},{2,6},{4,0},{6,2},{1,5},{3,7},{5,1},{7,3},{8,12},{10,14},{12... | collective-permute-start | bytes 393224 | tf_op jit(solution)/shard_map/ppermute | solution.py:36
  185.1 13.9 %collective-permute-start.22 = (bf16[64,1152]{1,0:T(8,128)(2,1)S(1)}, bf16[64,1152]{1,0:T(8,128)(2,1)S(1)}, u32[]{:S(2)}, u32[]{:S(2)}) collective-permute-start(bf16[64,1152]{1,0:T(8,128)(2,1)S(1)} %reduce_sum.12), channel_id=1, source_target_pairs={{0,256},{256,0},{1,257},{257,1},{2,258},{258,2},{3,259},{259,3},{4... | collective-permute-start | bytes 442376 | tf_op jit(solution)/shard_map/ppermute | solution.py:197
  (15 other events, 262.1 us)

commit v4 on v3

--- a/solution.py
+++ b/solution.py
@@ -127,29 +127,20 @@
         return jnp.concatenate((cut(earlier_input), cut(cotangent)), axis=1)
 
     features = [features_for(zl)]
-    c = lax.axis_index("c")
-    halves = []
-    for k, by in enumerate(SHIFTS):
+    for by in SHIFTS:
         sent = features_for(jnp.mod(zl + by + NZL, NZL))
-        if k:
-            tokens_half = sent.shape[0] // 2
-            sent = lax.dynamic_slice_in_dim(sent, c * tokens_half, tokens_half, 0)
-        arrived = shift_z(sent, by)
-        (halves if k else features).append(arrived)
-    halves = jnp.stack(halves)
-    others = lax.ppermute(halves, "c", [(0, 1), (1, 0)])
-    far = jnp.zeros((halves.shape[0], 2, *halves.shape[1:]), halves.dtype)
-    far = put(put(far, halves, c, 1), others, 1 - c, 1)
-    features += [f.reshape(-1, f.shape[-1]) for f in far]
+        features.append(shift_z(sent, by))
 
     near_rows = near.reshape(-1, 2 * width)
     near_up = dot(earlier_input, near_rows[:, :width])
     near_grad = dot(cotangent, near_rows[:, width:])
     gate_early = dot(earlier_input, gate_full)
-    near_up, near_grad = lax.optimization_barrier((near_up, near_grad))
+    far_x, far_cot = jnp.split(features_for(far_at), 2, axis=1)
+    near_up, near_grad, far_x, far_cot = lax.optimization_barrier(
+        (near_up, near_grad, far_x, far_cot)
+    )
     low = far_low.reshape(-1, 2 * width)
     high = far_high.reshape(-1, 2 * width)
-    far_x, far_cot = jnp.split(features_for(far_at), 2, axis=1)
 
     def with_far(total, array, at):
         n = low.shape[0]
@@ -180,7 +171,7 @@
     ).astype(bf)
     tokens = partial_late.shape[0]
     n_tp = lax.axis_size(TP)
-    x = lax.axis_index("x")
+    x, c = lax.axis_index("x"), lax.axis_index("c")
     own = reduce_on_tp(partial_late, partial_early, x, c)
     outs = everywhere_on_tp(own, x, c)
     later_output = outs[:, : tokens // n_tp].reshape(tokens, -1)

time: 202 us -> 195 us (0.965)
  the two profiles are of different devices: /device:TPU:4 before, /device:TPU:6 now
where the time goes in v4:
time: 195 us; the launch traced here: 194 us
  starting transfers between devices  98.1 us (50%)
  waiting for transfers between devices  53.8 us (28%)
  matrix products  16.9 us (9%)
  local copies, waits for them, and re-layouts  12.1 us (6%)
  other arithmetic  11.4 us (6%)
    ppermute x13, starting transfers between devices, shift_z(): return lax.ppermute(array, RING, [(i, (i + by) % NZ) for i in range(NZ)])  51 us
    ppermute x6, starting transfers between devices, shift(): lax.ppermute(array, axis, [(i, (i + by) % count) for i in range(count)])  21.2 us
    ppermute x13, waiting for transfers between devices, shift_z(): return lax.ppermute(array, RING, [(i, (i + by) % NZ) for i in range(NZ)])  17.5 us
    all_to_all x1, waiting for transfers between devices, per_device(): local = lax.all_to_all(local, 'y', split_axis=0, concat_axis=0, tiled=True)  12.9 us
    all_to_all x2, starting transfers between devices, spread_y(): return lax.all_to_all(block, 'y', split_axis=0, concat_axis=0, tiled=True)  10.7 us
    all_to_all x2, waiting for transfers between devices, spread_y(): return lax.all_to_all(block, 'y', split_axis=0, concat_axis=0, tiled=True)  8.87 us
    dot_general x8, matrix products, dot(): return jnp.dot(first, second, preferred_element_type=jnp.float32)  8.37 us
    ppermute x1, waiting for transfers between devices, per_device(): other = lax.ppermute(mine, 'zh', [(0, 1), (1, 0)])  6.93 us
  transfers between devices with their start and end apart: 25, of which 10 were waited for; matrix products, arithmetic and copies ran while one was open for 18% of the time, Pallas kernels for 0%

profile of v4, /device:TPU:6, one launch (start us, length us, event | category | flops | bytes accessed | tf_op | source)
XLA Modules:
  0.0 193.7 jit_solution(9050385028446010226)
XLA Ops:
  0.7 4.4 %collective-permute-start = (bf16[64,384]{1,0:T(8,128)(2,1)}, bf16[64,384]{1,0:T(8,128)(2,1)S(1)}, u32[]{:S(2)}, u32[]{:S(2)}) collective-permute-start(bf16[64,384]{1,0:T(8,128)(2,1)} %param.12), channel_id=1, source_target_pairs={{0,64},{64,128},{128,192},{192,256},{256,320},{320,384},{384,448},... | collective-permute-start | bytes 147464 | tf_op jit(solution)/shard_map/ppermute | solution.py:16
  5.1 8.6 %collective-permute-start.1 = (bf16[64,384]{1,0:T(8,128)(2,1)}, bf16[64,384]{1,0:T(8,128)(2,1)S(1)}, u32[]{:S(2)}, u32[]{:S(2)}) collective-permute-start(bf16[64,384]{1,0:T(8,128)(2,1)} %param.12), channel_id=1, source_target_pairs={{0,448},{64,0},{128,64},{192,128},{256,192},{320,256},{384,320},{4... | collective-permute-start | bytes 147464 | tf_op jit(solution)/shard_map/ppermute | solution.py:16
  13.7 3.9 %collective-permute-start.2 = (bf16[64,384]{1,0:T(8,128)(2,1)}, bf16[64,384]{1,0:T(8,128)(2,1)S(1)}, u32[]{:S(2)}, u32[]{:S(2)}) collective-permute-start(bf16[64,384]{1,0:T(8,128)(2,1)} %param.12), channel_id=1, source_target_pairs={{0,384},{64,448},{128,0},{192,64},{256,128},{320,192},{384,256},{4... | collective-permute-start | bytes 147464 | tf_op jit(solution)/shard_map/ppermute | solution.py:16
  19.4 7.1 %all-to-all-start.1 = ((bf16[8,64,768]{2,1,0:T(8,128)(2,1)}), bf16[8,64,768]{2,1,0:T(8,128)(2,1)S(1)}, u32[]{:S(2)}, u32[]{:S(2)}) async-start(bf16[8,64,768]{2,1,0:T(8,128)(2,1)} %broadcast_in_dim.69), calls=%async_computation.1 | async-start | bytes 1572864 | tf_op jit(solution)/shard_map/all_to_all | solution.py:44
  28.8 3.7 %collective-permute-start.17 = (bf16[128,1024]{1,0:T(8,128)(2,1)}, bf16[128,1024]{1,0:T(8,128)(2,1)}, u32[]{:S(2)}, u32[]{:S(2)}) collective-permute-start(bf16[128,1024]{1,0:T(8,128)(2,1)} %pad_maximum_fusion.6), channel_id=1, source_target_pairs={{0,384},{64,448},{128,0},{192,64},{256,128},{320,192},{384,256},{4... | collective-permute-start | bytes 786440 | tf_op jit(solution)/shard_map/ppermute | solution.py:16
  35.9 3.9 %collective-permute-start.15 = (bf16[128,1024]{1,0:T(8,128)(2,1)}, bf16[128,1024]{1,0:T(8,128)(2,1)}, u32[]{:S(2)}, u32[]{:S(2)}) collective-permute-start(bf16[128,1024]{1,0:T(8,128)(2,1)} %pad_maximum_fusion.4), channel_id=1, source_target_pairs={{0,64},{64,128},{128,192},{192,256},{256,320},{320,384},{384,448},... | collective-permute-start | bytes 786440 | tf_op jit(solution)/shard_map/ppermute | solution.py:16
  39.9 8.9 %all-to-all-done.1 = bf16[8,64,768]{2,1,0:T(8,128)(2,1)S(1)} async-done(((bf16[8,64,768]{2,1,0:T(8,128)(2,1)}), bf16[8,64,768]{2,1,0:T(8,128)(2,1)S(1)}, u32[]{:S(2)}, u32[]{:S(2)}) %all-to-all-start.1) | async-done | bytes 786464 | tf_op jit(solution)/shard_map/all_to_all | solution.py:44
  50.2 3.6 %all-to-all-start = ((bf16[8,4,64,384]{3,2,1,0:T(8,128)(2,1)}), bf16[8,4,64,384]{3,2,1,0:T(8,128)(2,1)S(1)}, u32[]{:S(2)}, u32[]{:S(2)}) async-start(bf16[8,4,64,384]{3,2,1,0:T(8,128)(2,1)} %broadcast_in_dim.67), calls=%async_computation | async-start | bytes 3145728 | tf_op jit(solution)/shard_map/all_to_all | solution.py:44
  53.8 3.4 %collective-permute-start.3 = (bf16[8,64,768]{2,1,0:T(8,128)(2,1)S(1)}, bf16[8,64,768]{2,1,0:T(8,128)(2,1)}, u32[]{:S(2)}, u32[]{:S(2)}) collective-permute-start(bf16[8,64,768]{2,1,0:T(8,128)(2,1)S(1)} %all-to-all-done.1), channel_id=1, source_target_pairs={{0,64},{64,128},{128,192},{192,256},{256,320},{320,384},{384,448},... | collective-permute-start | bytes 2359304 | tf_op jit(solution)/shard_map/ppermute | solution.py:16
  57.2 3.7 %collective-permute-start.4 = (bf16[8,64,768]{2,1,0:T(8,128)(2,1)S(1)}, bf16[8,64,768]{2,1,0:T(8,128)(2,1)S(1)}, u32[]{:S(2)}, u32[]{:S(2)}) collective-permute-start(bf16[8,64,768]{2,1,0:T(8,128)(2,1)S(1)} %all-to-all-done.1), channel_id=1, source_target_pairs={{0,448},{64,0},{128,64},{192,128},{256,192},{320,256},{384,320},{4... | collective-permute-start | bytes 2359304 | tf_op jit(solution)/shard_map/ppermute | solution.py:16
  65.7 4.3 %collective-permute-start.5 = (bf16[4,64,768]{2,1,0:T(8,128)(2,1)S(1)}, bf16[4,64,768]{2,1,0:T(8,128)(2,1)S(1)}, u32[]{:S(2)}, u32[]{:S(2)}) collective-permute-start(bf16[4,64,768]{2,1,0:T(8,128)(2,1)S(1)} %get-tuple-element.17), channel_id=1, source_target_pairs={{0,128},{64,192},{128,256},{192,320},{256,384},{320,448},{384,0},{... | collective-permute-start | bytes 1179656 | tf_op jit(solution)/shard_map/ppermute | solution.py:16
  73.0 12.8 %collective-permute-done.3 = bf16[8,64,768]{2,1,0:T(8,128)(2,1)} collective-permute-done((bf16[8,64,768]{2,1,0:T(8,128)(2,1)S(1)}, bf16[8,64,768]{2,1,0:T(8,128)(2,1)}, u32[]{:S(2)}, u32[]{:S(2)}) %collective-permute-start.3) | collective-permute-done | bytes 786464 | tf_op jit(solution)/shard_map/ppermute | solution.py:16
  101.1 4.9 %collective-permute-start.20 = (bf16[128,1152]{0,1:T(8,128)(2,1)}, bf16[128,1152]{0,1:T(8,128)(2,1)S(1)}, u32[]{:S(2)}, u32[]{:S(2)}) collective-permute-start(bf16[128,1152]{0,1:T(8,128)(2,1)} %pad_maximum_fusion.3), channel_id=1, source_target_pairs={{0,384},{64,448},{128,0},{192,64},{256,128},{320,192},{384,256},{4... | collective-permute-start | bytes 884744 | tf_op jit(solution)/shard_map/ppermute | solution.py:16
  108.0 3.9 %collective-permute-start.18 = (bf16[128,1152]{0,1:T(8,128)(2,1)}, bf16[128,1152]{0,1:T(8,128)(2,1)}, u32[]{:S(2)}, u32[]{:S(2)}) collective-permute-start(bf16[128,1152]{0,1:T(8,128)(2,1)} %pad_maximum_fusion.3), channel_id=1, source_target_pairs={{0,64},{64,128},{128,192},{192,256},{256,320},{320,384},{384,448},... | collective-permute-start | bytes 884744 | tf_op jit(solution)/shard_map/ppermute | solution.py:16
  112.5 3.8 %convolution_convert_fusion = bf16[128,2048]{1,0:T(8,128)(2,1)S(1)} fusion(bf16[2048,768]{1,0:T(8,128)(2,1)} %bitcast.11, bf16[128,2048]{1,0:T(8,128)(2,1)S(1)} %copy-done, f32[128,384]{0,1:T(8,128)S(1)} %convolution_bitcast_fusion.1), kind=kOutput, calls=%fused_computation.2 | convolution fusion | flops 403210240 | bytes 4390912 | tf_op jit(solution)/shard_map/dot_general | solution.py:20
  120.5 3.3 %collective-permute-done.19 = bf16[128,1152]{0,1:T(8,128)(2,1)} collective-permute-done((bf16[128,1152]{0,1:T(8,128)(2,1)}, bf16[128,1152]{0,1:T(8,128)(2,1)}, u32[]{:S(2)}, u32[]{:S(2)}) %collective-permute-start.19) | collective-permute-done | bytes 294944 | tf_op jit(solution)/shard_map/ppermute | solution.py:16
  125.8 3.3 %collective-permute-start.10 = (bf16[32,2048]{1,0:T(8,128)(2,1)S(1)}, bf16[32,2048]{1,0:T(8,128)(2,1)S(1)}, u32[]{:S(2)}, u32[]{:S(2)}) collective-permute-start(bf16[32,2048]{1,0:T(8,128)(2,1)S(1)} %get-tuple-element.28), channel_id=1, source_target_pairs={{0,4},{2,6},{4,0},{6,2},{1,5},{3,7},{5,1},{7,3},{8,12},{10,14},{12... | collective-permute-start | bytes 393224 | tf_op jit(solution)/shard_map/ppermute | solution.py:36
  131.0 5.1 %collective-permute-start.8 = (bf16[32,2048]{1,0:T(8,128)(2,1)S(1)}, bf16[32,2048]{1,0:T(8,128)(2,1)S(1)}, u32[]{:S(2)}, u32[]{:S(2)}) collective-permute-start(bf16[32,2048]{1,0:T(8,128)(2,1)S(1)} %get-tuple-element.27), channel_id=1, source_target_pairs={{0,2},{2,4},{4,6},{6,0},{1,3},{3,5},{5,7},{7,1},{8,10},{10,12},{12... | collective-permute-start | bytes 393224 | tf_op jit(solution)/shard_map/ppermute | solution.py:36
  138.8 5.6 %collective-permute-start.11 = (bf16[32,2048]{1,0:T(8,128)(2,1)S(1)}, bf16[32,2048]{1,0:T(8,128)(2,1)S(1)}, u32[]{:S(2)}, u32[]{:S(2)}) collective-permute-start(bf16[32,2048]{1,0:T(8,128)(2,1)S(1)} %get-tuple-element.14), channel_id=1, source_target_pairs={{0,2},{2,4},{4,6},{6,0},{1,3},{3,5},{5,7},{7,1},{8,10},{10,12},{12... | collective-permute-start | bytes 393224 | tf_op jit(solution)/shard_map/ppermute | solution.py:36
  145.5 6.8 %all-to-all-start.2 = ((bf16[8,64,1152]{2,1,0:T(8,128)(2,1)}), bf16[8,64,1152]{2,1,0:T(8,128)(2,1)S(1)}, u32[]{:S(2)}, u32[]{:S(2)}) async-start(bf16[8,64,1152]{2,1,0:T(8,128)(2,1)} %bitcast.91), calls=%async_computation.2 | async-start | bytes 2359296 | tf_op jit(solution)/shard_map/all_to_all | solution.py:186
  154.2 3.4 %collective-permute-start.13 = (bf16[32,2048]{1,0:T(8,128)(2,1)S(1)}, bf16[32,2048]{1,0:T(8,128)(2,1)S(1)}, u32[]{:S(2)}, u32[]{:S(2)}) collective-permute-start(bf16[32,2048]{1,0:T(8,128)(2,1)S(1)} %get-tuple-element.14), channel_id=1, source_target_pairs={{0,4},{2,6},{4,0},{6,2},{1,5},{3,7},{5,1},{7,3},{8,12},{10,14},{12... | collective-permute-start | bytes 393224 | tf_op jit(solution)/shard_map/ppermute | solution.py:36
  166.5 12.9 %all-to-all-done.2 = bf16[8,64,1152]{2,1,0:T(8,128)(2,1)S(1)} async-done(((bf16[8,64,1152]{2,1,0:T(8,128)(2,1)}), bf16[8,64,1152]{2,1,0:T(8,128)(2,1)S(1)}, u32[]{:S(2)}, u32[]{:S(2)}) %all-to-all-start.2) | async-done | bytes 1179680 | tf_op jit(solution)/shard_map/all_to_all | solution.py:186
  179.5 4.5 %collective-permute-start.21 = (bf16[64,1152]{1,0:T(8,128)(2,1)S(1)}, bf16[64,1152]{1,0:T(8,128)(2,1)S(1)}, u32[]{:S(2)}, u32[]{:S(2)}) collective-permute-start(bf16[64,1152]{1,0:T(8,128)(2,1)S(1)} %reduce_sum.12), channel_id=1, source_target_pairs={{0,256},{256,0},{1,257},{257,1},{2,258},{258,2},{3,259},{259,3},{4... | collective-permute-start | bytes 442376 | tf_op jit(solution)/shard_map/ppermute | solution.py:188
  185.1 6.9 %collective-permute-done.21 = bf16[64,1152]{1,0:T(8,128)(2,1)S(1)} collective-permute-done((bf16[64,1152]{1,0:T(8,128)(2,1)S(1)}, bf16[64,1152]{1,0:T(8,128)(2,1)S(1)}, u32[]{:S(2)}, u32[]{:S(2)}) %collective-permute-start.21) | collective-permute-done | bytes 147488 | tf_op jit(solution)/shard_map/ppermute | solution.py:188
  (107 shorter events, 59.7 us)
Async XLA Ops:
  0.7 35.2 %collective-permute-start = (bf16[64,384]{1,0:T(8,128)(2,1)}, bf16[64,384]{1,0:T(8,128)(2,1)S(1)}, u32[]{:S(2)}, u32[]{:S(2)}) collective-permute-start(bf16[64,384]{1,0:T(8,128)(2,1)} %param.12), channel_id=1, source_target_pairs={{0,64},{64,128},{128,192},{192,256},{256,320},{320,384},{384,448},... | collective-permute-start | bytes 147464 | tf_op jit(solution)/shard_map/ppermute | solution.py:16
  5.1 34.8 %collective-permute-start.1 = (bf16[64,384]{1,0:T(8,128)(2,1)}, bf16[64,384]{1,0:T(8,128)(2,1)S(1)}, u32[]{:S(2)}, u32[]{:S(2)}) collective-permute-start(bf16[64,384]{1,0:T(8,128)(2,1)} %param.12), channel_id=1, source_target_pairs={{0,448},{64,0},{128,64},{192,128},{256,192},{320,256},{384,320},{4... | collective-permute-start | bytes 147464 | tf_op jit(solution)/shard_map/ppermute | solution.py:16
  13.7 26.2 %collective-permute-start.2 = (bf16[64,384]{1,0:T(8,128)(2,1)}, bf16[64,384]{1,0:T(8,128)(2,1)S(1)}, u32[]{:S(2)}, u32[]{:S(2)}) collective-permute-start(bf16[64,384]{1,0:T(8,128)(2,1)} %param.12), channel_id=1, source_target_pairs={{0,384},{64,448},{128,0},{192,64},{256,128},{320,192},{384,256},{4... | collective-permute-start | bytes 147464 | tf_op jit(solution)/shard_map/ppermute | solution.py:16
  19.4 29.4 %all-to-all-start.1 = ((bf16[8,64,768]{2,1,0:T(8,128)(2,1)}), bf16[8,64,768]{2,1,0:T(8,128)(2,1)S(1)}, u32[]{:S(2)}, u32[]{:S(2)}) async-start(bf16[8,64,768]{2,1,0:T(8,128)(2,1)} %broadcast_in_dim.69), calls=%async_computation.1 | async-start | bytes 1572864 | tf_op jit(solution)/shard_map/all_to_all | solution.py:44
  28.8 32.1 %collective-permute-start.17 = (bf16[128,1024]{1,0:T(8,128)(2,1)}, bf16[128,1024]{1,0:T(8,128)(2,1)}, u32[]{:S(2)}, u32[]{:S(2)}) collective-permute-start(bf16[128,1024]{1,0:T(8,128)(2,1)} %pad_maximum_fusion.6), channel_id=1, source_target_pairs={{0,384},{64,448},{128,0},{192,64},{256,128},{320,192},{384,256},{4... | collective-permute-start | bytes 786440 | tf_op jit(solution)/shard_map/ppermute | solution.py:16
  33.2 27.7 %collective-permute-start.16 = (bf16[128,1024]{1,0:T(8,128)(2,1)}, bf16[128,1024]{1,0:T(8,128)(2,1)}, u32[]{:S(2)}, u32[]{:S(2)}) collective-permute-start(bf16[128,1024]{1,0:T(8,128)(2,1)} %pad_maximum_fusion.5), channel_id=1, source_target_pairs={{0,448},{64,0},{128,64},{192,128},{256,192},{320,256},{384,320},{4... | collective-permute-start | bytes 786440 | tf_op jit(solution)/shard_map/ppermute | solution.py:16
  35.9 25.0 %collective-permute-start.15 = (bf16[128,1024]{1,0:T(8,128)(2,1)}, bf16[128,1024]{1,0:T(8,128)(2,1)}, u32[]{:S(2)}, u32[]{:S(2)}) collective-permute-start(bf16[128,1024]{1,0:T(8,128)(2,1)} %pad_maximum_fusion.4), channel_id=1, source_target_pairs={{0,64},{64,128},{128,192},{192,256},{256,320},{320,384},{384,448},... | collective-permute-start | bytes 786440 | tf_op jit(solution)/shard_map/ppermute | solution.py:16
  50.2 47.9 %all-to-all-start = ((bf16[8,4,64,384]{3,2,1,0:T(8,128)(2,1)}), bf16[8,4,64,384]{3,2,1,0:T(8,128)(2,1)S(1)}, u32[]{:S(2)}, u32[]{:S(2)}) async-start(bf16[8,4,64,384]{3,2,1,0:T(8,128)(2,1)} %broadcast_in_dim.67), calls=%async_computation | async-start | bytes 3145728 | tf_op jit(solution)/shard_map/all_to_all | solution.py:44
  53.8 32.0 %collective-permute-start.3 = (bf16[8,64,768]{2,1,0:T(8,128)(2,1)S(1)}, bf16[8,64,768]{2,1,0:T(8,128)(2,1)}, u32[]{:S(2)}, u32[]{:S(2)}) collective-permute-start(bf16[8,64,768]{2,1,0:T(8,128)(2,1)S(1)} %all-to-all-done.1), channel_id=1, source_target_pairs={{0,64},{64,128},{128,192},{192,256},{256,320},{320,384},{384,448},... | collective-permute-start | bytes 2359304 | tf_op jit(solution)/shard_map/ppermute | solution.py:16
  57.2 30.7 %collective-permute-start.4 = (bf16[8,64,768]{2,1,0:T(8,128)(2,1)S(1)}, bf16[8,64,768]{2,1,0:T(8,128)(2,1)S(1)}, u32[]{:S(2)}, u32[]{:S(2)}) collective-permute-start(bf16[8,64,768]{2,1,0:T(8,128)(2,1)S(1)} %all-to-all-done.1), channel_id=1, source_target_pairs={{0,448},{64,0},{128,64},{192,128},{256,192},{320,256},{384,320},{4... | collective-permute-start | bytes 2359304 | tf_op jit(solution)/shard_map/ppermute | solution.py:16
  63.3 31.6 %collective-permute-start.6 = (bf16[4,64,768]{2,1,0:T(8,128)(2,1)S(1)}, bf16[4,64,768]{2,1,0:T(8,128)(2,1)S(1)}, u32[]{:S(2)}, u32[]{:S(2)}) collective-permute-start(bf16[4,64,768]{2,1,0:T(8,128)(2,1)S(1)} %get-tuple-element.18), channel_id=1, source_target_pairs={{0,384},{64,448},{128,0},{192,64},{256,128},{320,192},{384,256},{4... | collective-permute-start | bytes 1179656 | tf_op jit(solution)/shard_map/ppermute | solution.py:16
  65.7 29.2 %collective-permute-start.5 = (bf16[4,64,768]{2,1,0:T(8,128)(2,1)S(1)}, bf16[4,64,768]{2,1,0:T(8,128)(2,1)S(1)}, u32[]{:S(2)}, u32[]{:S(2)}) collective-permute-start(bf16[4,64,768]{2,1,0:T(8,128)(2,1)S(1)} %get-tuple-element.17), channel_id=1, source_target_pairs={{0,128},{64,192},{128,256},{192,320},{256,384},{320,448},{384,0},{... | collective-permute-start | bytes 1179656 | tf_op jit(solution)/shard_map/ppermute | solution.py:16
  101.1 19.4 %collective-permute-start.20 = (bf16[128,1152]{0,1:T(8,128)(2,1)}, bf16[128,1152]{0,1:T(8,128)(2,1)S(1)}, u32[]{:S(2)}, u32[]{:S(2)}) collective-permute-start(bf16[128,1152]{0,1:T(8,128)(2,1)} %pad_maximum_fusion.3), channel_id=1, source_target_pairs={{0,384},{64,448},{128,0},{192,64},{256,128},{320,192},{384,256},{4... | collective-permute-start | bytes 884744 | tf_op jit(solution)/shard_map/ppermute | solution.py:16
  106.0 17.7 %collective-permute-start.19 = (bf16[128,1152]{0,1:T(8,128)(2,1)}, bf16[128,1152]{0,1:T(8,128)(2,1)}, u32[]{:S(2)}, u32[]{:S(2)}) collective-permute-start(bf16[128,1152]{0,1:T(8,128)(2,1)} %pad_maximum_fusion.3), channel_id=1, source_target_pairs={{0,448},{64,0},{128,64},{192,128},{256,192},{320,256},{384,320},{4... | collective-permute-start | bytes 884744 | tf_op jit(solution)/shard_map/ppermute | solution.py:16
  108.0 15.8 %collective-permute-start.18 = (bf16[128,1152]{0,1:T(8,128)(2,1)}, bf16[128,1152]{0,1:T(8,128)(2,1)}, u32[]{:S(2)}, u32[]{:S(2)}) collective-permute-start(bf16[128,1152]{0,1:T(8,128)(2,1)} %pad_maximum_fusion.3), channel_id=1, source_target_pairs={{0,64},{64,128},{128,192},{192,256},{256,320},{320,384},{384,448},... | collective-permute-start | bytes 884744 | tf_op jit(solution)/shard_map/ppermute | solution.py:16
  118.4 7.2 %collective-permute-start.7 = (bf16[4,32,2048]{2,1,0:T(8,128)(2,1)S(1)}, bf16[4,32,2048]{2,1,0:T(8,128)(2,1)S(1)}, u32[]{:S(2)}, u32[]{:S(2)}) collective-permute-start(bf16[4,32,2048]{2,1,0:T(8,128)(2,1)S(1)} %fusion.32), channel_id=1, source_target_pairs={{0,1},{1,0},{2,3},{3,2},{4,5},{5,4},{6,7},{7,6},{8,9},{9,8},{10,11... | collective-permute-start | bytes 1572872 | tf_op jit(solution)/shard_map/ppermute | solution.py:76
  125.8 11.8 %collective-permute-start.10 = (bf16[32,2048]{1,0:T(8,128)(2,1)S(1)}, bf16[32,2048]{1,0:T(8,128)(2,1)S(1)}, u32[]{:S(2)}, u32[]{:S(2)}) collective-permute-start(bf16[32,2048]{1,0:T(8,128)(2,1)S(1)} %get-tuple-element.28), channel_id=1, source_target_pairs={{0,4},{2,6},{4,0},{6,2},{1,5},{3,7},{5,1},{7,3},{8,12},{10,14},{12... | collective-permute-start | bytes 393224 | tf_op jit(solution)/shard_map/ppermute | solution.py:36
  129.1 8.5 %collective-permute-start.9 = (bf16[32,2048]{1,0:T(8,128)(2,1)S(1)}, bf16[32,2048]{1,0:T(8,128)(2,1)S(1)}, u32[]{:S(2)}, u32[]{:S(2)}) collective-permute-start(bf16[32,2048]{1,0:T(8,128)(2,1)S(1)} %get-tuple-element.29), channel_id=1, source_target_pairs={{0,6},{2,0},{4,2},{6,4},{1,7},{3,1},{5,3},{7,5},{8,14},{10,8},{12,... | collective-permute-start | bytes 393224 | tf_op jit(solution)/shard_map/ppermute | solution.py:36
  131.0 7.6 %collective-permute-start.8 = (bf16[32,2048]{1,0:T(8,128)(2,1)S(1)}, bf16[32,2048]{1,0:T(8,128)(2,1)S(1)}, u32[]{:S(2)}, u32[]{:S(2)}) collective-permute-start(bf16[32,2048]{1,0:T(8,128)(2,1)S(1)} %get-tuple-element.27), channel_id=1, source_target_pairs={{0,2},{2,4},{4,6},{6,0},{1,3},{3,5},{5,7},{7,1},{8,10},{10,12},{12... | collective-permute-start | bytes 393224 | tf_op jit(solution)/shard_map/ppermute | solution.py:36
  138.8 18.8 %collective-permute-start.11 = (bf16[32,2048]{1,0:T(8,128)(2,1)S(1)}, bf16[32,2048]{1,0:T(8,128)(2,1)S(1)}, u32[]{:S(2)}, u32[]{:S(2)}) collective-permute-start(bf16[32,2048]{1,0:T(8,128)(2,1)S(1)} %get-tuple-element.14), channel_id=1, source_target_pairs={{0,2},{2,4},{4,6},{6,0},{1,3},{3,5},{5,7},{7,1},{8,10},{10,12},{12... | collective-permute-start | bytes 393224 | tf_op jit(solution)/shard_map/ppermute | solution.py:36
  145.5 33.8 %all-to-all-start.2 = ((bf16[8,64,1152]{2,1,0:T(8,128)(2,1)}), bf16[8,64,1152]{2,1,0:T(8,128)(2,1)S(1)}, u32[]{:S(2)}, u32[]{:S(2)}) async-start(bf16[8,64,1152]{2,1,0:T(8,128)(2,1)} %bitcast.91), calls=%async_computation.2 | async-start | bytes 2359296 | tf_op jit(solution)/shard_map/all_to_all | solution.py:186
  152.3 8.1 %collective-permute-start.12 = (bf16[32,2048]{1,0:T(8,128)(2,1)S(1)}, bf16[32,2048]{1,0:T(8,128)(2,1)S(1)}, u32[]{:S(2)}, u32[]{:S(2)}) collective-permute-start(bf16[32,2048]{1,0:T(8,128)(2,1)S(1)} %get-tuple-element.14), channel_id=1, source_target_pairs={{0,6},{2,0},{4,2},{6,4},{1,7},{3,1},{5,3},{7,5},{8,14},{10,8},{12,... | collective-permute-start | bytes 393224 | tf_op jit(solution)/shard_map/ppermute | solution.py:36
  154.2 8.4 %collective-permute-start.13 = (bf16[32,2048]{1,0:T(8,128)(2,1)S(1)}, bf16[32,2048]{1,0:T(8,128)(2,1)S(1)}, u32[]{:S(2)}, u32[]{:S(2)}) collective-permute-start(bf16[32,2048]{1,0:T(8,128)(2,1)S(1)} %get-tuple-element.14), channel_id=1, source_target_pairs={{0,4},{2,6},{4,0},{6,2},{1,5},{3,7},{5,1},{7,3},{8,12},{10,14},{12... | collective-permute-start | bytes 393224 | tf_op jit(solution)/shard_map/ppermute | solution.py:36
  179.5 12.5 %collective-permute-start.21 = (bf16[64,1152]{1,0:T(8,128)(2,1)S(1)}, bf16[64,1152]{1,0:T(8,128)(2,1)S(1)}, u32[]{:S(2)}, u32[]{:S(2)}) collective-permute-start(bf16[64,1152]{1,0:T(8,128)(2,1)S(1)} %reduce_sum.12), channel_id=1, source_target_pairs={{0,256},{256,0},{1,257},{257,1},{2,258},{258,2},{3,259},{259,3},{4... | collective-permute-start | bytes 442376 | tf_op jit(solution)/shard_map/ppermute | solution.py:188
  (16 other events, 262.7 us)

commit v5 on v4

--- a/solution.py
+++ b/solution.py
@@ -1,6 +1,9 @@
+import functools
+
 import jax
 import jax.numpy as jnp
 from jax import lax
+from jax.experimental import pallas as pl
 from jax.sharding import Mesh, PartitionSpec as P
 
 
@@ -96,6 +99,69 @@
     both = put(both, line, c, 1)
     both = put(both, other, 1 - c, 1)
     return both.reshape(2 * n_x, *own.shape)
+
+
+def early_kernel(gate, near_up, near_grad, far_x, far_cot, low, high, out):
+    n, width = low.shape[0], gate.shape[1]
+
+    def full(near, far, at):
+        cols = slice(at, at + width)
+        return (
+            near[...] + dot(far[:, :n], low[:, cols]) + dot(far[:, n:], high[:, cols])
+        )
+
+    g = gate[...]
+    up = full(near_up, far_x, 0)
+    grad = full(near_grad, far_cot, width)
+    s = jax.nn.sigmoid(g)
+    silu = g * s
+    out[:, :width] = (grad * up * s * (1.0 + g * (1.0 - s))).astype(out.dtype)
+    out[:, width : 2 * width] = (grad * silu).astype(out.dtype)
+    out[:, 2 * width :] = (silu * up).astype(out.dtype)
+
+
+def early_piece(*arrays):
+    tokens, width = arrays[0].shape
+    return pl.pallas_call(
+        early_kernel,
+        out_shape=jax.ShapeDtypeStruct((tokens, 3 * width), jnp.bfloat16),
+        cost_estimate=pl.CostEstimate(
+            flops=800_000_000, bytes_accessed=2_600_000, transcendentals=50_000
+        ),
+    )(*arrays)
+
+
+def grads_kernel(count, *refs):
+    x, cot, pieces, out = (
+        refs[:count],
+        refs[count : 2 * count],
+        refs[2 * count : 3 * count],
+        refs[3 * count],
+    )
+    cut = out.shape[1] * 2 // 3
+    both = sum(contract_first(a[...], p[:, :cut]) for a, p in zip(x, pieces))
+    out[:, :cut] = both.astype(out.dtype)
+    down = sum(contract_first(a[...], p[:, cut:]) for a, p in zip(cot, pieces))
+    out[:, cut:] = down.astype(out.dtype)
+
+
+def local_grads(features, pieces):
+    count, (tokens, columns) = len(features), features[0].shape
+    rows, width = columns // 2, pieces[0].shape[1]
+    step = 128
+    steps = rows // step
+    return pl.pallas_call(
+        functools.partial(grads_kernel, count),
+        grid=(steps,),
+        in_specs=[pl.BlockSpec((tokens, step), lambda i: (0, i))] * count
+        + [pl.BlockSpec((tokens, step), lambda i: (0, steps + i))] * count
+        + [pl.BlockSpec((tokens, width), lambda i: (0, 0))] * count,
+        out_specs=pl.BlockSpec((step, width), lambda i: (i, 0)),
+        out_shape=jax.ShapeDtypeStruct((rows, width), jnp.bfloat16),
+        cost_estimate=pl.CostEstimate(
+            flops=1_200_000_000, bytes_accessed=3_400_000, transcendentals=0
+        ),
+    )(*features, *features, *pieces)
 
 
 def per_device(
@@ -142,22 +208,12 @@
     low = far_low.reshape(-1, 2 * width)
     high = far_high.reshape(-1, 2 * width)
 
-    def with_far(total, array, at):
-        n = low.shape[0]
-        total = total + dot(array[:, :n], low[:, at : at + width])
-        return total + dot(array[:, n:], high[:, at : at + width])
-
-    up_early = with_far(near_up, far_x, 0)
-    hidden_grad = with_far(near_grad, far_cot, width)
-    sigmoid_gate = jax.nn.sigmoid(gate_early)
-    silu_early = gate_early * sigmoid_gate
-    gate_grad = (
-        hidden_grad * up_early * sigmoid_gate * (1.0 + gate_early * (1.0 - sigmoid_gate))
-    ).astype(bf)
-    up_grad = (hidden_grad * silu_early).astype(bf)
-    hidden_early = (silu_early * up_early).astype(bf)
-
-    piece = jnp.concatenate((gate_grad, up_grad, hidden_early), axis=1)
+    piece = early_piece(
+        gate_early, near_up, near_grad, far_x, far_cot, low, high
+    )
+    gate_grad = piece[:, :width]
+    up_grad = piece[:, width : 2 * width]
+
     pieces = [piece]
     for by in SHIFTS:
         pieces.append(shift_z(piece, by))
@@ -177,11 +233,7 @@
     later_output = outs[:, : tokens // n_tp].reshape(tokens, -1)
     earlier_input_grad = outs[:, tokens // n_tp :].reshape(tokens, -1)
 
-    first = jnp.concatenate(features, axis=0)
-    second = jnp.concatenate(pieces, axis=0)
-    both_local = contract_first(first[:, :block], second[:, : 2 * width])
-    down_local = contract_first(first[:, block:], second[:, 2 * width :])
-    local = jnp.concatenate((both_local.astype(bf), down_local.astype(bf)), axis=1)
+    local = local_grads(features, pieces)
     local = local.reshape(NY, rows, 3 * width)
     local = lax.all_to_all(local, "y", split_axis=0, concat_axis=0, tiled=True)
     mine = jnp.sum(local.astype(jnp.float32), axis=0).astype(bf)

time: 195 us -> 220 us (1.13)
  the two profiles are of different devices: /device:TPU:6 before, /device:TPU:129 now
where the time goes in v5:
time: 220 us; the launch traced here: 219 us
  starting transfers between devices  95.9 us (44%)
  waiting for transfers between devices  78.8 us (36%)
  matrix products  14.1 us (6%)
  local copies, waits for them, and re-layouts  13.1 us (6%)
  other arithmetic  8.41 us (4%)
  Pallas kernels  7.23 us (3%)
    ppermute x13, starting transfers between devices, shift_z(): return lax.ppermute(array, RING, [(i, (i + by) % NZ) for i in range(NZ)])  47 us
    ppermute x13, waiting for transfers between devices, shift_z(): return lax.ppermute(array, RING, [(i, (i + by) % NZ) for i in range(NZ)])  39.8 us
    ppermute x6, starting transfers between devices, shift(): lax.ppermute(array, axis, [(i, (i + by) % count) for i in range(count)])  17.8 us
    all_to_all x1, waiting for transfers between devices, per_device(): local = lax.all_to_all(local, 'y', split_axis=0, concat_axis=0, tiled=True)  15.7 us
    all_to_all x2, starting transfers between devices, spread_y(): return lax.all_to_all(block, 'y', split_axis=0, concat_axis=0, tiled=True)  11.3 us
    ppermute x1, waiting for transfers between devices, per_device(): other = lax.ppermute(mine, 'zh', [(0, 1), (1, 0)])  8.95 us
    all_to_all x2, waiting for transfers between devices, spread_y(): return lax.all_to_all(block, 'y', split_axis=0, concat_axis=0, tiled=True)  7.97 us
    dot_general x3, matrix products, contract_last(): lax.dot_general(first, second, (((1,), (1,)), ((), ())), preferred_elemen...  7.37 us
  transfers between devices with their start and end apart: 25, of which 13 were waited for; matrix products, arithmetic and copies ran while one was open for 9% of the time, Pallas kernels for 2%

profile of v5, /device:TPU:129, one launch (start us, length us, event | category | flops | bytes accessed | tf_op | source)
XLA Modules:
  0.0 219.0 jit_solution(2384515444162961722)
XLA Ops:
  2.5 6.8 %all-to-all-start.1 = ((bf16[8,64,768]{2,1,0:T(8,128)(2,1)}), bf16[8,64,768]{2,1,0:T(8,128)(2,1)S(1)}, u32[]{:S(2)}, u32[]{:S(2)}) async-start(bf16[8,64,768]{2,1,0:T(8,128)(2,1)} %broadcast_in_dim.69), calls=%async_computation.1 | async-start | bytes 1572864 | tf_op jit(solution)/shard_map/all_to_all | solution.py:47
  9.3 4.0 %collective-permute-start = (bf16[64,384]{1,0:T(8,128)(2,1)S(1)}, bf16[64,384]{1,0:T(8,128)(2,1)S(1)}, u32[]{:S(2)}, u32[]{:S(2)}) collective-permute-start(bf16[64,384]{1,0:T(8,128)(2,1)S(1)} %copy-done.17), channel_id=1, source_target_pairs={{0,64},{64,128},{128,192},{192,256},{256,320},{320,384},{384,448},... | collective-permute-start | bytes 147464 | tf_op jit(solution)/shard_map/ppermute | solution.py:19
  15.3 7.0 %collective-permute-start.2 = (bf16[64,384]{1,0:T(8,128)(2,1)S(1)}, bf16[64,384]{1,0:T(8,128)(2,1)S(1)}, u32[]{:S(2)}, u32[]{:S(2)}) collective-permute-start(bf16[64,384]{1,0:T(8,128)(2,1)S(1)} %copy-done.17), channel_id=1, source_target_pairs={{0,384},{64,448},{128,0},{192,64},{256,128},{320,192},{384,256},{4... | collective-permute-start | bytes 147464 | tf_op jit(solution)/shard_map/ppermute | solution.py:19
  24.9 8.0 %all-to-all-done.1 = bf16[8,64,768]{2,1,0:T(8,128)(2,1)S(1)} async-done(((bf16[8,64,768]{2,1,0:T(8,128)(2,1)}), bf16[8,64,768]{2,1,0:T(8,128)(2,1)S(1)}, u32[]{:S(2)}, u32[]{:S(2)}) %all-to-all-start.1) | async-done | bytes 786464 | tf_op jit(solution)/shard_map/all_to_all | solution.py:47
  34.3 4.4 %all-to-all-start = ((bf16[8,4,64,384]{3,2,1,0:T(8,128)(2,1)}), bf16[8,4,64,384]{3,2,1,0:T(8,128)(2,1)}, u32[]{:S(2)}, u32[]{:S(2)}) async-start(bf16[8,4,64,384]{3,2,1,0:T(8,128)(2,1)} %broadcast_in_dim.67), calls=%async_computation | async-start | bytes 3145728 | tf_op jit(solution)/shard_map/all_to_all | solution.py:47
  38.8 4.0 %collective-permute-start.3 = (bf16[8,64,768]{2,1,0:T(8,128)(2,1)S(1)}, bf16[8,64,768]{2,1,0:T(8,128)(2,1)S(1)}, u32[]{:S(2)}, u32[]{:S(2)}) collective-permute-start(bf16[8,64,768]{2,1,0:T(8,128)(2,1)S(1)} %all-to-all-done.1), channel_id=1, source_target_pairs={{0,64},{64,128},{128,192},{192,256},{256,320},{320,384},{384,448},... | collective-permute-start | bytes 2359304 | tf_op jit(solution)/shard_map/ppermute | solution.py:19
  45.7 7.6 %collective-permute-start.5 = (bf16[4,64,768]{2,1,0:T(8,128)(2,1)S(1)}, bf16[4,64,768]{2,1,0:T(8,128)(2,1)S(1)}, u32[]{:S(2)}, u32[]{:S(2)}) collective-permute-start(bf16[4,64,768]{2,1,0:T(8,128)(2,1)S(1)} %get-tuple-element.17), channel_id=1, source_target_pairs={{0,128},{64,192},{128,256},{192,320},{256,384},{320,448},{384,0},{... | collective-permute-start | bytes 1179656 | tf_op jit(solution)/shard_map/ppermute | solution.py:19
  61.2 4.0 %collective-permute-done.4 = bf16[8,64,768]{2,1,0:T(8,128)(2,1)} collective-permute-done((bf16[8,64,768]{2,1,0:T(8,128)(2,1)S(1)}, bf16[8,64,768]{2,1,0:T(8,128)(2,1)}, u32[]{:S(2)}, u32[]{:S(2)}) %collective-permute-start.4) | collective-permute-done | bytes 786464 | tf_op jit(solution)/shard_map/ppermute | solution.py:19
  72.4 11.7 %collective-permute-done.6 = bf16[4,64,768]{2,1,0:T(8,128)(2,1)S(1)} collective-permute-done((bf16[4,64,768]{2,1,0:T(8,128)(2,1)S(1)}, bf16[4,64,768]{2,1,0:T(8,128)(2,1)S(1)}, u32[]{:S(2)}, u32[]{:S(2)}) %collective-permute-start.6) | collective-permute-done | bytes 393248 | tf_op jit(solution)/shard_map/ppermute | solution.py:19
  95.2 3.8 %convolution_convert_fusion = bf16[128,2048]{1,0:T(8,128)(2,1)S(1)} fusion(bf16[2048,768]{1,0:T(8,128)(2,1)} %bitcast.11, bf16[128,2048]{1,0:T(8,128)(2,1)S(1)} %copy-done, f32[128,384]{0,1:T(8,128)S(1)} %convolution_bitcast_fusion.1), kind=kOutput, calls=%fused_computation.2 | convolution fusion | flops 403210240 | bytes 4390912 | tf_op jit(solution)/shard_map/dot_general | solution.py:23
  99.1 3.7 %collective-permute-start.7 = (bf16[4,32,2048]{2,1,0:T(8,128)(2,1)S(1)}, bf16[4,32,2048]{2,1,0:T(8,128)(2,1)S(1)}, u32[]{:S(2)}, u32[]{:S(2)}) collective-permute-start(bf16[4,32,2048]{2,1,0:T(8,128)(2,1)S(1)} %fusion.30), channel_id=1, source_target_pairs={{0,1},{1,0},{2,3},{3,2},{4,5},{5,4},{6,7},{7,6},{8,9},{9,8},{10,11... | collective-permute-start | bytes 1572872 | tf_op jit(solution)/shard_map/ppermute | solution.py:79
  106.7 4.7 %collective-permute-start.10 = (bf16[32,2048]{1,0:T(8,128)(2,1)S(1)}, bf16[32,2048]{1,0:T(8,128)(2,1)S(1)}, u32[]{:S(2)}, u32[]{:S(2)}) collective-permute-start(bf16[32,2048]{1,0:T(8,128)(2,1)S(1)} %get-tuple-element.28), channel_id=1, source_target_pairs={{0,4},{2,6},{4,0},{6,2},{1,5},{3,7},{5,1},{7,3},{8,12},{10,14},{12... | collective-permute-start | bytes 393224 | tf_op jit(solution)/shard_map/ppermute | solution.py:39
  113.6 4.3 %collective-permute-start.9 = (bf16[32,2048]{1,0:T(8,128)(2,1)S(1)}, bf16[32,2048]{1,0:T(8,128)(2,1)}, u32[]{:S(2)}, u32[]{:S(2)}) collective-permute-start(bf16[32,2048]{1,0:T(8,128)(2,1)S(1)} %get-tuple-element.29), channel_id=1, source_target_pairs={{0,6},{2,0},{4,2},{6,4},{1,7},{3,1},{5,3},{7,5},{8,14},{10,8},{12,... | collective-permute-start | bytes 393224 | tf_op jit(solution)/shard_map/ppermute | solution.py:39
  127.7 3.4 %collective-permute-start.19 = (bf16[128,1152]{1,0:T(8,128)(2,1)}, bf16[128,1152]{1,0:T(8,128)(2,1)S(1)}, u32[]{:S(2)}, u32[]{:S(2)}) collective-permute-start(bf16[128,1152]{1,0:T(8,128)(2,1)} %shard_map.128.refs_8_), channel_id=1, source_target_pairs={{0,448},{64,0},{128,64},{192,128},{256,192},{320,256},{384,320},{4... | collective-permute-start | bytes 884744 | tf_op jit(solution)/shard_map/ppermute | solution.py:19
  131.0 5.0 %collective-permute-start.20 = (bf16[128,1152]{1,0:T(8,128)(2,1)}, bf16[128,1152]{1,0:T(8,128)(2,1)}, u32[]{:S(2)}, u32[]{:S(2)}) collective-permute-start(bf16[128,1152]{1,0:T(8,128)(2,1)} %shard_map.128.refs_8_), channel_id=1, source_target_pairs={{0,384},{64,448},{128,0},{192,64},{256,128},{320,192},{384,256},{4... | collective-permute-start | bytes 884744 | tf_op jit(solution)/shard_map/ppermute | solution.py:19
  140.5 5.4 %collective-permute-done.19.refs_10_ = bf16[128,1152]{1,0:T(8,128)(2,1)S(1)} collective-permute-done((bf16[128,1152]{1,0:T(8,128)(2,1)}, bf16[128,1152]{1,0:T(8,128)(2,1)S(1)}, u32[]{:S(2)}, u32[]{:S(2)}) %collective-permute-start.19) | collective-permute-done | bytes 294944 | tf_op jit(solution)/shard_map/ppermute | solution.py:19
  145.9 13.9 %collective-permute-done.20.refs_11_ = bf16[128,1152]{1,0:T(8,128)(2,1)} collective-permute-done((bf16[128,1152]{1,0:T(8,128)(2,1)}, bf16[128,1152]{1,0:T(8,128)(2,1)}, u32[]{:S(2)}, u32[]{:S(2)}) %collective-permute-start.20) | collective-permute-done | bytes 294944 | tf_op jit(solution)/shard_map/ppermute | solution.py:19
  159.9 4.8 %shard_map.129 = bf16[512,1152]{1,0:T(8,128)(2,1)} custom-call(bf16[128,1024]{1,0:T(8,128)(2,1)} %pad_maximum_fusion.refs_0_.refs_4_, bf16[128,1024]{1,0:T(8,128)(2,1)} %copy-done.2, bf16[128,1024]{1,0:T(8,128)(2,1)} %copy-done.3, bf16[128,1024]{1,0:T(8,128)(2,1)} %copy-done.4, bf16[128,1024]{1,0:T(8,128)(2,1)} %pad_maximum_fusion.refs_0_.refs_4_, ...), custom_call_target="tpu_custom_call" | custom-call | flops 1200000000 | bytes 3400000 | tf_op jit(solution)/shard_map/pallas_call | solution.py:153
  164.6 6.8 %all-to-all-start.2 = ((bf16[8,64,1152]{2,1,0:T(8,128)(2,1)}), bf16[8,64,1152]{2,1,0:T(8,128)(2,1)S(1)}, u32[]{:S(2)}, u32[]{:S(2)}) async-start(bf16[8,64,1152]{2,1,0:T(8,128)(2,1)} %bitcast.89), calls=%async_computation.2 | async-start | bytes 2359296 | tf_op jit(solution)/shard_map/all_to_all | solution.py:238
  177.6 3.7 %collective-permute-done.13 = bf16[32,2048]{1,0:T(8,128)(2,1)S(1)} collective-permute-done((bf16[32,2048]{1,0:T(8,128)(2,1)}, bf16[32,2048]{1,0:T(8,128)(2,1)S(1)}, u32[]{:S(2)}, u32[]{:S(2)}) %collective-permute-start.13) | collective-permute-done | bytes 131104 | tf_op jit(solution)/shard_map/ppermute | solution.py:39
  181.3 4.8 %collective-permute-start.14 = (bf16[4,32,2048]{2,1,0:T(8,128)(2,1)S(1)}, bf16[4,32,2048]{2,1,0:T(8,128)(2,1)S(1)}, u32[]{:S(2)}, u32[]{:S(2)}) collective-permute-start(bf16[4,32,2048]{2,1,0:T(8,128)(2,1)S(1)} %bitcast_dynamic-update-slice_fusion.5), channel_id=1, source_target_pairs={{0,1},{1,0},{2,3},{3,2},{4,5},{5,4},{6,7},{7,6},{8,9},{9,8},{10,11... | collective-permute-start | bytes 1572872 | tf_op jit(solution)/shard_map/ppermute | solution.py:97
  187.8 15.7 %all-to-all-done.2 = bf16[8,64,1152]{2,1,0:T(8,128)(2,1)S(1)} async-done(((bf16[8,64,1152]{2,1,0:T(8,128)(2,1)}), bf16[8,64,1152]{2,1,0:T(8,128)(2,1)S(1)}, u32[]{:S(2)}, u32[]{:S(2)}) %all-to-all-start.2) | async-done | bytes 1179680 | tf_op jit(solution)/shard_map/all_to_all | solution.py:238
  203.6 4.6 %collective-permute-start.21 = (bf16[64,1152]{1,0:T(8,128)(2,1)S(1)}, bf16[64,1152]{1,0:T(8,128)(2,1)S(1)}, u32[]{:S(2)}, u32[]{:S(2)}) collective-permute-start(bf16[64,1152]{1,0:T(8,128)(2,1)S(1)} %reduce_sum.12), channel_id=1, source_target_pairs={{0,256},{256,0},{1,257},{257,1},{2,258},{258,2},{3,259},{259,3},{4... | collective-permute-start | bytes 442376 | tf_op jit(solution)/shard_map/ppermute | solution.py:240
  209.3 9.0 %collective-permute-done.21 = bf16[64,1152]{1,0:T(8,128)(2,1)S(1)} collective-permute-done((bf16[64,1152]{1,0:T(8,128)(2,1)S(1)}, bf16[64,1152]{1,0:T(8,128)(2,1)S(1)}, u32[]{:S(2)}, u32[]{:S(2)}) %collective-permute-start.21) | collective-permute-done | bytes 147488 | tf_op jit(solution)/shard_map/ppermute | solution.py:240
  (106 shorter events, 66.8 us)
Async XLA Ops:
  2.5 30.4 %all-to-all-start.1 = ((bf16[8,64,768]{2,1,0:T(8,128)(2,1)}), bf16[8,64,768]{2,1,0:T(8,128)(2,1)S(1)}, u32[]{:S(2)}, u32[]{:S(2)}) async-start(bf16[8,64,768]{2,1,0:T(8,128)(2,1)} %broadcast_in_dim.69), calls=%async_computation.1 | async-start | bytes 1572864 | tf_op jit(solution)/shard_map/all_to_all | solution.py:47
  9.3 13.1 %collective-permute-start = (bf16[64,384]{1,0:T(8,128)(2,1)S(1)}, bf16[64,384]{1,0:T(8,128)(2,1)S(1)}, u32[]{:S(2)}, u32[]{:S(2)}) collective-permute-start(bf16[64,384]{1,0:T(8,128)(2,1)S(1)} %copy-done.17), channel_id=1, source_target_pairs={{0,64},{64,128},{128,192},{192,256},{256,320},{320,384},{384,448},... | collective-permute-start | bytes 147464 | tf_op jit(solution)/shard_map/ppermute | solution.py:19
  13.3 9.1 %collective-permute-start.1 = (bf16[64,384]{1,0:T(8,128)(2,1)S(1)}, bf16[64,384]{1,0:T(8,128)(2,1)S(1)}, u32[]{:S(2)}, u32[]{:S(2)}) collective-permute-start(bf16[64,384]{1,0:T(8,128)(2,1)S(1)} %copy-done.17), channel_id=1, source_target_pairs={{0,448},{64,0},{128,64},{192,128},{256,192},{320,256},{384,320},{4... | collective-permute-start | bytes 147464 | tf_op jit(solution)/shard_map/ppermute | solution.py:19
  15.3 9.7 %collective-permute-start.2 = (bf16[64,384]{1,0:T(8,128)(2,1)S(1)}, bf16[64,384]{1,0:T(8,128)(2,1)S(1)}, u32[]{:S(2)}, u32[]{:S(2)}) collective-permute-start(bf16[64,384]{1,0:T(8,128)(2,1)S(1)} %copy-done.17), channel_id=1, source_target_pairs={{0,384},{64,448},{128,0},{192,64},{256,128},{320,192},{384,256},{4... | collective-permute-start | bytes 147464 | tf_op jit(solution)/shard_map/ppermute | solution.py:19
  34.3 51.5 %all-to-all-start = ((bf16[8,4,64,384]{3,2,1,0:T(8,128)(2,1)}), bf16[8,4,64,384]{3,2,1,0:T(8,128)(2,1)}, u32[]{:S(2)}, u32[]{:S(2)}) async-start(bf16[8,4,64,384]{3,2,1,0:T(8,128)(2,1)} %broadcast_in_dim.67), calls=%async_computation | async-start | bytes 3145728 | tf_op jit(solution)/shard_map/all_to_all | solution.py:47
  38.8 21.5 %collective-permute-start.3 = (bf16[8,64,768]{2,1,0:T(8,128)(2,1)S(1)}, bf16[8,64,768]{2,1,0:T(8,128)(2,1)S(1)}, u32[]{:S(2)}, u32[]{:S(2)}) collective-permute-start(bf16[8,64,768]{2,1,0:T(8,128)(2,1)S(1)} %all-to-all-done.1), channel_id=1, source_target_pairs={{0,64},{64,128},{128,192},{192,256},{256,320},{320,384},{384,448},... | collective-permute-start | bytes 2359304 | tf_op jit(solution)/shard_map/ppermute | solution.py:19
  42.8 22.5 %collective-permute-start.4 = (bf16[8,64,768]{2,1,0:T(8,128)(2,1)S(1)}, bf16[8,64,768]{2,1,0:T(8,128)(2,1)}, u32[]{:S(2)}, u32[]{:S(2)}) collective-permute-start(bf16[8,64,768]{2,1,0:T(8,128)(2,1)S(1)} %all-to-all-done.1), channel_id=1, source_target_pairs={{0,448},{64,0},{128,64},{192,128},{256,192},{320,256},{384,320},{4... | collective-permute-start | bytes 2359304 | tf_op jit(solution)/shard_map/ppermute | solution.py:19
  45.7 26.7 %collective-permute-start.5 = (bf16[4,64,768]{2,1,0:T(8,128)(2,1)S(1)}, bf16[4,64,768]{2,1,0:T(8,128)(2,1)S(1)}, u32[]{:S(2)}, u32[]{:S(2)}) collective-permute-start(bf16[4,64,768]{2,1,0:T(8,128)(2,1)S(1)} %get-tuple-element.17), channel_id=1, source_target_pairs={{0,128},{64,192},{128,256},{192,320},{256,384},{320,448},{384,0},{... | collective-permute-start | bytes 1179656 | tf_op jit(solution)/shard_map/ppermute | solution.py:19
  53.3 30.8 %collective-permute-start.6 = (bf16[4,64,768]{2,1,0:T(8,128)(2,1)S(1)}, bf16[4,64,768]{2,1,0:T(8,128)(2,1)S(1)}, u32[]{:S(2)}, u32[]{:S(2)}) collective-permute-start(bf16[4,64,768]{2,1,0:T(8,128)(2,1)S(1)} %get-tuple-element.18), channel_id=1, source_target_pairs={{0,384},{64,448},{128,0},{192,64},{256,128},{320,192},{384,256},{4... | collective-permute-start | bytes 1179656 | tf_op jit(solution)/shard_map/ppermute | solution.py:19
  99.1 7.5 %collective-permute-start.7 = (bf16[4,32,2048]{2,1,0:T(8,128)(2,1)S(1)}, bf16[4,32,2048]{2,1,0:T(8,128)(2,1)S(1)}, u32[]{:S(2)}, u32[]{:S(2)}) collective-permute-start(bf16[4,32,2048]{2,1,0:T(8,128)(2,1)S(1)} %fusion.30), channel_id=1, source_target_pairs={{0,1},{1,0},{2,3},{3,2},{4,5},{5,4},{6,7},{7,6},{8,9},{9,8},{10,11... | collective-permute-start | bytes 1572872 | tf_op jit(solution)/shard_map/ppermute | solution.py:79
  103.5 19.1 %collective-permute-start.15 = (bf16[128,1024]{1,0:T(8,128)(2,1)}, bf16[128,1024]{1,0:T(8,128)(2,1)S(1)}, u32[]{:S(2)}, u32[]{:S(2)}) collective-permute-start(bf16[128,1024]{1,0:T(8,128)(2,1)} %pad_maximum_fusion.1), channel_id=1, source_target_pairs={{0,64},{64,128},{128,192},{192,256},{256,320},{320,384},{384,448},... | collective-permute-start | bytes 786440 | tf_op jit(solution)/shard_map/ppermute | solution.py:19
  106.7 19.0 %collective-permute-start.10 = (bf16[32,2048]{1,0:T(8,128)(2,1)S(1)}, bf16[32,2048]{1,0:T(8,128)(2,1)S(1)}, u32[]{:S(2)}, u32[]{:S(2)}) collective-permute-start(bf16[32,2048]{1,0:T(8,128)(2,1)S(1)} %get-tuple-element.28), channel_id=1, source_target_pairs={{0,4},{2,6},{4,0},{6,2},{1,5},{3,7},{5,1},{7,3},{8,12},{10,14},{12... | collective-permute-start | bytes 393224 | tf_op jit(solution)/shard_map/ppermute | solution.py:39
  111.4 16.2 %collective-permute-start.8 = (bf16[32,2048]{1,0:T(8,128)(2,1)S(1)}, bf16[32,2048]{1,0:T(8,128)(2,1)S(1)}, u32[]{:S(2)}, u32[]{:S(2)}) collective-permute-start(bf16[32,2048]{1,0:T(8,128)(2,1)S(1)} %get-tuple-element.27), channel_id=1, source_target_pairs={{0,2},{2,4},{4,6},{6,0},{1,3},{3,5},{5,7},{7,1},{8,10},{10,12},{12... | collective-permute-start | bytes 393224 | tf_op jit(solution)/shard_map/ppermute | solution.py:39
  113.6 17.4 %collective-permute-start.9 = (bf16[32,2048]{1,0:T(8,128)(2,1)S(1)}, bf16[32,2048]{1,0:T(8,128)(2,1)}, u32[]{:S(2)}, u32[]{:S(2)}) collective-permute-start(bf16[32,2048]{1,0:T(8,128)(2,1)S(1)} %get-tuple-element.29), channel_id=1, source_target_pairs={{0,6},{2,0},{4,2},{6,4},{1,7},{3,1},{5,3},{7,5},{8,14},{10,8},{12,... | collective-permute-start | bytes 393224 | tf_op jit(solution)/shard_map/ppermute | solution.py:39
  119.6 18.1 %collective-permute-start.16 = (bf16[128,1024]{1,0:T(8,128)(2,1)}, bf16[128,1024]{1,0:T(8,128)(2,1)S(1)}, u32[]{:S(2)}, u32[]{:S(2)}) collective-permute-start(bf16[128,1024]{1,0:T(8,128)(2,1)} %pad_maximum_fusion.2), channel_id=1, source_target_pairs={{0,448},{64,0},{128,64},{192,128},{256,192},{320,256},{384,320},{4... | collective-permute-start | bytes 786440 | tf_op jit(solution)/shard_map/ppermute | solution.py:19
  122.6 17.9 %collective-permute-start.17 = (bf16[128,1024]{1,0:T(8,128)(2,1)}, bf16[128,1024]{1,0:T(8,128)(2,1)S(1)}, u32[]{:S(2)}, u32[]{:S(2)}) collective-permute-start(bf16[128,1024]{1,0:T(8,128)(2,1)} %pad_maximum_fusion.3), channel_id=1, source_target_pairs={{0,384},{64,448},{128,0},{192,64},{256,128},{320,192},{384,256},{4... | collective-permute-start | bytes 786440 | tf_op jit(solution)/shard_map/ppermute | solution.py:19
  125.7 14.8 %collective-permute-start.18 = (bf16[128,1152]{1,0:T(8,128)(2,1)}, bf16[128,1152]{1,0:T(8,128)(2,1)S(1)}, u32[]{:S(2)}, u32[]{:S(2)}) collective-permute-start(bf16[128,1152]{1,0:T(8,128)(2,1)} %shard_map.128.refs_8_), channel_id=1, source_target_pairs={{0,64},{64,128},{128,192},{192,256},{256,320},{320,384},{384,448},... | collective-permute-start | bytes 884744 | tf_op jit(solution)/shard_map/ppermute | solution.py:19
  127.7 18.3 %collective-permute-start.19 = (bf16[128,1152]{1,0:T(8,128)(2,1)}, bf16[128,1152]{1,0:T(8,128)(2,1)S(1)}, u32[]{:S(2)}, u32[]{:S(2)}) collective-permute-start(bf16[128,1152]{1,0:T(8,128)(2,1)} %shard_map.128.refs_8_), channel_id=1, source_target_pairs={{0,448},{64,0},{128,64},{192,128},{256,192},{320,256},{384,320},{4... | collective-permute-start | bytes 884744 | tf_op jit(solution)/shard_map/ppermute | solution.py:19
  131.0 28.8 %collective-permute-start.20 = (bf16[128,1152]{1,0:T(8,128)(2,1)}, bf16[128,1152]{1,0:T(8,128)(2,1)}, u32[]{:S(2)}, u32[]{:S(2)}) collective-permute-start(bf16[128,1152]{1,0:T(8,128)(2,1)} %shard_map.128.refs_8_), channel_id=1, source_target_pairs={{0,384},{64,448},{128,0},{192,64},{256,128},{320,192},{384,256},{4... | collective-permute-start | bytes 884744 | tf_op jit(solution)/shard_map/ppermute | solution.py:19
  137.7 38.5 %collective-permute-start.11 = (bf16[32,2048]{1,0:T(8,128)(2,1)}, bf16[32,2048]{1,0:T(8,128)(2,1)S(1)}, u32[]{:S(2)}, u32[]{:S(2)}) collective-permute-start(bf16[32,2048]{1,0:T(8,128)(2,1)} %get-tuple-element.14), channel_id=1, source_target_pairs={{0,2},{2,4},{4,6},{6,0},{1,3},{3,5},{5,7},{7,1},{8,10},{10,12},{12... | collective-permute-start | bytes 393224 | tf_op jit(solution)/shard_map/ppermute | solution.py:39
  164.6 38.8 %all-to-all-start.2 = ((bf16[8,64,1152]{2,1,0:T(8,128)(2,1)}), bf16[8,64,1152]{2,1,0:T(8,128)(2,1)S(1)}, u32[]{:S(2)}, u32[]{:S(2)}) async-start(bf16[8,64,1152]{2,1,0:T(8,128)(2,1)} %bitcast.89), calls=%async_computation.2 | async-start | bytes 2359296 | tf_op jit(solution)/shard_map/all_to_all | solution.py:238
  173.6 7.7 %collective-permute-start.13 = (bf16[32,2048]{1,0:T(8,128)(2,1)}, bf16[32,2048]{1,0:T(8,128)(2,1)S(1)}, u32[]{:S(2)}, u32[]{:S(2)}) collective-permute-start(bf16[32,2048]{1,0:T(8,128)(2,1)} %get-tuple-element.14), channel_id=1, source_target_pairs={{0,4},{2,6},{4,0},{6,2},{1,5},{3,7},{5,1},{7,3},{8,12},{10,14},{12... | collective-permute-start | bytes 393224 | tf_op jit(solution)/shard_map/ppermute | solution.py:39
  181.3 6.4 %collective-permute-start.14 = (bf16[4,32,2048]{2,1,0:T(8,128)(2,1)S(1)}, bf16[4,32,2048]{2,1,0:T(8,128)(2,1)S(1)}, u32[]{:S(2)}, u32[]{:S(2)}) collective-permute-start(bf16[4,32,2048]{2,1,0:T(8,128)(2,1)S(1)} %bitcast_dynamic-update-slice_fusion.5), channel_id=1, source_target_pairs={{0,1},{1,0},{2,3},{3,2},{4,5},{5,4},{6,7},{7,6},{8,9},{9,8},{10,11... | collective-permute-start | bytes 1572872 | tf_op jit(solution)/shard_map/ppermute | solution.py:97
  203.6 14.6 %collective-permute-start.21 = (bf16[64,1152]{1,0:T(8,128)(2,1)S(1)}, bf16[64,1152]{1,0:T(8,128)(2,1)S(1)}, u32[]{:S(2)}, u32[]{:S(2)}) collective-permute-start(bf16[64,1152]{1,0:T(8,128)(2,1)S(1)} %reduce_sum.12), channel_id=1, source_target_pairs={{0,256},{256,0},{1,257},{257,1},{2,258},{258,2},{3,259},{259,3},{4... | collective-permute-start | bytes 442376 | tf_op jit(solution)/shard_map/ppermute | solution.py:240
  (19 other events, 336.2 us)

commit v6 on v4

--- a/solution.py
+++ b/solution.py
@@ -142,13 +142,13 @@
     low = far_low.reshape(-1, 2 * width)
     high = far_high.reshape(-1, 2 * width)
 
-    def with_far(total, array, at):
-        n = low.shape[0]
-        total = total + dot(array[:, :n], low[:, at : at + width])
-        return total + dot(array[:, n:], high[:, at : at + width])
-
-    up_early = with_far(near_up, far_x, 0)
-    hidden_grad = with_far(near_grad, far_cot, width)
+    n = low.shape[0]
+    near_up = near_up + dot(far_x[:, :n], low[:, :width])
+    near_grad = near_grad + dot(far_cot[:, :n], low[:, width:])
+    near_up, near_grad = lax.optimization_barrier((near_up, near_grad))
+
+    up_early = near_up + dot(far_x[:, n:], high[:, :width])
+    hidden_grad = near_grad + dot(far_cot[:, n:], high[:, width:])
     sigmoid_gate = jax.nn.sigmoid(gate_early)
     silu_early = gate_early * sigmoid_gate
     gate_grad = (

time: 195 us -> 195 us (level)
  the two profiles are of different devices: /device:TPU:6 before, /device:TPU:64 now
where the time goes in v6:
time: 195 us; the launch traced here: 194 us
  starting transfers between devices  94.1 us (48%)
  waiting for transfers between devices  58.7 us (30%)
  matrix products  16.2 us (8%)
  local copies, waits for them, and re-layouts  12 us (6%)
  other arithmetic  11.4 us (6%)
    ppermute x13, starting transfers between devices, shift_z(): return lax.ppermute(array, RING, [(i, (i + by) % NZ) for i in range(NZ)])  48.6 us
    ppermute x6, starting transfers between devices, shift(): lax.ppermute(array, axis, [(i, (i + by) % count) for i in range(count)])  19.7 us
    ppermute x13, waiting for transfers between devices, shift_z(): return lax.ppermute(array, RING, [(i, (i + by) % NZ) for i in range(NZ)])  15.5 us
    all_to_all x1, waiting for transfers between devices, per_device(): local = lax.all_to_all(local, 'y', split_axis=0, concat_axis=0, tiled=True)  12.6 us
    all_to_all x2, starting transfers between devices, spread_y(): return lax.all_to_all(block, 'y', split_axis=0, concat_axis=0, tiled=True)  10.7 us
    ppermute x6, waiting for transfers between devices, shift(): lax.ppermute(array, axis, [(i, (i + by) % count) for i in range(count)])  10.2 us
    all_to_all x2, waiting for transfers between devices, spread_y(): return lax.all_to_all(block, 'y', split_axis=0, concat_axis=0, tiled=True)  10.1 us
    ppermute x1, waiting for transfers between devices, per_device(): other = lax.ppermute(mine, 'zh', [(0, 1), (1, 0)])  8.55 us
  transfers between devices with their start and end apart: 25, of which 11 were waited for; matrix products, arithmetic and copies ran while one was open for 18% of the time, Pallas kernels for 0%

profile of v6, /device:TPU:64, one launch (start us, length us, event | category | flops | bytes accessed | tf_op | source)
XLA Modules:
  0.0 193.8 jit_solution(5158066250117761921)
XLA Ops:
  0.7 4.4 %collective-permute-start = (bf16[64,384]{1,0:T(8,128)(2,1)}, bf16[64,384]{1,0:T(8,128)(2,1)S(1)}, u32[]{:S(2)}, u32[]{:S(2)}) collective-permute-start(bf16[64,384]{1,0:T(8,128)(2,1)} %param.12), channel_id=1, source_target_pairs={{0,64},{64,128},{128,192},{192,256},{256,320},{320,384},{384,448},... | collective-permute-start | bytes 147464 | tf_op jit(solution)/shard_map/ppermute | solution.py:16
  5.1 4.5 %collective-permute-start.1 = (bf16[64,384]{1,0:T(8,128)(2,1)}, bf16[64,384]{1,0:T(8,128)(2,1)S(1)}, u32[]{:S(2)}, u32[]{:S(2)}) collective-permute-start(bf16[64,384]{1,0:T(8,128)(2,1)} %param.12), channel_id=1, source_target_pairs={{0,448},{64,0},{128,64},{192,128},{256,192},{320,256},{384,320},{4... | collective-permute-start | bytes 147464 | tf_op jit(solution)/shard_map/ppermute | solution.py:16
  9.6 7.1 %collective-permute-start.2 = (bf16[64,384]{1,0:T(8,128)(2,1)}, bf16[64,384]{1,0:T(8,128)(2,1)S(1)}, u32[]{:S(2)}, u32[]{:S(2)}) collective-permute-start(bf16[64,384]{1,0:T(8,128)(2,1)} %param.12), channel_id=1, source_target_pairs={{0,384},{64,448},{128,0},{192,64},{256,128},{320,192},{384,256},{4... | collective-permute-start | bytes 147464 | tf_op jit(solution)/shard_map/ppermute | solution.py:16
  18.5 7.1 %all-to-all-start.1 = ((bf16[8,64,768]{2,1,0:T(8,128)(2,1)}), bf16[8,64,768]{2,1,0:T(8,128)(2,1)S(1)}, u32[]{:S(2)}, u32[]{:S(2)}) async-start(bf16[8,64,768]{2,1,0:T(8,128)(2,1)} %broadcast_in_dim.69), calls=%async_computation.1 | async-start | bytes 1572864 | tf_op jit(solution)/shard_map/all_to_all | solution.py:44
  31.1 3.7 %collective-permute-start.16 = (bf16[128,1024]{1,0:T(8,128)(2,1)}, bf16[128,1024]{1,0:T(8,128)(2,1)}, u32[]{:S(2)}, u32[]{:S(2)}) collective-permute-start(bf16[128,1024]{1,0:T(8,128)(2,1)} %pad_maximum_fusion.5), channel_id=1, source_target_pairs={{0,448},{64,0},{128,64},{192,128},{256,192},{320,256},{384,320},{4... | collective-permute-start | bytes 786440 | tf_op jit(solution)/shard_map/ppermute | solution.py:16
  37.8 10.1 %all-to-all-done.1 = bf16[8,64,768]{2,1,0:T(8,128)(2,1)S(1)} async-done(((bf16[8,64,768]{2,1,0:T(8,128)(2,1)}), bf16[8,64,768]{2,1,0:T(8,128)(2,1)S(1)}, u32[]{:S(2)}, u32[]{:S(2)}) %all-to-all-start.1) | async-done | bytes 786464 | tf_op jit(solution)/shard_map/all_to_all | solution.py:44
  49.3 3.6 %all-to-all-start = ((bf16[8,4,64,384]{3,2,1,0:T(8,128)(2,1)}), bf16[8,4,64,384]{3,2,1,0:T(8,128)(2,1)S(1)}, u32[]{:S(2)}, u32[]{:S(2)}) async-start(bf16[8,4,64,384]{3,2,1,0:T(8,128)(2,1)} %broadcast_in_dim.67), calls=%async_computation | async-start | bytes 3145728 | tf_op jit(solution)/shard_map/all_to_all | solution.py:44
  55.1 3.6 %collective-permute-start.4 = (bf16[8,64,768]{2,1,0:T(8,128)(2,1)S(1)}, bf16[8,64,768]{2,1,0:T(8,128)(2,1)S(1)}, u32[]{:S(2)}, u32[]{:S(2)}) collective-permute-start(bf16[8,64,768]{2,1,0:T(8,128)(2,1)S(1)} %all-to-all-done.1), channel_id=1, source_target_pairs={{0,448},{64,0},{128,64},{192,128},{256,192},{320,256},{384,320},{4... | collective-permute-start | bytes 2359304 | tf_op jit(solution)/shard_map/ppermute | solution.py:16
  61.1 3.1 %collective-permute-start.6 = (bf16[4,64,768]{2,1,0:T(8,128)(2,1)S(1)}, bf16[4,64,768]{2,1,0:T(8,128)(2,1)S(1)}, u32[]{:S(2)}, u32[]{:S(2)}) collective-permute-start(bf16[4,64,768]{2,1,0:T(8,128)(2,1)S(1)} %get-tuple-element.22), channel_id=1, source_target_pairs={{0,384},{64,448},{128,0},{192,64},{256,128},{320,192},{384,256},{4... | collective-permute-start | bytes 1179656 | tf_op jit(solution)/shard_map/ppermute | solution.py:16
  64.3 3.6 %collective-permute-start.5 = (bf16[4,64,768]{2,1,0:T(8,128)(2,1)S(1)}, bf16[4,64,768]{2,1,0:T(8,128)(2,1)S(1)}, u32[]{:S(2)}, u32[]{:S(2)}) collective-permute-start(bf16[4,64,768]{2,1,0:T(8,128)(2,1)S(1)} %get-tuple-element.21), channel_id=1, source_target_pairs={{0,128},{64,192},{128,256},{192,320},{256,384},{320,448},{384,0},{... | collective-permute-start | bytes 1179656 | tf_op jit(solution)/shard_map/ppermute | solution.py:16
  70.8 5.6 %collective-permute-done.3 = bf16[8,64,768]{2,1,0:T(8,128)(2,1)} collective-permute-done((bf16[8,64,768]{2,1,0:T(8,128)(2,1)S(1)}, bf16[8,64,768]{2,1,0:T(8,128)(2,1)}, u32[]{:S(2)}, u32[]{:S(2)}) %collective-permute-start.3) | collective-permute-done | bytes 786464 | tf_op jit(solution)/shard_map/ppermute | solution.py:16
  85.7 5.4 %collective-permute-done.5 = bf16[4,64,768]{2,1,0:T(8,128)(2,1)S(1)} collective-permute-done((bf16[4,64,768]{2,1,0:T(8,128)(2,1)S(1)}, bf16[4,64,768]{2,1,0:T(8,128)(2,1)S(1)}, u32[]{:S(2)}, u32[]{:S(2)}) %collective-permute-start.5) | collective-permute-done | bytes 393248 | tf_op jit(solution)/shard_map/ppermute | solution.py:16
  97.3 5.8 %collective-permute-start.20 = (bf16[128,1152]{0,1:T(8,128)(2,1)}, bf16[128,1152]{0,1:T(8,128)(2,1)S(1)}, u32[]{:S(2)}, u32[]{:S(2)}) collective-permute-start(bf16[128,1152]{0,1:T(8,128)(2,1)} %pad_maximum_fusion.3), channel_id=1, source_target_pairs={{0,384},{64,448},{128,0},{192,64},{256,128},{320,192},{384,256},{4... | collective-permute-start | bytes 884744 | tf_op jit(solution)/shard_map/ppermute | solution.py:16
  103.1 3.2 %collective-permute-start.19 = (bf16[128,1152]{0,1:T(8,128)(2,1)}, bf16[128,1152]{0,1:T(8,128)(2,1)}, u32[]{:S(2)}, u32[]{:S(2)}) collective-permute-start(bf16[128,1152]{0,1:T(8,128)(2,1)} %pad_maximum_fusion.3), channel_id=1, source_target_pairs={{0,448},{64,0},{128,64},{192,128},{256,192},{320,256},{384,320},{4... | collective-permute-start | bytes 884744 | tf_op jit(solution)/shard_map/ppermute | solution.py:16
  109.6 3.8 %convolution_convert_fusion = bf16[128,2048]{1,0:T(8,128)(2,1)S(1)} fusion(bf16[2048,768]{1,0:T(8,128)(2,1)} %bitcast.11, bf16[128,2048]{1,0:T(8,128)(2,1)S(1)} %copy-done, f32[128,384]{0,1:T(8,128)S(1)} %convolution_bitcast_fusion.1), kind=kOutput, calls=%fused_computation.2 | convolution fusion | flops 403210240 | bytes 4390912 | tf_op jit(solution)/shard_map/dot_general | solution.py:20
  122.0 4.9 %collective-permute-start.10 = (bf16[32,2048]{1,0:T(8,128)(2,1)S(1)}, bf16[32,2048]{1,0:T(8,128)(2,1)S(1)}, u32[]{:S(2)}, u32[]{:S(2)}) collective-permute-start(bf16[32,2048]{1,0:T(8,128)(2,1)S(1)} %get-tuple-element.32), channel_id=1, source_target_pairs={{0,4},{2,6},{4,0},{6,2},{1,5},{3,7},{5,1},{7,3},{8,12},{10,14},{12... | collective-permute-start | bytes 393224 | tf_op jit(solution)/shard_map/ppermute | solution.py:36
  126.9 3.1 %collective-permute-start.9 = (bf16[32,2048]{1,0:T(8,128)(2,1)S(1)}, bf16[32,2048]{1,0:T(8,128)(2,1)S(1)}, u32[]{:S(2)}, u32[]{:S(2)}) collective-permute-start(bf16[32,2048]{1,0:T(8,128)(2,1)S(1)} %get-tuple-element.33), channel_id=1, source_target_pairs={{0,6},{2,0},{4,2},{6,4},{1,7},{3,1},{5,3},{7,5},{8,14},{10,8},{12,... | collective-permute-start | bytes 393224 | tf_op jit(solution)/shard_map/ppermute | solution.py:36
  134.2 3.8 %collective-permute-done.8 = bf16[32,2048]{1,0:T(8,128)(2,1)S(1)} collective-permute-done((bf16[32,2048]{1,0:T(8,128)(2,1)S(1)}, bf16[32,2048]{1,0:T(8,128)(2,1)S(1)}, u32[]{:S(2)}, u32[]{:S(2)}) %collective-permute-start.8) | collective-permute-done | bytes 131104 | tf_op jit(solution)/shard_map/ppermute | solution.py:36
  141.3 6.6 %all-to-all-start.2 = ((bf16[8,64,1152]{2,1,0:T(8,128)(2,1)}), bf16[8,64,1152]{2,1,0:T(8,128)(2,1)S(1)}, u32[]{:S(2)}, u32[]{:S(2)}) async-start(bf16[8,64,1152]{2,1,0:T(8,128)(2,1)} %bitcast.91), calls=%async_computation.2 | async-start | bytes 2359296 | tf_op jit(solution)/shard_map/all_to_all | solution.py:186
  147.8 5.1 %collective-permute-start.12 = (bf16[32,2048]{1,0:T(8,128)(2,1)S(1)}, bf16[32,2048]{1,0:T(8,128)(2,1)S(1)}, u32[]{:S(2)}, u32[]{:S(2)}) collective-permute-start(bf16[32,2048]{1,0:T(8,128)(2,1)S(1)} %get-tuple-element.18), channel_id=1, source_target_pairs={{0,6},{2,0},{4,2},{6,4},{1,7},{3,1},{5,3},{7,5},{8,14},{10,8},{12,... | collective-permute-start | bytes 393224 | tf_op jit(solution)/shard_map/ppermute | solution.py:36
  156.3 5.0 %collective-permute-done.13 = bf16[32,2048]{1,0:T(8,128)(2,1)S(1)} collective-permute-done((bf16[32,2048]{1,0:T(8,128)(2,1)S(1)}, bf16[32,2048]{1,0:T(8,128)(2,1)S(1)}, u32[]{:S(2)}, u32[]{:S(2)}) %collective-permute-start.13) | collective-permute-done | bytes 131104 | tf_op jit(solution)/shard_map/ppermute | solution.py:36
  165.2 12.6 %all-to-all-done.2 = bf16[8,64,1152]{2,1,0:T(8,128)(2,1)S(1)} async-done(((bf16[8,64,1152]{2,1,0:T(8,128)(2,1)}), bf16[8,64,1152]{2,1,0:T(8,128)(2,1)S(1)}, u32[]{:S(2)}, u32[]{:S(2)}) %all-to-all-start.2) | async-done | bytes 1179680 | tf_op jit(solution)/shard_map/all_to_all | solution.py:186
  178.0 4.6 %collective-permute-start.21 = (bf16[64,1152]{1,0:T(8,128)(2,1)S(1)}, bf16[64,1152]{1,0:T(8,128)(2,1)S(1)}, u32[]{:S(2)}, u32[]{:S(2)}) collective-permute-start(bf16[64,1152]{1,0:T(8,128)(2,1)S(1)} %reduce_sum.12), channel_id=1, source_target_pairs={{0,256},{256,0},{1,257},{257,1},{2,258},{258,2},{3,259},{259,3},{4... | collective-permute-start | bytes 442376 | tf_op jit(solution)/shard_map/ppermute | solution.py:188
  183.6 8.6 %collective-permute-done.21 = bf16[64,1152]{1,0:T(8,128)(2,1)S(1)} collective-permute-done((bf16[64,1152]{1,0:T(8,128)(2,1)S(1)}, bf16[64,1152]{1,0:T(8,128)(2,1)S(1)}, u32[]{:S(2)}, u32[]{:S(2)}) %collective-permute-start.21) | collective-permute-done | bytes 147488 | tf_op jit(solution)/shard_map/ppermute | solution.py:188
  (105 shorter events, 63.7 us)
Async XLA Ops:
  0.7 34.9 %collective-permute-start = (bf16[64,384]{1,0:T(8,128)(2,1)}, bf16[64,384]{1,0:T(8,128)(2,1)S(1)}, u32[]{:S(2)}, u32[]{:S(2)}) collective-permute-start(bf16[64,384]{1,0:T(8,128)(2,1)} %param.12), channel_id=1, source_target_pairs={{0,64},{64,128},{128,192},{192,256},{256,320},{320,384},{384,448},... | collective-permute-start | bytes 147464 | tf_op jit(solution)/shard_map/ppermute | solution.py:16
  5.1 32.7 %collective-permute-start.1 = (bf16[64,384]{1,0:T(8,128)(2,1)}, bf16[64,384]{1,0:T(8,128)(2,1)S(1)}, u32[]{:S(2)}, u32[]{:S(2)}) collective-permute-start(bf16[64,384]{1,0:T(8,128)(2,1)} %param.12), channel_id=1, source_target_pairs={{0,448},{64,0},{128,64},{192,128},{256,192},{320,256},{384,320},{4... | collective-permute-start | bytes 147464 | tf_op jit(solution)/shard_map/ppermute | solution.py:16
  9.6 28.1 %collective-permute-start.2 = (bf16[64,384]{1,0:T(8,128)(2,1)}, bf16[64,384]{1,0:T(8,128)(2,1)S(1)}, u32[]{:S(2)}, u32[]{:S(2)}) collective-permute-start(bf16[64,384]{1,0:T(8,128)(2,1)} %param.12), channel_id=1, source_target_pairs={{0,384},{64,448},{128,0},{192,64},{256,128},{320,192},{384,256},{4... | collective-permute-start | bytes 147464 | tf_op jit(solution)/shard_map/ppermute | solution.py:16
  18.5 29.4 %all-to-all-start.1 = ((bf16[8,64,768]{2,1,0:T(8,128)(2,1)}), bf16[8,64,768]{2,1,0:T(8,128)(2,1)S(1)}, u32[]{:S(2)}, u32[]{:S(2)}) async-start(bf16[8,64,768]{2,1,0:T(8,128)(2,1)} %broadcast_in_dim.69), calls=%async_computation.1 | async-start | bytes 1572864 | tf_op jit(solution)/shard_map/all_to_all | solution.py:44
  27.9 30.9 %collective-permute-start.17 = (bf16[128,1024]{1,0:T(8,128)(2,1)}, bf16[128,1024]{1,0:T(8,128)(2,1)}, u32[]{:S(2)}, u32[]{:S(2)}) collective-permute-start(bf16[128,1024]{1,0:T(8,128)(2,1)} %pad_maximum_fusion.6), channel_id=1, source_target_pairs={{0,384},{64,448},{128,0},{192,64},{256,128},{320,192},{384,256},{4... | collective-permute-start | bytes 786440 | tf_op jit(solution)/shard_map/ppermute | solution.py:16
  31.1 27.7 %collective-permute-start.16 = (bf16[128,1024]{1,0:T(8,128)(2,1)}, bf16[128,1024]{1,0:T(8,128)(2,1)}, u32[]{:S(2)}, u32[]{:S(2)}) collective-permute-start(bf16[128,1024]{1,0:T(8,128)(2,1)} %pad_maximum_fusion.5), channel_id=1, source_target_pairs={{0,448},{64,0},{128,64},{192,128},{256,192},{320,256},{384,320},{4... | collective-permute-start | bytes 786440 | tf_op jit(solution)/shard_map/ppermute | solution.py:16
  35.5 23.3 %collective-permute-start.15 = (bf16[128,1024]{1,0:T(8,128)(2,1)}, bf16[128,1024]{1,0:T(8,128)(2,1)}, u32[]{:S(2)}, u32[]{:S(2)}) collective-permute-start(bf16[128,1024]{1,0:T(8,128)(2,1)} %pad_maximum_fusion.4), channel_id=1, source_target_pairs={{0,64},{64,128},{128,192},{192,256},{256,320},{320,384},{384,448},... | collective-permute-start | bytes 786440 | tf_op jit(solution)/shard_map/ppermute | solution.py:16
  49.3 45.0 %all-to-all-start = ((bf16[8,4,64,384]{3,2,1,0:T(8,128)(2,1)}), bf16[8,4,64,384]{3,2,1,0:T(8,128)(2,1)S(1)}, u32[]{:S(2)}, u32[]{:S(2)}) async-start(bf16[8,4,64,384]{3,2,1,0:T(8,128)(2,1)} %broadcast_in_dim.67), calls=%async_computation | async-start | bytes 3145728 | tf_op jit(solution)/shard_map/all_to_all | solution.py:44
  52.9 23.6 %collective-permute-start.3 = (bf16[8,64,768]{2,1,0:T(8,128)(2,1)S(1)}, bf16[8,64,768]{2,1,0:T(8,128)(2,1)}, u32[]{:S(2)}, u32[]{:S(2)}) collective-permute-start(bf16[8,64,768]{2,1,0:T(8,128)(2,1)S(1)} %all-to-all-done.1), channel_id=1, source_target_pairs={{0,64},{64,128},{128,192},{192,256},{256,320},{320,384},{384,448},... | collective-permute-start | bytes 2359304 | tf_op jit(solution)/shard_map/ppermute | solution.py:16
  55.1 25.6 %collective-permute-start.4 = (bf16[8,64,768]{2,1,0:T(8,128)(2,1)S(1)}, bf16[8,64,768]{2,1,0:T(8,128)(2,1)S(1)}, u32[]{:S(2)}, u32[]{:S(2)}) collective-permute-start(bf16[8,64,768]{2,1,0:T(8,128)(2,1)S(1)} %all-to-all-done.1), channel_id=1, source_target_pairs={{0,448},{64,0},{128,64},{192,128},{256,192},{320,256},{384,320},{4... | collective-permute-start | bytes 2359304 | tf_op jit(solution)/shard_map/ppermute | solution.py:16
  61.1 31.2 %collective-permute-start.6 = (bf16[4,64,768]{2,1,0:T(8,128)(2,1)S(1)}, bf16[4,64,768]{2,1,0:T(8,128)(2,1)S(1)}, u32[]{:S(2)}, u32[]{:S(2)}) collective-permute-start(bf16[4,64,768]{2,1,0:T(8,128)(2,1)S(1)} %get-tuple-element.22), channel_id=1, source_target_pairs={{0,384},{64,448},{128,0},{192,64},{256,128},{320,192},{384,256},{4... | collective-permute-start | bytes 1179656 | tf_op jit(solution)/shard_map/ppermute | solution.py:16
  64.3 26.8 %collective-permute-start.5 = (bf16[4,64,768]{2,1,0:T(8,128)(2,1)S(1)}, bf16[4,64,768]{2,1,0:T(8,128)(2,1)S(1)}, u32[]{:S(2)}, u32[]{:S(2)}) collective-permute-start(bf16[4,64,768]{2,1,0:T(8,128)(2,1)S(1)} %get-tuple-element.21), channel_id=1, source_target_pairs={{0,128},{64,192},{128,256},{192,320},{256,384},{320,448},{384,0},{... | collective-permute-start | bytes 1179656 | tf_op jit(solution)/shard_map/ppermute | solution.py:16
  97.3 20.3 %collective-permute-start.20 = (bf16[128,1152]{0,1:T(8,128)(2,1)}, bf16[128,1152]{0,1:T(8,128)(2,1)S(1)}, u32[]{:S(2)}, u32[]{:S(2)}) collective-permute-start(bf16[128,1152]{0,1:T(8,128)(2,1)} %pad_maximum_fusion.3), channel_id=1, source_target_pairs={{0,384},{64,448},{128,0},{192,64},{256,128},{320,192},{384,256},{4... | collective-permute-start | bytes 884744 | tf_op jit(solution)/shard_map/ppermute | solution.py:16
  103.1 16.8 %collective-permute-start.19 = (bf16[128,1152]{0,1:T(8,128)(2,1)}, bf16[128,1152]{0,1:T(8,128)(2,1)}, u32[]{:S(2)}, u32[]{:S(2)}) collective-permute-start(bf16[128,1152]{0,1:T(8,128)(2,1)} %pad_maximum_fusion.3), channel_id=1, source_target_pairs={{0,448},{64,0},{128,64},{192,128},{256,192},{320,256},{384,320},{4... | collective-permute-start | bytes 884744 | tf_op jit(solution)/shard_map/ppermute | solution.py:16
  106.3 13.6 %collective-permute-start.18 = (bf16[128,1152]{0,1:T(8,128)(2,1)}, bf16[128,1152]{0,1:T(8,128)(2,1)}, u32[]{:S(2)}, u32[]{:S(2)}) collective-permute-start(bf16[128,1152]{0,1:T(8,128)(2,1)} %pad_maximum_fusion.3), channel_id=1, source_target_pairs={{0,64},{64,128},{128,192},{192,256},{256,320},{320,384},{384,448},... | collective-permute-start | bytes 884744 | tf_op jit(solution)/shard_map/ppermute | solution.py:16
  115.5 6.3 %collective-permute-start.7 = (bf16[4,32,2048]{2,1,0:T(8,128)(2,1)S(1)}, bf16[4,32,2048]{2,1,0:T(8,128)(2,1)S(1)}, u32[]{:S(2)}, u32[]{:S(2)}) collective-permute-start(bf16[4,32,2048]{2,1,0:T(8,128)(2,1)S(1)} %fusion.30), channel_id=1, source_target_pairs={{0,1},{1,0},{2,3},{3,2},{4,5},{5,4},{6,7},{7,6},{8,9},{9,8},{10,11... | collective-permute-start | bytes 1572872 | tf_op jit(solution)/shard_map/ppermute | solution.py:76
  122.0 12.2 %collective-permute-start.10 = (bf16[32,2048]{1,0:T(8,128)(2,1)S(1)}, bf16[32,2048]{1,0:T(8,128)(2,1)S(1)}, u32[]{:S(2)}, u32[]{:S(2)}) collective-permute-start(bf16[32,2048]{1,0:T(8,128)(2,1)S(1)} %get-tuple-element.32), channel_id=1, source_target_pairs={{0,4},{2,6},{4,0},{6,2},{1,5},{3,7},{5,1},{7,3},{8,12},{10,14},{12... | collective-permute-start | bytes 393224 | tf_op jit(solution)/shard_map/ppermute | solution.py:36
  126.9 7.3 %collective-permute-start.9 = (bf16[32,2048]{1,0:T(8,128)(2,1)S(1)}, bf16[32,2048]{1,0:T(8,128)(2,1)S(1)}, u32[]{:S(2)}, u32[]{:S(2)}) collective-permute-start(bf16[32,2048]{1,0:T(8,128)(2,1)S(1)} %get-tuple-element.33), channel_id=1, source_target_pairs={{0,6},{2,0},{4,2},{6,4},{1,7},{3,1},{5,3},{7,5},{8,14},{10,8},{12,... | collective-permute-start | bytes 393224 | tf_op jit(solution)/shard_map/ppermute | solution.py:36
  130.0 8.1 %collective-permute-start.8 = (bf16[32,2048]{1,0:T(8,128)(2,1)S(1)}, bf16[32,2048]{1,0:T(8,128)(2,1)S(1)}, u32[]{:S(2)}, u32[]{:S(2)}) collective-permute-start(bf16[32,2048]{1,0:T(8,128)(2,1)S(1)} %get-tuple-element.31), channel_id=1, source_target_pairs={{0,2},{2,4},{4,6},{6,0},{1,3},{3,5},{5,7},{7,1},{8,10},{10,12},{12... | collective-permute-start | bytes 393224 | tf_op jit(solution)/shard_map/ppermute | solution.py:36
  138.2 16.7 %collective-permute-start.11 = (bf16[32,2048]{1,0:T(8,128)(2,1)S(1)}, bf16[32,2048]{1,0:T(8,128)(2,1)S(1)}, u32[]{:S(2)}, u32[]{:S(2)}) collective-permute-start(bf16[32,2048]{1,0:T(8,128)(2,1)S(1)} %get-tuple-element.18), channel_id=1, source_target_pairs={{0,2},{2,4},{4,6},{6,0},{1,3},{3,5},{5,7},{7,1},{8,10},{10,12},{12... | collective-permute-start | bytes 393224 | tf_op jit(solution)/shard_map/ppermute | solution.py:36
  141.3 36.6 %all-to-all-start.2 = ((bf16[8,64,1152]{2,1,0:T(8,128)(2,1)}), bf16[8,64,1152]{2,1,0:T(8,128)(2,1)S(1)}, u32[]{:S(2)}, u32[]{:S(2)}) async-start(bf16[8,64,1152]{2,1,0:T(8,128)(2,1)} %bitcast.91), calls=%async_computation.2 | async-start | bytes 2359296 | tf_op jit(solution)/shard_map/all_to_all | solution.py:186
  147.8 8.5 %collective-permute-start.12 = (bf16[32,2048]{1,0:T(8,128)(2,1)S(1)}, bf16[32,2048]{1,0:T(8,128)(2,1)S(1)}, u32[]{:S(2)}, u32[]{:S(2)}) collective-permute-start(bf16[32,2048]{1,0:T(8,128)(2,1)S(1)} %get-tuple-element.18), channel_id=1, source_target_pairs={{0,6},{2,0},{4,2},{6,4},{1,7},{3,1},{5,3},{7,5},{8,14},{10,8},{12,... | collective-permute-start | bytes 393224 | tf_op jit(solution)/shard_map/ppermute | solution.py:36
  152.9 8.4 %collective-permute-start.13 = (bf16[32,2048]{1,0:T(8,128)(2,1)S(1)}, bf16[32,2048]{1,0:T(8,128)(2,1)S(1)}, u32[]{:S(2)}, u32[]{:S(2)}) collective-permute-start(bf16[32,2048]{1,0:T(8,128)(2,1)S(1)} %get-tuple-element.18), channel_id=1, source_target_pairs={{0,4},{2,6},{4,0},{6,2},{1,5},{3,7},{5,1},{7,3},{8,12},{10,14},{12... | collective-permute-start | bytes 393224 | tf_op jit(solution)/shard_map/ppermute | solution.py:36
  178.0 14.2 %collective-permute-start.21 = (bf16[64,1152]{1,0:T(8,128)(2,1)S(1)}, bf16[64,1152]{1,0:T(8,128)(2,1)S(1)}, u32[]{:S(2)}, u32[]{:S(2)}) collective-permute-start(bf16[64,1152]{1,0:T(8,128)(2,1)S(1)} %reduce_sum.12), channel_id=1, source_target_pairs={{0,256},{256,0},{1,257},{257,1},{2,258},{258,2},{3,259},{259,3},{4... | collective-permute-start | bytes 442376 | tf_op jit(solution)/shard_map/ppermute | solution.py:188
  (15 other events, 255.1 us)
